TPU v7x, 512 devices: a 8x2x16 block of a 8x16x16 slice. The times are simulated.
512 devices in a mesh: grp: 2 (over y), ep: 16 (over z), tp: 16 (over x, core).
Axes of the slice: x: 8, y: 2, z: 16, core: 2. Of those that a mesh axis runs over, the one named last changes fastest.
The devices are a block of a 8x16x16 slice.
Arguments:
- tokens: bfloat16 [192, 2048], P('grp', 'ep'), parts along dimension 0, may hold values from -70 to 70
- first_gain: float32 [2048], replicated, may hold values from 0.1 to 1.9
- w_query: bfloat16 [2048, 2048], P('ep', 'tp'), may hold values from -0.125 to 0.125
- w_key: bfloat16 [2048, 2048], P('ep', 'tp'), may hold values from -0.125 to 0.125
- w_value: bfloat16 [2048, 4096], P('ep', 'tp'), may hold values from -0.125 to 0.125
- w_outgate: bfloat16 [2048, 4096], P('ep', 'tp'), may hold values from -0.125 to 0.125
- w_input: bfloat16 [2048, 16], replicated, may hold values from -0.125 to 0.125
- w_forget: bfloat16 [2048, 16], replicated, may hold values from -0.125 to 0.125
- input_bias: float32 [16], replicated, may hold values from -3 to 3
- forget_bias: float32 [16], replicated, may hold values from -2 to 5
- head_gain: float32 [4096], replicated, may hold values from 0.1 to 1.9
- w_project: bfloat16 [4096, 2048], P('tp', 'ep'), may hold values from -0.09375 to 0.09375
- cell_state: float32 [192, 16, 128, 256], P(('grp', 'ep'), 'tp'), parts along dimension 0, may hold values from -6 to 6
- norm_state: float32 [192, 16, 128], P(('grp', 'ep'), 'tp'), parts along dimension 0, may hold values from -6 to 6
- max_state: float32 [192, 16], P(('grp', 'ep'), 'tp'), parts along dimension 0, may hold values from -110 to 110
- second_gain: float32 [2048], replicated, may hold values from 0.1 to 1.9
- routes: int32 [192, 2], P('grp'), parts along dimension 0, may hold values from 0 to 15, all different within a row; in each aligned block of 6 rows (0 to 5, 6 to 11, ...) at most 2 rows name the same one
- route_weight: float32 [192, 2], P('grp'), parts along dimension 0, may hold values from 0.2 to 1
- expert_gate: bfloat16 [16, 2048, 4096], P('ep', None, 'tp'), may hold values from -0.125 to 0.125
- expert_up: bfloat16 [16, 2048, 4096], P('ep', None, 'tp'), may hold values from -0.125 to 0.125
- expert_down: bfloat16 [16, 4096, 2048], P('ep', 'tp'), may hold values from -0.09375 to 0.09375
Outputs:
- layer_out: bfloat16 [192, 2048], P('grp', 'ep'), parts along dimension 0
- new_cell: float32 [192, 16, 128, 256], P(('grp', 'ep'), 'tp'), parts along dimension 0
- new_norm: float32 [192, 16, 128], P(('grp', 'ep'), 'tp'), parts along dimension 0
- new_max: float32 [192, 16], P(('grp', 'ep'), 'tp'), parts along dimension 0
There are 2 independent parts, one for each index of `grp`. A program takes and returns all parts, laid end to end along the dimension named above; an argument that names none is the same for every part. Nothing has to cross between parts.
Inputs may be any that keep to these rules, and one draw needn't show every extreme that they name: `routes`: each sequence names 2 different experts. In each aligned block of 6 sequences no expert is named by more than 2 of them, a bound that some block reaches.
All inputs are finite; a program needn't handle non-finite values.
Results may differ from a plain program's by a relative error of at most 0.0065.
Values may be sent and summed in bfloat16 or wider, within the bound.
No kernel may reach another device: no remote copies, remote signals or barrier semaphores. Data moves between devices by JAX's collectives and lax.ppermute only.
A program may use at most 64 MiB of HBM per device.

v0:
```python
import jax
import jax.numpy as jnp
from jax import lax
from jax.sharding import PartitionSpec as P

EXP_DEV = 1


NORM_EPS = 1e-05
HEAD_EPS = 1e-06


def from_everyone(array, axis):
    peers = lax.axis_size(axis)
    return lax.all_to_all(
        jnp.broadcast_to(array[None], (peers, *array.shape)), axis, 0, 0, tiled=True
    )


def taken_together(array, axis):
    everything = from_everyone(array, axis)
    return jnp.sum(everything, axis=0)


def in_one(arrays, axis):
    ends = [0]
    for a in arrays:
        ends.append(ends[-1] + a.size)
    subtotal = taken_together(jnp.concatenate([a.ravel() for a in arrays]), axis)
    return tuple((subtotal[b:e].reshape(a.shape) for a, b, e in zip(arrays, ends, ends[1:])))


def cut_along(array, dim, peers):
    lengths = array.shape
    blocks = array.reshape(*lengths[:dim], peers, lengths[dim] // peers, *lengths[dim + 1 :])
    return jnp.moveaxis(blocks, dim, 0)


def summed_on_arrival(array, axis, dim):
    blocks = cut_along(array, dim, lax.axis_size(axis))
    arrived = lax.all_to_all(blocks, axis, split_axis=0, concat_axis=0, tiled=True)
    return arrived.astype(jnp.float32).sum(axis=0)


def summed_on_arrival_2(array, axis, dim):
    blocks = cut_along(array, dim, lax.axis_size(axis))
    arrived = lax.all_to_all(blocks, axis, split_axis=0, concat_axis=0, tiled=True)
    return arrived.sum(axis=0)


def side_by_side(arrays, axis, dim, along):
    ends, at = ([], 0)
    for a in arrays[:-1]:
        at += a.shape[along]
        ends.append(at)
    both = jnp.concatenate(arrays, axis=along)
    return tuple(jnp.split(summed_on_arrival_2(both, axis, dim), ends, axis=along))


def joined_along(blocks, dim):
    lengths = list(blocks.shape[1:])
    lengths[dim] *= blocks.shape[0]
    return jnp.moveaxis(blocks, 0, dim).reshape(lengths)


def gather_directly(array, axis, dim):
    return joined_along(from_everyone(array, axis), dim)


def gathered_total(array, axis):
    blocks = lax.all_gather(array, axis)
    return blocks.sum(axis=0)


def row_norm(stream_rows, gain_whole):
    col_count = stream_rows.shape[1]
    gain_cols = lax.dynamic_slice_in_dim(gain_whole, lax.axis_index("ep") * col_count, col_count, 0)
    values = stream_rows.astype(jnp.float32)
    totals, squares = in_one((jnp.sum(values, axis=1), jnp.sum(values * values, axis=1)), "ep")
    features = col_count * lax.axis_size("ep")
    row_mean = totals / features
    spread = squares / features - row_mean * row_mean
    inv_scale = lax.rsqrt(spread + NORM_EPS)
    return ((values - row_mean[:, None]) * inv_scale[:, None] * gain_cols).astype(jnp.bfloat16)


def expert_act(gate_sum, up_sum):
    return (jax.nn.silu(gate_sum) * up_sum).astype(jnp.bfloat16)


def scatter_slots(active, expert_down):
    slot_major = jnp.moveaxis(active, 1, 0)
    return summed_on_arrival(
        jnp.einsum(
            "pef,efd->ped", slot_major, expert_down, preferred_element_type=jnp.float32
        ).astype(jnp.bfloat16),
        "tp",
        0,
    ).astype(jnp.bfloat16)


def on_device(
    tokens,
    first_gain,
    w_query,
    w_key,
    w_value,
    w_outgate,
    w_input,
    w_forget,
    input_bias,
    forget_bias,
    head_gain,
    w_project,
    cell_state,
    norm_state,
    max_state,
    second_gain,
    routes,
    route_weight,
    expert_gate,
    expert_up,
    expert_down,
):
    blocks = lax.axis_size("ep")
    columns = tokens.shape[1]
    seq_total = tokens.shape[0]
    seq_local = seq_total // blocks
    heads_local = cell_state.shape[1]
    key_size = cell_state.shape[2]
    value_size = cell_state.shape[3]
    col_start = lax.axis_index("ep") * columns
    head_start = lax.axis_index("tp") * heads_local
    normed = row_norm(tokens, first_gain)
    input_cols = lax.dynamic_slice(w_input, (col_start, head_start), (columns, heads_local))
    forget_cols = lax.dynamic_slice(w_forget, (col_start, head_start), (columns, heads_local))

    def project_part(weight):
        return jnp.dot(normed, weight, preferred_element_type=jnp.float32)

    summed = side_by_side(
        (
            project_part(w_query),
            project_part(w_key),
            project_part(w_value),
            project_part(w_outgate),
            project_part(input_cols),
            project_part(forget_cols),
        ),
        "ep",
        0,
        1,
    )
    queries = summed[0].astype(jnp.bfloat16).reshape(seq_local, heads_local, key_size)
    key_rows = summed[1].astype(jnp.bfloat16).reshape(seq_local, heads_local, key_size)
    value_rows = summed[2].astype(jnp.bfloat16).reshape(seq_local, heads_local, value_size)
    outgate = summed[3].astype(jnp.bfloat16)
    input_pre = summed[4] + lax.dynamic_slice_in_dim(input_bias, head_start, heads_local, 0)
    forget_pre = summed[5] + lax.dynamic_slice_in_dim(forget_bias, head_start, heads_local, 0)
    carried = jax.nn.log_sigmoid(forget_pre) + max_state
    new_max = jnp.maximum(carried, input_pre)
    keep_old = jnp.exp(carried - new_max)
    admit_new = jnp.exp(input_pre - new_max)
    key_float = key_rows.astype(jnp.float32)
    value_float = value_rows.astype(jnp.float32)
    new_cell = (
        keep_old[:, :, None, None] * cell_state
        + admit_new[:, :, None, None] * key_float[:, :, :, None] * value_float[:, :, None, :]
    )
    new_norm = keep_old[:, :, None] * norm_state + admit_new[:, :, None] * key_float
    query_float = queries.astype(jnp.float32) * key_size ** (-0.5)
    readout = jnp.einsum("shk,shkv->shv", query_float, new_cell, precision=lax.Precision.HIGHEST)
    head_mean = jnp.mean(readout, axis=2, keepdims=True)
    centred = readout - head_mean
    head_var = jnp.mean(centred * centred, axis=2, keepdims=True)
    gains_here = lax.dynamic_slice_in_dim(
        head_gain, head_start * value_size, heads_local * value_size, 0
    )
    mixed_heads = (
        (centred * lax.rsqrt(head_var + HEAD_EPS)).reshape(seq_local, heads_local * value_size)
        * gains_here
        * jax.nn.sigmoid(outgate.astype(jnp.float32))
    ).astype(jnp.bfloat16)
    head_terms = jnp.dot(
        gather_directly(mixed_heads, "ep", 0), w_project, preferred_element_type=jnp.float32
    )
    mixer_out = gathered_total(head_terms, "tp")
    stream = (tokens.astype(jnp.float32) + mixer_out).astype(jnp.bfloat16)
    second_normed = row_norm(stream, second_gain)
    experts = blocks * EXP_DEV
    top_count = routes.shape[1]
    capacity = max(2, 2 * seq_local * top_count // experts)
    slot_count = blocks * capacity
    expert_ids = lax.broadcasted_iota(jnp.int32, (1, 1, experts), 2)
    matches = routes[:, :, None] == expert_ids
    routed = jnp.sum(matches.astype(jnp.int32), axis=1)
    combine = jnp.sum(jnp.where(matches, route_weight[:, :, None], 0.0), axis=1)
    running = (
        jnp.cumsum(routed.reshape(blocks, seq_local, experts), axis=1).reshape(seq_total, experts)
        - routed
    )
    block_ids = lax.broadcasted_iota(jnp.int32, (seq_total, experts), 0) // seq_local
    slot_of = block_ids * capacity + running
    slot_ids = lax.broadcasted_iota(jnp.int32, (experts, slot_count, seq_total), 1)
    placed = (slot_of.T[:, None, :] == slot_ids) & (routed.T[:, None, :] > 0)
    picker = placed.astype(jnp.bfloat16)
    weighted = jnp.where(placed, combine.T[:, None, :], 0.0)
    outbound = jnp.einsum(
        "eps,sd->epd", picker, second_normed, preferred_element_type=jnp.float32
    ).astype(jnp.bfloat16)
    arrived = lax.all_to_all(outbound, "ep", split_axis=0, concat_axis=2, tiled=True)
    gate_sum = jnp.einsum("end,edf->enf", arrived, expert_gate, preferred_element_type=jnp.float32)
    up_sum = jnp.einsum("end,edf->enf", arrived, expert_up, preferred_element_type=jnp.float32)
    active = expert_act(gate_sum, up_sum)
    share = scatter_slots(active, expert_down)
    back = lax.all_to_all(share, "ep", split_axis=2, concat_axis=1, tiled=True)
    every_slot = gather_directly(back, "tp", 0)
    moe_out = jnp.einsum(
        "eps,ped->sd", weighted, every_slot.astype(jnp.float32), precision=lax.Precision.HIGHEST
    )
    layer_out = (stream.astype(jnp.float32) + moe_out).astype(jnp.bfloat16)
    return (layer_out, new_cell, new_norm, new_max)


def solution(mesh):
    placed = (
        P("grp", "ep"),
        P(),
        P("ep", "tp"),
        P("ep", "tp"),
        P("ep", "tp"),
        P("ep", "tp"),
        P(),
        P(),
        P(),
        P(),
        P(),
        P("tp", "ep"),
        P(("grp", "ep"), "tp", None, None),
        P(("grp", "ep"), "tp", None),
        P(("grp", "ep"), "tp"),
        P(),
        P("grp", None),
        P("grp", None),
        P("ep", None, "tp"),
        P("ep", None, "tp"),
        P("ep", "tp", None),
    )
    return jax.shard_map(
        on_device,
        mesh=mesh,
        in_specs=placed,
        out_specs=(
            P("grp", "ep"),
            P(("grp", "ep"), "tp", None, None),
            P(("grp", "ep"), "tp", None),
            P(("grp", "ep"), "tp"),
        ),
        check_vma=False,
    )
```

profile of v0, /device:TPU:80, one launch (start us, length us, event | category | flops | bytes accessed | tf_op | source)
XLA Modules:
  0.0 230.9 jit_solution(2197950431508416456)
XLA Ops:
  0.6 0.9 convert_reduce_fusion.1
  2.3 43.7 %all-to-all-start = ((f32[16,1,192]{2,1,0:T(1,128)}), f32[16,1,192]{2,1,0:T(1,128)S(1)}, u32[]{:S(2)}, u32[]{:S(2)}) async-start(f32[16,1,192]{2,1,0:T(1,128)} %broadcast_in_dim.26), calls=%async_computation | async-start | bytes 32768 | tf_op jit(solution)/shard_map/all_to_all | solution.py:15
  46.0 0.8 dynamic_slice.21
  46.8 11.5 %all-to-all-done = f32[16,1,192]{2,1,0:T(1,128)S(1)} async-done(((f32[16,1,192]{2,1,0:T(1,128)}), f32[16,1,192]{2,1,0:T(1,128)S(1)}, u32[]{:S(2)}, u32[]{:S(2)}) %all-to-all-start) | async-done | bytes 12320 | tf_op jit(solution)/shard_map/all_to_all | solution.py:15
  58.5 0.9 fusion.46
  59.5 0.9 fusion.48
  60.5 0.6 copy-done.9
  61.3 0.7 copy-done.10
  63.2 0.8 copy-done.7
  64.2 0.9 concatenate.23
  65.1 4.1 %all-to-all-start.1 = ((f32[16,6,770]{2,1,0:T(8,128)}), f32[16,6,770]{2,1,0:T(8,128)S(1)}, u32[]{:S(2)}, u32[]{:S(2)}) async-start(f32[16,6,770]{2,1,0:T(8,128)} %concatenate.23), calls=%async_computation.1 | async-start | bytes 917504 | tf_op jit(solution)/shard_map/all_to_all | solution.py:47
  72.1 0.8 dynamic_slice.26
  72.9 20.5 %all-to-all-done.1 = f32[16,6,770]{2,1,0:T(8,128)S(1)} async-done(((f32[16,6,770]{2,1,0:T(8,128)}), f32[16,6,770]{2,1,0:T(8,128)S(1)}, u32[]{:S(2)}, u32[]{:S(2)}) %all-to-all-start.1) | async-done | bytes 295712 | tf_op jit(solution)/shard_map/all_to_all | solution.py:47
  93.4 1.5 exponential_reduce_fusion.1
  96.8 7.2 %all-to-all-start.2 = ((bf16[16,6,256]{2,1,0:T(8,128)(2,1)}), bf16[16,6,256]{2,1,0:T(8,128)(2,1)S(1)}, u32[]{:S(2)}, u32[]{:S(2)}) async-start(bf16[16,6,256]{2,1,0:T(8,128)(2,1)} %broadcast_in_dim.27), calls=%async_computation.2 | async-start | bytes 131072 | tf_op jit(solution)/shard_map/all_to_all | solution.py:15
  104.0 12.5 %all-to-all-done.2 = bf16[16,6,256]{2,1,0:T(8,128)(2,1)S(1)} async-done(((bf16[16,6,256]{2,1,0:T(8,128)(2,1)}), bf16[16,6,256]{2,1,0:T(8,128)(2,1)S(1)}, u32[]{:S(2)}, u32[]{:S(2)}) %all-to-all-start.2) | async-done | bytes 49184 | tf_op jit(solution)/shard_map/all_to_all | solution.py:15
  116.7 20.2 %all-gather = f32[1536,128]{1,0:T(8,128)S(1)} all-gather(f32[96,128]{1,0:T(8,128)S(1)} %fusion.74), channel_id=2, replica_groups=mesh['grp'=2,'ep'=16,'tp'=16] {'tp'}, dimensions={0}, use_global_device_ids=true | all-gather | bytes 835584 | tf_op jit(solution)/shard_map/all_gather | solution.py:71
  137.7 3.9 %all-to-all-start.3 = ((f32[16,1,192]{2,1,0:T(1,128)}), f32[16,1,192]{2,1,0:T(1,128)S(1)}, u32[]{:S(2)}, u32[]{:S(2)}) async-start(f32[16,1,192]{2,1,0:T(1,128)} %broadcast_in_dim.32), calls=%async_computation.3 | async-start | bytes 32768 | tf_op jit(solution)/shard_map/all_to_all | solution.py:15
  141.6 0.8 dynamic_slice.27
  142.4 11.4 %all-to-all-done.3 = f32[16,1,192]{2,1,0:T(1,128)S(1)} async-done(((f32[16,1,192]{2,1,0:T(1,128)}), f32[16,1,192]{2,1,0:T(1,128)S(1)}, u32[]{:S(2)}, u32[]{:S(2)}) %all-to-all-start.3) | async-done | bytes 12320 | tf_op jit(solution)/shard_map/all_to_all | solution.py:15
  154.2 16.6 %all_to_all.56 = bf16[16,32,128]{2,1,0:T(8,128)(2,1)S(1)} all-to-all(bf16[16,32,128]{2,1,0:T(8,128)(2,1)S(1)} %convolution_convert_fusion.1), channel_id=1, replica_groups=mesh['grp'=2,'ep'=16,'tp'=16] {'ep'}, dimensions={0} | all-to-all | bytes 262144 | tf_op jit(solution)/shard_map/all_to_all | solution.py:211
  171.1 0.7 fusion
  172.0 12.8 %all_to_all.57 = bf16[16,2,1,2048]{3,1,2,0:T(2,128)(2,1)S(1)} all-to-all(bf16[16,2,1,2048]{3,1,2,0:T(2,128)(2,1)S(1)} %bitcast.105), channel_id=1, replica_groups=mesh['grp'=2,'ep'=16,'tp'=16] {'tp'}, dimensions={0} | all-to-all | bytes 262144 | tf_op jit(solution)/shard_map/all_to_all | solution.py:41
  184.9 0.9 copy.101
  186.3 11.5 %reduce.12 = bf16[2048,2]{1,0:T(8,128)(2,1)S(1)} reduce(bf16[2048,1,2]{2,1,0:T(2,128)(2,1)S(1)} %bitcast.99, bf16[]{:T(256)} %broadcast.140), dimensions={1}, to_apply=%bitcast.86.reduce_sub_computation | reduce | bytes 16386
  197.8 0.6 reshape.218
  198.5 16.4 %all_to_all.58 = bf16[16,2,128]{2,1,0:T(2,128)(2,1)S(1)} all-to-all(bf16[16,2,128]{2,1,0:T(2,128)(2,1)S(1)} %reshape.218), channel_id=1, replica_groups=mesh['grp'=2,'ep'=16,'tp'=16] {'ep'}, dimensions={0} | all-to-all | bytes 16384 | tf_op jit(solution)/shard_map/all_to_all | solution.py:216
  214.9 1.2 reshape.219
  216.8 0.7 broadcast_in_dim.34
  217.5 4.1 %all-to-all-start.7 = ((bf16[16,2,16,128]{3,1,2,0:T(2,128)(2,1)}), bf16[16,2,16,128]{3,1,2,0:T(2,128)(2,1)S(1)}, u32[]{:S(2)}, u32[]{:S(2)}) async-start(bf16[16,2,16,128]{3,1,2,0:T(2,128)(2,1)} %broadcast_in_dim.34), calls=%async_computation.7 | async-start | bytes 262144 | tf_op jit(solution)/shard_map/all_to_all | solution.py:15
  223.0 6.9 %all-to-all-done.7 = bf16[16,2,16,128]{3,1,2,0:T(2,128)(2,1)S(1)} async-done(((bf16[16,2,16,128]{3,1,2,0:T(2,128)(2,1)}), bf16[16,2,16,128]{3,1,2,0:T(2,128)(2,1)S(1)}, u32[]{:S(2)}, u32[]{:S(2)}) %all-to-all-start.7) | async-done | bytes 131104 | tf_op jit(solution)/shard_map/all_to_all | solution.py:15
  230.0 1.0 fusion.2
  (94 shorter events, 11.9 us)
Async XLA Ops:
  0.6 170.5 %copy-start = (bf16[1,256,2048]{2,1,0:T(8,128)(2,1)S(1)}, bf16[1,256,2048]{2,1,0:T(8,128)(2,1)}, u32[]{:S(2)}) copy-start(bf16[1,256,2048]{2,1,0:T(8,128)(2,1)} %param.41) | copy-start | bytes 3145732
  2.3 56.0 %all-to-all-start = ((f32[16,1,192]{2,1,0:T(1,128)}), f32[16,1,192]{2,1,0:T(1,128)S(1)}, u32[]{:S(2)}, u32[]{:S(2)}) async-start(f32[16,1,192]{2,1,0:T(1,128)} %broadcast_in_dim.26), calls=%async_computation | async-start | bytes 32768 | tf_op jit(solution)/shard_map/all_to_all | solution.py:15
  46.0 12.4 %copy-start.5 = (bf16[96,128]{1,0:T(8,128)(2,1)S(1)}, bf16[96,128]{1,0:T(8,128)(2,1)}, u32[]{:S(2)}) copy-start(bf16[96,128]{1,0:T(8,128)(2,1)} %param.21) | copy-start | bytes 73732
  60.4 0.8 copy-start.9
  61.3 0.8 copy-start.10
  62.2 0.8 copy-start.6
  63.2 0.9 copy-start.7
  65.1 30.0 %copy-start.4 = (f32[6,1,128,256]{3,2,1,0:T(8,128)S(1)}, f32[6,1,128,256]{3,2,1,0:T(8,128)}, u32[]{:S(2)}) copy-start(f32[6,1,128,256]{3,2,1,0:T(8,128)} %param.33) | copy-start | bytes 2359300
  65.1 28.3 %all-to-all-start.1 = ((f32[16,6,770]{2,1,0:T(8,128)}), f32[16,6,770]{2,1,0:T(8,128)S(1)}, u32[]{:S(2)}, u32[]{:S(2)}) async-start(f32[16,6,770]{2,1,0:T(8,128)} %concatenate.23), calls=%async_computation.1 | async-start | bytes 917504 | tf_op jit(solution)/shard_map/all_to_all | solution.py:47
  69.2 0.7 copy-start.15
  69.9 0.7 copy-start.16
  70.5 0.7 copy-start.14
  71.2 0.7 copy-start.11
  95.2 41.6 %copy-start.1 = (f32[6,1,128,256]{3,2,1,0:T(8,128)}, f32[6,1,128,256]{3,2,1,0:T(8,128)S(1)}, u32[]{:S(2)}) copy-start(f32[6,1,128,256]{3,2,1,0:T(8,128)S(1)} %multiply_add_fusion) | copy-start | bytes 2359300
  96.8 19.7 %all-to-all-start.2 = ((bf16[16,6,256]{2,1,0:T(8,128)(2,1)}), bf16[16,6,256]{2,1,0:T(8,128)(2,1)S(1)}, u32[]{:S(2)}, u32[]{:S(2)}) async-start(bf16[16,6,256]{2,1,0:T(8,128)(2,1)} %broadcast_in_dim.27), calls=%async_computation.2 | async-start | bytes 131072 | tf_op jit(solution)/shard_map/all_to_all | solution.py:15
  104.0 12.6 %copy-start.8 = (bf16[256,128]{1,0:T(8,128)(2,1)S(1)}, bf16[256,128]{1,0:T(8,128)(2,1)}, u32[]{:S(2)}) copy-start(bf16[256,128]{1,0:T(8,128)(2,1)} %param.32) | copy-start | bytes 196612
  136.8 34.0 %copy-start.3 = (bf16[1,2048,256]{2,1,0:T(8,128)(2,1)S(1)}, bf16[1,2048,256]{2,1,0:T(8,128)(2,1)}, u32[]{:S(2)}) copy-start(bf16[1,2048,256]{2,1,0:T(8,128)(2,1)} %param.39) | copy-start | bytes 3145732
  137.0 34.1 %copy-start.2 = (bf16[1,2048,256]{2,1,0:T(8,128)(2,1)S(1)}, bf16[1,2048,256]{2,1,0:T(8,128)(2,1)}, u32[]{:S(2)}) copy-start(bf16[1,2048,256]{2,1,0:T(8,128)(2,1)} %param.40) | copy-start | bytes 3145732
  137.7 16.1 %all-to-all-start.3 = ((f32[16,1,192]{2,1,0:T(1,128)}), f32[16,1,192]{2,1,0:T(1,128)S(1)}, u32[]{:S(2)}, u32[]{:S(2)}) async-start(f32[16,1,192]{2,1,0:T(1,128)} %broadcast_in_dim.32), calls=%async_computation.3 | async-start | bytes 32768 | tf_op jit(solution)/shard_map/all_to_all | solution.py:15
  217.5 4.1 %copy-start.13 = (f32[96,2]{0,1:T(2,128)S(1)}, f32[96,2]{0,1:T(2,128)}, u32[]{:S(2)}) copy-start(f32[96,2]{0,1:T(2,128)} %param.38) | copy-start | bytes 2308
  217.5 12.4 %all-to-all-start.7 = ((bf16[16,2,16,128]{3,1,2,0:T(2,128)(2,1)}), bf16[16,2,16,128]{3,1,2,0:T(2,128)(2,1)S(1)}, u32[]{:S(2)}, u32[]{:S(2)}) async-start(bf16[16,2,16,128]{3,1,2,0:T(2,128)(2,1)} %broadcast_in_dim.34), calls=%async_computation.7 | async-start | bytes 262144 | tf_op jit(solution)/shard_map/all_to_all | solution.py:15
  221.6 0.7 copy-start.12
where the time goes:
time: 234 us; the launch traced here: 231 us
  blocking collectives  66 us (28%)
  starting transfers between devices  63 us (27%)
  waiting for transfers between devices  62.8 us (27%)
  local copies, waits for them, and re-layouts  17.4 us (7%)
  other arithmetic  15.6 us (7%)
  matrix products  5.14 us (2%)
    all_to_all x4, starting transfers between devices, from_everyone(): lax.all_to_all(jnp.broadcast_to(array[None], (peers, *array.shape)), axis...  58.9 us
    all_to_all x4, waiting for transfers between devices, from_everyone(): lax.all_to_all(jnp.broadcast_to(array[None], (peers, *array.shape)), axis...  42.3 us
    all_to_all x1, waiting for transfers between devices, summed_on_arrival_2(): lax.all_to_all(blocks, axis, split_axis=0, concat_axis=0, tiled=True)  20.5 us
    all_gather x1, blocking collectives, gathered_total(): blocks = lax.all_gather(array, axis)  20.2 us
    all_to_all x1, blocking collectives, on_device(): lax.all_to_all(outbound, 'ep', split_axis=0, concat_axis=2, tiled=True)  16.6 us
    all_to_all x1, blocking collectives, on_device(): back = lax.all_to_all(share, 'ep', split_axis=2, concat_axis=1, tiled=True)  16.4 us
    all_to_all x1, blocking collectives, summed_on_arrival(): lax.all_to_all(blocks, axis, split_axis=0, concat_axis=0, tiled=True)  12.8 us
    unnamed x1, other arithmetic  11.5 us
  transfers between devices with their start and end apart: 5, of which 5 were waited for; matrix products, arithmetic and copies ran while one was open for 2% of the time, Pallas kernels for 0%

commit v1 on v0

v1 whole, which is shorter than its diff:
```python
import jax
import jax.numpy as jnp
from jax import lax
from jax.sharding import PartitionSpec as P

NORM_EPS = 1e-05
HEAD_EPS = 1e-06
CAPACITY = 2


def exchanged(blocks, axis):
    return lax.all_to_all(blocks, axis, split_axis=0, concat_axis=0, tiled=True)


def from_everyone(array, axis):
    peers = lax.axis_size(axis)
    return exchanged(jnp.broadcast_to(array[None], (peers, *array.shape)), axis)


def in_pieces(values, count):
    pieces = []
    for _ in range(count - 1):
        head = lax.reduce_precision(values, 8, 7)
        pieces.append(head)
        values = values - head
    pieces.append(values)
    return pieces


def summed_over_tp(part):
    return jnp.sum(lax.all_gather(part.astype(jnp.bfloat16), "tp").astype(jnp.float32), axis=0)


def on_device(
    tokens,
    first_gain,
    w_query,
    w_key,
    w_value,
    w_outgate,
    w_input,
    w_forget,
    input_bias,
    forget_bias,
    head_gain,
    w_project,
    cell_state,
    norm_state,
    max_state,
    second_gain,
    routes,
    route_weight,
    expert_gate,
    expert_up,
    expert_down,
):
    blocks = lax.axis_size("ep")
    seq_total, columns = tokens.shape
    seq_local = seq_total // blocks
    key_size = cell_state.shape[2]
    value_size = cell_state.shape[3]
    features = columns * blocks
    col_start = lax.axis_index("ep") * columns
    head = lax.axis_index("tp")

    experts = blocks
    slot_count = blocks * CAPACITY
    expert_ids = lax.broadcasted_iota(jnp.int32, (1, 1, experts), 2)
    matches = routes[:, :, None] == expert_ids
    routed = jnp.sum(matches.astype(jnp.int32), axis=1)
    combine = jnp.sum(jnp.where(matches, route_weight[:, :, None], 0.0), axis=1)
    running = (
        jnp.cumsum(routed.reshape(blocks, seq_local, experts), axis=1).reshape(seq_total, experts)
        - routed
    )
    block_ids = lax.broadcasted_iota(jnp.int32, (seq_total, experts), 0) // seq_local
    slot_of = block_ids * CAPACITY + running
    slot_ids = lax.broadcasted_iota(jnp.int32, (experts, slot_count, seq_total), 1)
    placed = (slot_of.T[:, None, :] == slot_ids) & (routed.T[:, None, :] > 0)
    picker = placed.astype(jnp.bfloat16)
    weighted = jnp.where(placed, combine.T[:, None, :], 0.0)

    gains = lax.dynamic_slice_in_dim(first_gain, col_start, columns, 0)
    input_cols = lax.dynamic_slice(w_input, (col_start, head), (columns, 1))
    forget_cols = lax.dynamic_slice(w_forget, (col_start, head), (columns, 1))
    weights = jnp.concatenate(
        [w_query, w_key, w_value, w_outgate, input_cols, forget_cols], axis=1
    )
    gained = (weights.astype(jnp.float32) * gains[:, None]).astype(jnp.bfloat16)
    rows = jnp.concatenate([tokens, jnp.ones((1, columns), jnp.bfloat16)], axis=0)
    product = jnp.dot(rows, gained, preferred_element_type=jnp.float32)
    col_sums = product[seq_total:]
    values = tokens.astype(jnp.float32)
    block_mean = jnp.mean(values, axis=1, keepdims=True)
    offsets = values - block_mean
    moment = jnp.sum(offsets * offsets, axis=1, keepdims=True)
    centred = product[:seq_total] - block_mean * col_sums
    width = weights.shape[1] - 2

    def laid_out(part, mean_part, moment_part):
        gate = in_pieces(part[:, width:], 2)
        return jnp.concatenate(
            [part[:, :width], *gate, *in_pieces(mean_part, 3), *in_pieces(moment_part, 2)], axis=1
        )

    row_part = laid_out(centred, block_mean, moment).reshape(blocks, seq_local, -1)
    nothing = jnp.zeros((1, 1), jnp.float32)
    sum_part = laid_out(col_sums, nothing, nothing)
    outgoing = jnp.concatenate(
        [row_part, jnp.broadcast_to(sum_part[None], (blocks, 1, sum_part.shape[1]))], axis=1
    ).astype(jnp.bfloat16)
    incoming = exchanged(outgoing, "ep").astype(jnp.float32)

    means = jnp.sum(incoming[:, :seq_local, width + 4 : width + 7], axis=2, keepdims=True)
    moments = jnp.sum(incoming[:, :seq_local, width + 7 :], axis=2, keepdims=True)
    row_mean = jnp.mean(means, axis=0, keepdims=True)
    shifts = means - row_mean
    spread = jnp.sum(moments + columns * shifts * shifts, axis=0) / features
    inv_scale = lax.rsqrt(spread + NORM_EPS)
    projected = inv_scale * jnp.sum(
        incoming[:, :seq_local, : width + 4]
        + shifts * incoming[:, seq_local:, : width + 4],
        axis=0,
    )
    queries = projected[:, :key_size].astype(jnp.bfloat16)
    key_rows = projected[:, key_size : 2 * key_size].astype(jnp.bfloat16)
    value_rows = projected[:, 2 * key_size : 2 * key_size + value_size].astype(jnp.bfloat16)
    outgate = projected[:, 2 * key_size + value_size : width].astype(jnp.bfloat16)
    input_pre = (
        projected[:, width : width + 1]
        + projected[:, width + 2 : width + 3]
        + lax.dynamic_slice_in_dim(input_bias, head, 1, 0)
    )
    forget_pre = (
        projected[:, width + 1 : width + 2]
        + projected[:, width + 3 : width + 4]
        + lax.dynamic_slice_in_dim(forget_bias, head, 1, 0)
    )

    carried = jax.nn.log_sigmoid(forget_pre) + max_state
    new_max = jnp.maximum(carried, input_pre)
    keep_old = jnp.exp(carried - new_max)
    admit_new = jnp.exp(input_pre - new_max)
    key_float = key_rows.astype(jnp.float32)
    value_float = value_rows.astype(jnp.float32)
    old_cell = cell_state[:, 0]
    new_cell = (
        keep_old[:, :, None] * old_cell
        + admit_new[:, :, None] * key_float[:, :, None] * value_float[:, None, :]
    )
    new_norm = keep_old * norm_state[:, 0] + admit_new * key_float
    query_float = queries.astype(jnp.float32) * key_size ** (-0.5)
    readout = jnp.sum(query_float[:, :, None] * new_cell, axis=1)
    head_mean = jnp.mean(readout, axis=1, keepdims=True)
    around = readout - head_mean
    head_var = jnp.mean(around * around, axis=1, keepdims=True)
    gains_here = lax.dynamic_slice_in_dim(head_gain, head * value_size, value_size, 0)
    mixed_heads = (
        around
        * lax.rsqrt(head_var + HEAD_EPS)
        * gains_here
        * jax.nn.sigmoid(outgate.astype(jnp.float32))
    ).astype(jnp.bfloat16)

    all_mixed = from_everyone(mixed_heads, "ep").reshape(seq_total, value_size)
    head_terms = jnp.dot(all_mixed, w_project, preferred_element_type=jnp.float32)
    stream = (tokens.astype(jnp.float32) + summed_over_tp(head_terms)).astype(jnp.bfloat16)

    outbound = jnp.einsum(
        "eps,sd->epd", picker, stream, preferred_element_type=jnp.float32
    ).astype(jnp.bfloat16)
    arrived = lax.all_to_all(outbound, "ep", split_axis=0, concat_axis=2, tiled=True)[0]
    slot_rows = arrived.astype(jnp.float32)
    slot_mean = jnp.mean(slot_rows, axis=1, keepdims=True)
    slot_spread = jnp.mean(slot_rows * slot_rows, axis=1, keepdims=True) - slot_mean * slot_mean
    normed = (
        (slot_rows - slot_mean) * lax.rsqrt(slot_spread + NORM_EPS) * second_gain
    ).astype(jnp.bfloat16)
    gate_sum = jnp.dot(normed, expert_gate[0], preferred_element_type=jnp.float32)
    up_sum = jnp.dot(normed, expert_up[0], preferred_element_type=jnp.float32)
    active = (jax.nn.silu(gate_sum) * up_sum).astype(jnp.bfloat16)
    slot_out = jnp.dot(active, expert_down[0], preferred_element_type=jnp.float32)
    back = lax.all_to_all(
        slot_out.astype(jnp.bfloat16), "ep", split_axis=1, concat_axis=0, tiled=True
    )
    weight_table = weighted.reshape(experts * slot_count, seq_total)
    moe_part = sum(
        lax.dot_general(
            piece.astype(jnp.bfloat16),
            back,
            (((0,), (0,)), ((), ())),
            preferred_element_type=jnp.float32,
        )
        for piece in in_pieces(weight_table, 2)
    )
    layer_out = (stream.astype(jnp.float32) + summed_over_tp(moe_part)).astype(jnp.bfloat16)
    return (layer_out, new_cell[:, None], new_norm[:, None], new_max)


def solution(mesh):
    placed = (
        P("grp", "ep"),
        P(),
        P("ep", "tp"),
        P("ep", "tp"),
        P("ep", "tp"),
        P("ep", "tp"),
        P(),
        P(),
        P(),
        P(),
        P(),
        P("tp", "ep"),
        P(("grp", "ep"), "tp", None, None),
        P(("grp", "ep"), "tp", None),
        P(("grp", "ep"), "tp"),
        P(),
        P("grp", None),
        P("grp", None),
        P("ep", None, "tp"),
        P("ep", None, "tp"),
        P("ep", "tp", None),
    )
    return jax.shard_map(
        on_device,
        mesh=mesh,
        in_specs=placed,
        out_specs=(
            P("grp", "ep"),
            P(("grp", "ep"), "tp", None, None),
            P(("grp", "ep"), "tp", None),
            P(("grp", "ep"), "tp"),
        ),
        check_vma=False,
    )
```

time: 234 us -> 171 us (0.73)
  waiting for transfers between devices: 62.8 us -> 38.2 us
  blocking collectives: 66 us -> 51.7 us
  other arithmetic: 15.6 us -> 7.33 us
  starting transfers between devices: 63 us -> 55.3 us
  local copies, waits for them, and re-layouts: 17.4 us -> 13.2 us
  matrix products: 5.14 us -> 2.06 us
    all_to_all x3 -> x1, blocking collectives: 45.9 us -> 16.6 us  [on_device(): lax.all_to_all(outbound, 'ep', split_axis=0, concat_axis=2, tiled=True)[0]]
    all_to_all x5 -> x3, waiting for transfers between devices: 62.8 us -> 38.2 us  [the longest x2 25.9 us: exchanged(): return lax.all_to_all(blocks, axis, split_axis=0, concat_axis=0, tiled=True)]
    all_gather x1 -> x2, blocking collectives: 20.2 us -> 35.1 us  [summed_over_tp(): lax.all_gather(part.astype(jnp.bfloat16), 'tp').astype(jnp.float32)]
    unnamed x1 -> x0, other arithmetic: 11.5 us -> none
    all_to_all x5 -> x3, starting transfers between devices: 63 us -> 55.3 us  [the longest x2 49.5 us: exchanged(): return lax.all_to_all(blocks, axis, split_axis=0, concat_axis=0, tiled=True)]
    unnamed x40 -> x35, local copies, waits for them, and re-layouts: 7.97 us -> 4.04 us
    dot_general x12 -> x7, matrix products: 5.14 us -> 2.06 us  [the longest x1 0.72 us: on_device(): jnp.dot(active, expert_down[0], preferred_element_type=jnp.float32)]
  transfers between devices with their start and end apart: 5 -> 3, of which waited for: 5 -> 3; matrix products, arithmetic and copies ran while one was open for 2% -> 3% of each run, Pallas kernels for 0% -> 0%
where the time goes in v1:
time: 171 us; the launch traced here: 169 us
  starting transfers between devices  55.3 us (32%)
  blocking collectives  51.7 us (30%)
  waiting for transfers between devices  38.2 us (22%)
  local copies, waits for them, and re-layouts  13.2 us (8%)
  other arithmetic  7.33 us (4%)
  matrix products  2.06 us (1%)
    all_to_all x2, starting transfers between devices, exchanged(): return lax.all_to_all(blocks, axis, split_axis=0, concat_axis=0, tiled=True)  49.5 us
    all_gather x2, blocking collectives, summed_over_tp(): lax.all_gather(part.astype(jnp.bfloat16), 'tp').astype(jnp.float32)  35.1 us
    all_to_all x2, waiting for transfers between devices, exchanged(): return lax.all_to_all(blocks, axis, split_axis=0, concat_axis=0, tiled=True)  25.9 us
    all_to_all x1, blocking collectives, on_device(): lax.all_to_all(outbound, 'ep', split_axis=0, concat_axis=2, tiled=True)[0]  16.6 us
    all_to_all x1, waiting for transfers between devices, on_device(): lax.all_to_all(slot_out.astype(jnp.bfloat16), 'ep', split_axis=1, concat_...  12.3 us
    all_to_all x1, starting transfers between devices, on_device(): lax.all_to_all(slot_out.astype(jnp.bfloat16), 'ep', split_axis=1, concat_...  5.79 us
    unnamed x35, local copies, waits for them, and re-layouts  4.04 us
  transfers between devices with their start and end apart: 3, of which 3 were waited for; matrix products, arithmetic and copies ran while one was open for 3% of the time, Pallas kernels for 0%

profile of v1, /device:TPU:80, one launch (start us, length us, event | category | flops | bytes accessed | tf_op | source)
XLA Modules:
  0.0 168.9 jit_solution(15618581632866811593)
XLA Ops:
  0.7 0.9 convert_reduce_fusion.3
  1.9 0.8 dynamic_slice.20
  2.7 0.8 dynamic_slice.18
  3.4 0.8 dynamic_slice.19
  4.5 0.9 concatenate.25
  8.2 0.8 pad_maximum_fusion
  9.1 43.7 %all-to-all-start = ((bf16[16,7,777]{2,1,0:T(8,128)(2,1)}), bf16[16,7,777]{2,1,0:T(8,128)(2,1)S(1)}, u32[]{:S(2)}, u32[]{:S(2)}) async-start(bf16[16,7,777]{2,1,0:T(8,128)(2,1)} %pad_maximum_fusion), calls=%async_computation | async-start | bytes 458752 | tf_op jit(solution)/shard_map/all_to_all | solution.py:12
  52.8 0.6 copy-done.13
  53.4 0.6 dynamic_slice.21
  54.1 0.6 dynamic_slice.22
  54.8 0.6 copy-done.9
  55.6 0.8 dynamic_slice.23
  56.5 13.3 %all-to-all-done = bf16[16,7,777]{2,1,0:T(8,128)(2,1)S(1)} async-done(((bf16[16,7,777]{2,1,0:T(8,128)(2,1)}), bf16[16,7,777]{2,1,0:T(8,128)(2,1)S(1)}, u32[]{:S(2)}, u32[]{:S(2)}) %all-to-all-start) | async-done | bytes 174080 | tf_op jit(solution)/shard_map/all_to_all | solution.py:12
  70.5 1.5 exponential_reduce_fusion.1
  72.1 0.7 copy-done.10
  72.8 0.4 fusion.11
  73.5 0.7 broadcast_in_dim.34
  74.1 5.8 %all-to-all-start.1 = ((bf16[16,6,256]{2,1,0:T(8,128)(2,1)}), bf16[16,6,256]{2,1,0:T(8,128)(2,1)S(1)}, u32[]{:S(2)}, u32[]{:S(2)}) async-start(bf16[16,6,256]{2,1,0:T(8,128)(2,1)} %broadcast_in_dim.34), calls=%async_computation.1 | async-start | bytes 131072 | tf_op jit(solution)/shard_map/all_to_all | solution.py:12
  80.0 12.6 %all-to-all-done.1 = bf16[16,6,256]{2,1,0:T(8,128)(2,1)S(1)} async-done(((bf16[16,6,256]{2,1,0:T(8,128)(2,1)}), bf16[16,6,256]{2,1,0:T(8,128)(2,1)S(1)}, u32[]{:S(2)}, u32[]{:S(2)}) %all-to-all-start.1) | async-done | bytes 49184 | tf_op jit(solution)/shard_map/all_to_all | solution.py:12
  92.7 19.2 %all-gather = bf16[1536,128]{1,0:T(8,128)(2,1)S(1)} all-gather(bf16[96,128]{1,0:T(8,128)(2,1)S(1)} %convolution_convert_fusion.2), channel_id=2, replica_groups=mesh['grp'=2,'ep'=16,'tp'=16] {'tp'}, dimensions={0}, use_global_device_ids=true | all-gather | bytes 417792 | tf_op jit(solution)/shard_map/all_gather | solution.py:31
  112.2 16.6 %all_to_all.35 = bf16[16,32,128]{2,1,0:T(8,128)(2,1)S(1)} all-to-all(bf16[16,32,128]{2,1,0:T(8,128)(2,1)S(1)} %convolution_convert_fusion.1), channel_id=1, replica_groups=mesh['grp'=2,'ep'=16,'tp'=16] {'ep'}, dimensions={0} | all-to-all | bytes 262144 | tf_op jit(solution)/shard_map/all_to_all | solution.py:172
  129.2 0.3 fusion.7
  129.5 0.5 copy-done.2
  130.0 0.7 fusion
  130.7 0.7 copy.136
  131.4 5.8 %all-to-all-start.3 = ((bf16[32,16,128]{2,0,1:T(8,128)(2,1)}), bf16[32,16,128]{2,0,1:T(8,128)(2,1)S(1)}, u32[]{:S(2)}, u32[]{:S(2)}) async-start(bf16[32,16,128]{2,0,1:T(8,128)(2,1)} %bitcast.94), calls=%async_computation.3 | async-start | bytes 262144 | tf_op jit(solution)/shard_map/all_to_all | solution.py:183
  137.2 0.6 copy.118
  137.8 0.6 copy.117
  138.4 1.1 multiply_add_fusion
  139.5 12.3 %all-to-all-done.3 = bf16[32,16,128]{2,0,1:T(8,128)(2,1)S(1)} async-done(((bf16[32,16,128]{2,0,1:T(8,128)(2,1)}), bf16[32,16,128]{2,0,1:T(8,128)(2,1)S(1)}, u32[]{:S(2)}, u32[]{:S(2)}) %all-to-all-start.3) | async-done | bytes 131104 | tf_op jit(solution)/shard_map/all_to_all | solution.py:183
  152.3 15.9 %all-gather.1 = bf16[1536,128]{1,0:T(8,128)(2,1)S(1)} all-gather(bf16[96,128]{1,0:T(8,128)(2,1)S(1)} %fusion.2), channel_id=3, replica_groups=mesh['grp'=2,'ep'=16,'tp'=16] {'tp'}, dimensions={0}, use_global_device_ids=true | all-gather | bytes 417792 | tf_op jit(solution)/shard_map/all_gather | solution.py:31
  168.2 0.6 add_convert_fusion
  (100 shorter events, 6.3 us)
Async XLA Ops:
  0.6 128.9 %copy-start = (bf16[1,256,2048]{2,1,0:T(8,128)(2,1)S(1)}, bf16[1,256,2048]{2,1,0:T(8,128)(2,1)}, u32[]{:S(2)}) copy-start(bf16[1,256,2048]{2,1,0:T(8,128)(2,1)} %param.41) | copy-start | bytes 3145732
  0.6 1.0 copy-start.4
  1.6 2.9 %copy-start.6 = (bf16[128,256]{1,0:T(8,128)(2,1)S(1)}, bf16[128,256]{1,0:T(8,128)(2,1)}, u32[]{:S(2)}) copy-start(bf16[128,256]{1,0:T(8,128)(2,1)} %param.26) | copy-start | bytes 196612
  1.6 2.8 %copy-start.5 = (bf16[128,256]{1,0:T(8,128)(2,1)S(1)}, bf16[128,256]{1,0:T(8,128)(2,1)}, u32[]{:S(2)}) copy-start(bf16[128,256]{1,0:T(8,128)(2,1)} %param.25) | copy-start | bytes 196612
  9.1 60.7 %all-to-all-start = ((bf16[16,7,777]{2,1,0:T(8,128)(2,1)}), bf16[16,7,777]{2,1,0:T(8,128)(2,1)S(1)}, u32[]{:S(2)}, u32[]{:S(2)}) async-start(bf16[16,7,777]{2,1,0:T(8,128)(2,1)} %pad_maximum_fusion), calls=%async_computation | async-start | bytes 458752 | tf_op jit(solution)/shard_map/all_to_all | solution.py:12
  52.8 0.7 copy-start.13
  53.4 0.7 copy-start.14
  54.1 0.7 copy-start.12
  54.7 0.7 copy-start.9
  56.5 16.4 %copy-start.1 = (f32[6,1,128,256]{3,2,1,0:T(8,128)S(1)}, f32[6,1,128,256]{3,2,1,0:T(8,128)}, u32[]{:S(2)}) copy-start(f32[6,1,128,256]{3,2,1,0:T(8,128)} %param.33) | copy-start | bytes 2359300
  72.0 0.7 copy-start.10
  74.1 18.4 %all-to-all-start.1 = ((bf16[16,6,256]{2,1,0:T(8,128)(2,1)}), bf16[16,6,256]{2,1,0:T(8,128)(2,1)S(1)}, u32[]{:S(2)}, u32[]{:S(2)}) async-start(bf16[16,6,256]{2,1,0:T(8,128)(2,1)} %broadcast_in_dim.34), calls=%async_computation.1 | async-start | bytes 131072 | tf_op jit(solution)/shard_map/all_to_all | solution.py:12
  80.0 12.6 %copy-start.7 = (bf16[256,128]{1,0:T(8,128)(2,1)S(1)}, bf16[256,128]{1,0:T(8,128)(2,1)}, u32[]{:S(2)}) copy-start(bf16[256,128]{1,0:T(8,128)(2,1)} %param.32) | copy-start | bytes 196612
  92.7 36.5 %copy-start.3 = (bf16[1,2048,256]{2,1,0:T(8,128)(2,1)S(1)}, bf16[1,2048,256]{2,1,0:T(8,128)(2,1)}, u32[]{:S(2)}) copy-start(bf16[1,2048,256]{2,1,0:T(8,128)(2,1)} %param.39) | copy-start | bytes 3145732
  112.2 16.9 %copy-start.8 = (f32[2048]{0:T(1024)S(1)}, f32[2048]{0:T(1024)}, u32[]{:S(2)}) copy-start(f32[2048]{0:T(1024)} %param.36) | copy-start | bytes 24580
  128.8 1.2 copy-start.2
  131.4 5.8 %copy-start.11 = (f32[96,2]{0,1:T(2,128)S(1)}, f32[96,2]{0,1:T(2,128)}, u32[]{:S(2)}) copy-start(f32[96,2]{0,1:T(2,128)} %param.38) | copy-start | bytes 2308
  131.4 20.4 %all-to-all-start.3 = ((bf16[32,16,128]{2,0,1:T(8,128)(2,1)}), bf16[32,16,128]{2,0,1:T(8,128)(2,1)S(1)}, u32[]{:S(2)}, u32[]{:S(2)}) async-start(bf16[32,16,128]{2,0,1:T(8,128)(2,1)} %bitcast.94), calls=%async_computation.3 | async-start | bytes 262144 | tf_op jit(solution)/shard_map/all_to_all | solution.py:183

commit v2 on v1

v2 whole, which is shorter than its diff:
```python
import functools

import jax
import jax.numpy as jnp
from jax import lax
from jax.experimental import pallas as pl
from jax.experimental.pallas import tpu as pltpu
from jax.sharding import PartitionSpec as P

NORM_EPS = 1e-05
HEAD_EPS = 1e-06
CAPACITY = 2
LANES = 128
PADDED = 8
GATE_SUMS = 16
F32 = jnp.float32
BF16 = jnp.bfloat16


def exchanged(blocks, axis):
    return lax.all_to_all(blocks, axis, split_axis=0, concat_axis=0, tiled=True)


def from_everyone(array, axis):
    peers = lax.axis_size(axis)
    return exchanged(jnp.broadcast_to(array[None], (peers, *array.shape)), axis)


def in_pieces(values, count):
    pieces = []
    for _ in range(count - 1):
        head = lax.reduce_precision(values, 8, 7)
        pieces.append(head)
        values = values - head
    pieces.append(values)
    return pieces


def summed_over_tp(part):
    return jnp.sum(from_everyone(part.astype(BF16), "tp").astype(F32), axis=0)


def rounded_pieces(values, count):
    pieces = []
    for _ in range(count):
        head = values.astype(BF16).astype(F32)
        pieces.append(head)
        values = values - head
    return pieces


def dot(a, b):
    return jnp.dot(a, b, preferred_element_type=F32)


def grid_index(shape):
    return lax.broadcasted_iota(jnp.int32, shape, 0), lax.broadcasted_iota(jnp.int32, shape, 1)


def one_hot(condition):
    return jnp.where(condition, 1.0, 0.0).astype(BF16)


def send_kernel(where_ref, tok_ref, gain_ref, wq, wk, wv, wo, wi, wf, out_ref, *, seq_local):
    head = where_ref[1]
    seq_total, columns = tok_ref.shape
    blocks = seq_total // seq_local
    count = blocks * PADDED
    row, col = grid_index((count, seq_total))
    spread_rows = one_hot(
        ((row & (PADDED - 1)) < seq_local)
        & (col == (row >> 3) * seq_local + (row & (PADDED - 1)))
    )
    slot = lax.broadcasted_iota(jnp.int32, (count, columns), 0) & (PADDED - 1)
    values = dot(spread_rows, tok_ref[...])
    values = jnp.where(slot == seq_local, 1.0, values)
    own = slot[:, :1] < seq_local
    block_mean = jnp.where(own, jnp.sum(values, axis=1, keepdims=True) * (1.0 / columns), 0.0)
    offsets = values - block_mean
    moment = jnp.where(own, jnp.sum(offsets * offsets, axis=1, keepdims=True), 0.0)
    gain_row = gain_ref[...]
    down, across = grid_index((columns, columns))
    gain_col = jnp.sum(jnp.where(down == across, gain_row, 0.0), axis=1, keepdims=True)
    exact = values.astype(BF16)
    parts = []
    for ref in (wq, wk, wv, wo):
        high, low = rounded_pieces(ref[...].astype(F32) * gain_col, 2)
        parts.append(dot(exact, high.astype(BF16)) + dot(exact, low.astype(BF16)))
    product = jnp.concatenate(parts, axis=1)
    tiles = product.reshape(blocks, PADDED, product.shape[1])
    sums = tiles[:, seq_local : seq_local + 1, :]
    centred = tiles - block_mean.reshape(blocks, PADDED, 1) * sums

    pick, _ = grid_index(wi.shape)

    def gate_part(ref):
        chosen = jnp.sum(jnp.where(pick == head, ref[...].astype(F32), 0.0), axis=0, keepdims=True)
        return jnp.sum(offsets * (chosen * gain_row), axis=1, keepdims=True)

    gates = [*rounded_pieces(gate_part(wi), 2), *rounded_pieces(gate_part(wf), 2)]
    lane = lax.broadcasted_iota(jnp.int32, (count, LANES), 1)
    start = jnp.where(slot[:, :1] == seq_local, GATE_SUMS, 0)
    table = jnp.zeros((count, LANES), F32)
    for k, piece in enumerate(gates):
        table = jnp.where(lane == start + k, piece, table)
    table = jnp.where(slot == PADDED - 1, 0.0, table)
    for k, piece in enumerate([*rounded_pieces(block_mean, 3), *rounded_pieces(moment, 2)]):
        table = jnp.where((lane == 4 + k) & own, piece, table)
    exact_table = table.astype(BF16)
    down, across = grid_index((count, count))
    same = (down >> 3) == (across >> 3)
    last = (down & (PADDED - 1)) == PADDED - 1
    inner = across & (PADDED - 1)
    laid = []
    for r in range(seq_local):
        laid.append(dot(one_hot(same & last & ((inner == r) | (inner == seq_local))), exact_table))
    side = jnp.concatenate(laid, axis=1).reshape(tiles.shape)
    out_ref[...] = (centred + side).astype(BF16)


def receive_kernel(
    where_ref, in_bias, for_bias, got_ref, cell_ref, norm_ref, max_ref, gain_ref,
    mixed_ref, keep_ref, admit_ref, value_ref, norm_out, max_out, *, columns
):
    head = where_ref[1]
    blocks, padded, width = got_ref.shape
    seq_local, _, key_size, value_size = cell_ref.shape
    count = blocks * padded
    got = got_ref[...].astype(F32)
    flat = got.reshape(count, width).astype(BF16)
    down, across = grid_index((count, count))
    same = (down >> 3) == (across >> 3)
    inner = across & (PADDED - 1)
    outer = down & (PADDED - 1)
    table = jnp.zeros((count, LANES), F32)
    for r in range(seq_local):
        back = one_hot(same & (outer == r) & (inner == PADDED - 1))
        table = table + dot(back, flat[:, r * LANES : (r + 1) * LANES])
    sums = dot(one_hot(same & (inner == seq_local)), flat).reshape(blocks, padded, width)
    lane = lax.broadcasted_iota(jnp.int32, (count, LANES), 1)

    def lanes(first, number):
        kept = jnp.where((lane >= first) & (lane < first + number), table, 0.0)
        return jnp.sum(kept, axis=1, keepdims=True).reshape(blocks, padded, 1)

    means = lanes(4, 3)
    row_mean = jnp.sum(means, axis=0, keepdims=True) * (1.0 / blocks)
    shifts = means - row_mean
    spread = jnp.sum(lanes(7, 2) + columns * shifts * shifts, axis=0) * (1.0 / (blocks * columns))
    inv_scale = lax.rsqrt(spread + NORM_EPS)
    projected = inv_scale * jnp.sum(got + shifts * sums, axis=0)

    def rounded(a, b):
        return projected[:, a:b].astype(BF16).astype(F32)

    query = rounded(0, key_size) * key_size**-0.5
    key = rounded(key_size, 2 * key_size)
    value = rounded(2 * key_size, 2 * key_size + value_size)
    outgate = rounded(2 * key_size + value_size, width)
    input_pre = (
        inv_scale * jnp.sum(lanes(0, 2) + shifts * lanes(GATE_SUMS, 2), axis=0) + in_bias[head]
    )[:seq_local]
    forget_pre = (
        inv_scale * jnp.sum(lanes(2, 2) + shifts * lanes(GATE_SUMS + 2, 2), axis=0)
        + for_bias[head]
    )[:seq_local]
    log_forget = jnp.minimum(forget_pre, 0.0) - jnp.log1p(jnp.exp(-jnp.abs(forget_pre)))
    carried = log_forget + max_ref[...]
    new_max = jnp.maximum(carried, input_pre)
    keep_old = jnp.exp(carried - new_max)
    admit_key = jnp.exp(input_pre - new_max) * key[:seq_local]
    max_out[...] = new_max
    keep_ref[...] = keep_old
    admit_ref[...] = admit_key
    value_ref[...] = value[:seq_local]
    norm_out[...] = keep_old * norm_ref[...] + admit_key
    turned = query.T
    rows = lax.broadcasted_iota(jnp.int32, (padded, value_size), 0)
    against_cell = jnp.zeros((padded, value_size), F32)
    for s in range(seq_local):
        one = jnp.sum(turned[:, s : s + 1] * cell_ref[s, 0], axis=0, keepdims=True)
        against_cell = jnp.where(rows == s, one, against_cell)
    scores = jnp.sum(query[:seq_local] * admit_key, axis=1, keepdims=True)
    readout = keep_old * against_cell[:seq_local] + scores * value[:seq_local]
    head_mean = jnp.mean(readout, axis=1, keepdims=True)
    around = readout - head_mean
    head_var = jnp.mean(around * around, axis=1, keepdims=True)
    gain = gain_ref[:, pl.ds(pl.multiple_of(head * value_size, LANES), value_size)]
    opened = 1.0 / (1.0 + jnp.exp(-outgate[:seq_local]))
    mixed = around * lax.rsqrt(head_var + HEAD_EPS) * gain * opened
    mixed = jnp.concatenate([mixed, jnp.zeros((padded - seq_local, value_size), F32)], axis=0)
    mixed_ref[...] = jnp.broadcast_to(mixed[None], (blocks, padded, value_size)).astype(BF16)


def in_vmem(array):
    return pltpu.with_memory_space_constraint(array, pltpu.VMEM)


def whole(shape):
    return pl.BlockSpec(shape, lambda i, where, n=len(shape): (0,) * n)


def parts_to_send(where, tokens, gain, w_query, w_key, w_value, w_outgate, w_input, w_forget, blocks):
    seq_total, columns = tokens.shape
    width = 2 * (w_query.shape[1] + w_value.shape[1])
    gate_block = pl.BlockSpec((w_input.shape[0], columns), lambda i, where: (0, where[0]))
    return pl.pallas_call(
        functools.partial(send_kernel, seq_local=seq_total // blocks),
        grid_spec=pltpu.PrefetchScalarGridSpec(
            num_scalar_prefetch=1,
            grid=(1,),
            in_specs=[
                whole(tokens.shape),
                pl.BlockSpec((1, columns), lambda i, where: (0, where[0])),
                *(whole(w.shape) for w in (w_query, w_key, w_value, w_outgate)),
                gate_block,
                gate_block,
            ],
            out_specs=whole((blocks, PADDED, width)),
        ),
        out_shape=jax.ShapeDtypeStruct((blocks, PADDED, width), BF16),
        name="send_parts",
    )(where, tokens, gain, w_query, w_key, w_value, w_outgate, w_input, w_forget)


def cell_step(where, input_bias, forget_bias, got, cell, norm, top, gain, columns):
    blocks = got.shape[0]
    seq_local, _, key_size, value_size = cell.shape
    shapes = [
        pltpu.VMEM((blocks, PADDED, value_size), BF16),
        pltpu.VMEM((seq_local, 1), F32),
        pltpu.VMEM((seq_local, key_size), F32),
        pltpu.VMEM((seq_local, value_size), F32),
        pltpu.VMEM((seq_local, key_size), F32),
        pltpu.VMEM((seq_local, 1), F32),
    ]
    scalars = pl.BlockSpec(memory_space=pltpu.SMEM)
    near = pl.BlockSpec(memory_space=pltpu.VMEM)
    return pl.pallas_call(
        functools.partial(receive_kernel, columns=columns),
        in_specs=[scalars, scalars, scalars, near, near, near, near, near],
        out_specs=[near] * len(shapes),
        out_shape=shapes,
        name="cell_step",
    )(where, input_bias, forget_bias, *(in_vmem(a) for a in (got, cell, norm, top, gain)))


def on_device(
    tokens,
    first_gain,
    w_query,
    w_key,
    w_value,
    w_outgate,
    w_input,
    w_forget,
    input_bias,
    forget_bias,
    head_gain,
    w_project,
    cell_state,
    norm_state,
    max_state,
    second_gain,
    routes,
    route_weight,
    expert_gate,
    expert_up,
    expert_down,
):
    blocks = lax.axis_size("ep")
    seq_total, columns = tokens.shape
    seq_local = seq_total // blocks
    value_size = cell_state.shape[3]
    where = jnp.stack([lax.axis_index("ep"), lax.axis_index("tp")]).astype(jnp.int32)

    experts = blocks
    slot_count = blocks * CAPACITY
    expert_ids = lax.broadcasted_iota(jnp.int32, (1, 1, experts), 2)
    matches = routes[:, :, None] == expert_ids
    routed = jnp.sum(matches.astype(jnp.int32), axis=1)
    combine = jnp.sum(jnp.where(matches, route_weight[:, :, None], 0.0), axis=1)
    running = (
        jnp.cumsum(routed.reshape(blocks, seq_local, experts), axis=1).reshape(seq_total, experts)
        - routed
    )
    block_ids = lax.broadcasted_iota(jnp.int32, (seq_total, experts), 0) // seq_local
    slot_of = block_ids * CAPACITY + running
    slot_ids = lax.broadcasted_iota(jnp.int32, (experts, slot_count, seq_total), 1)
    placed = (slot_of.T[:, None, :] == slot_ids) & (routed.T[:, None, :] > 0)
    picker = placed.astype(jnp.bfloat16)
    weighted = jnp.where(placed, combine.T[:, None, :], 0.0)

    outgoing = parts_to_send(
        where,
        tokens,
        first_gain.reshape(1, -1),
        w_query,
        w_key,
        w_value,
        w_outgate,
        w_input.T,
        w_forget.T,
        blocks,
    )
    incoming = exchanged(outgoing, "ep")
    mixed, keep_old, admit_key, value, new_norm, new_max = cell_step(
        where,
        input_bias,
        forget_bias,
        incoming,
        cell_state,
        norm_state[:, 0],
        max_state,
        head_gain.reshape(1, -1),
        columns,
    )
    new_cell = (
        keep_old[:, :, None] * cell_state[:, 0] + admit_key[:, :, None] * value[:, None, :]
    )

    all_mixed = exchanged(mixed, "ep")[:, :seq_local].reshape(seq_total, value_size)
    head_terms = jnp.dot(all_mixed, w_project, preferred_element_type=jnp.float32)
    stream = (tokens.astype(jnp.float32) + summed_over_tp(head_terms)).astype(jnp.bfloat16)

    outbound = jnp.einsum(
        "eps,sd->epd", picker, stream, preferred_element_type=jnp.float32
    ).astype(jnp.bfloat16)
    arrived = lax.all_to_all(outbound, "ep", split_axis=0, concat_axis=2, tiled=True)[0]
    slot_rows = arrived.astype(jnp.float32)
    slot_mean = jnp.mean(slot_rows, axis=1, keepdims=True)
    slot_spread = jnp.mean(slot_rows * slot_rows, axis=1, keepdims=True) - slot_mean * slot_mean
    normed = (
        (slot_rows - slot_mean) * lax.rsqrt(slot_spread + NORM_EPS) * second_gain
    ).astype(jnp.bfloat16)
    gate_sum = jnp.dot(normed, expert_gate[0], preferred_element_type=jnp.float32)
    up_sum = jnp.dot(normed, expert_up[0], preferred_element_type=jnp.float32)
    active = (jax.nn.silu(gate_sum) * up_sum).astype(jnp.bfloat16)
    slot_out = jnp.dot(active, expert_down[0], preferred_element_type=jnp.float32)
    back = exchanged(
        jnp.swapaxes(slot_out.astype(BF16).reshape(slot_count, blocks, columns), 0, 1), "ep"
    ).reshape(experts * slot_count, columns)
    weight_table = weighted.reshape(experts * slot_count, seq_total)
    moe_part = sum(
        lax.dot_general(
            piece.astype(jnp.bfloat16),
            back,
            (((0,), (0,)), ((), ())),
            preferred_element_type=jnp.float32,
        )
        for piece in in_pieces(weight_table, 2)
    )
    layer_out = (stream.astype(jnp.float32) + summed_over_tp(moe_part)).astype(jnp.bfloat16)
    return (layer_out, new_cell[:, None], new_norm[:, None], new_max)


def solution(mesh):
    placed = (
        P("grp", "ep"),
        P(),
        P("ep", "tp"),
        P("ep", "tp"),
        P("ep", "tp"),
        P("ep", "tp"),
        P(),
        P(),
        P(),
        P(),
        P(),
        P("tp", "ep"),
        P(("grp", "ep"), "tp", None, None),
        P(("grp", "ep"), "tp", None),
        P(("grp", "ep"), "tp"),
        P(),
        P("grp", None),
        P("grp", None),
        P("ep", None, "tp"),
        P("ep", None, "tp"),
        P("ep", "tp", None),
    )
    return jax.shard_map(
        on_device,
        mesh=mesh,
        in_specs=placed,
        out_specs=(
            P("grp", "ep"),
            P(("grp", "ep"), "tp", None, None),
            P(("grp", "ep"), "tp", None),
            P(("grp", "ep"), "tp"),
        ),
        check_vma=False,
    )
```

time: 171 us -> 170 us (level)
  blocking collectives: 51.7 us -> 34.2 us
  waiting for transfers between devices: 38.2 us -> 53.7 us
  local copies, waits for them, and re-layouts: 13.2 us -> 5.31 us
  starting transfers between devices: 55.3 us -> 62.1 us
  Pallas kernels: 0 us -> 4.52 us
  other arithmetic: 7.33 us -> 2.99 us
    all_gather x2 -> x0, blocking collectives: 35.1 us -> none  [summed_over_tp(): lax.all_gather(part.astype(jnp.bfloat16), 'tp').astype(jnp.float32)]
    all_to_all x2 -> x4, waiting for transfers between devices: 25.9 us -> 53.7 us  [exchanged(): return lax.all_to_all(blocks, axis, split_axis=0, concat_axis=0, tiled=True)]
    all_to_all x0 -> x1, blocking collectives: none -> 17.5 us  [exchanged(): return lax.all_to_all(blocks, axis, split_axis=0, concat_axis=0, tiled=True)]
    all_to_all x2 -> x4, starting transfers between devices: 49.5 us -> 62.1 us  [exchanged(): return lax.all_to_all(blocks, axis, split_axis=0, concat_axis=0, tiled=True)]
    all_to_all x1 -> x0, waiting for transfers between devices: 12.3 us -> none  [on_device(): lax.all_to_all(slot_out.astype(jnp.bfloat16), 'ep', split_axis=1, concat_...]
    all_to_all x1 -> x0, starting transfers between devices: 5.79 us -> none  [on_device(): lax.all_to_all(slot_out.astype(jnp.bfloat16), 'ep', split_axis=1, concat_...]
    pallas_call x0 -> x2, Pallas kernels: none -> 4.52 us  [the longest x1 2.9 us: parts_to_send(): pl.pallas_call(functools.partial(send_kernel, seq_local=seq_total // bloc...]
    dynamic_slice x8 -> x0, local copies, waits for them, and re-layouts: 4.5 us -> none  [the longest x2 0.89 us: on_device(): forget_cols = lax.dynamic_slice(w_forget, (col_start, head), (columns, 1))]
  transfers between devices with their start and end apart: 3 -> 4, of which waited for: 3 -> 4; matrix products, arithmetic and copies ran while one was open for 3% -> 2% of each run, Pallas kernels for 0% -> 0%
where the time goes in v2:
time: 170 us; the launch traced here: 167 us
  starting transfers between devices  62.1 us (37%)
  waiting for transfers between devices  53.7 us (32%)
  blocking collectives  34.2 us (20%)
  local copies, waits for them, and re-layouts  5.31 us (3%)
  Pallas kernels  4.52 us (3%)
  matrix products  3.03 us (2%)
  other arithmetic  2.99 us (2%)
    all_to_all x4, starting transfers between devices, exchanged(): return lax.all_to_all(blocks, axis, split_axis=0, concat_axis=0, tiled=True)  62.1 us
    all_to_all x4, waiting for transfers between devices, exchanged(): return lax.all_to_all(blocks, axis, split_axis=0, concat_axis=0, tiled=True)  53.7 us
    all_to_all x1, blocking collectives, exchanged(): return lax.all_to_all(blocks, axis, split_axis=0, concat_axis=0, tiled=True)  17.5 us
    all_to_all x1, blocking collectives, on_device(): lax.all_to_all(outbound, 'ep', split_axis=0, concat_axis=2, tiled=True)[0]  16.6 us
  transfers between devices with their start and end apart: 4, of which 4 were waited for; matrix products, arithmetic and copies ran while one was open for 2% of the time, Pallas kernels for 0%

profile of v2, /device:TPU:80, one launch (start us, length us, event | category | flops | bytes accessed | tf_op | source)
XLA Modules:
  0.0 166.7 jit_solution(16491839843963619601)
XLA Ops:
  0.7 0.6 pad_add_fusion.where_ref
  1.2 2.9 %send_parts.1 = bf16[16,8,768]{2,1,0:T(8,128)(2,1)} custom-call(s32[2]{0:T(128)} %pad_add_fusion.where_ref, bf16[96,128]{1,0:T(8,128)(2,1)} %tok_ref.1, f32[1,2048]{1,0:T(1,128)} %bitcast.84, bf16[128,128]{1,0:T(8,128)(2,1)} %wq.1, bf16[128,128]{1,0:T(8,128)(2,1)} %wk.1, bf16[128,256]{1,0:T(8,128)(2,1)} %wv.1, bf16[128,256]{1,0:T(8,128)(2,1)} %wo.1, ...), custom_call_target="tpu_custom_call" | custom-call | tf_op jit(solution)/shard_map/send_parts/pallas_call | solution.py:207
  4.2 43.8 %all-to-all-start = ((bf16[16,8,768]{2,1,0:T(8,128)(2,1)}), bf16[16,8,768]{2,1,0:T(8,128)(2,1)S(1)}, u32[]{:S(2)}, u32[]{:S(2)}) async-start(bf16[16,8,768]{2,1,0:T(8,128)(2,1)} %send_parts.1), calls=%async_computation | async-start | bytes 393216 | tf_op jit(solution)/shard_map/all_to_all | solution.py:21
  48.0 0.6 copy-done.10
  48.7 15.4 %all-to-all-done.got_ref = bf16[16,8,768]{2,1,0:T(8,128)(2,1)S(1)} async-done(((bf16[16,8,768]{2,1,0:T(8,128)(2,1)}), bf16[16,8,768]{2,1,0:T(8,128)(2,1)S(1)}, u32[]{:S(2)}, u32[]{:S(2)}) %all-to-all-start) | async-done | bytes 196640 | tf_op jit(solution)/shard_map/all_to_all | solution.py:21
  64.2 1.6 cell_step.1
  65.8 17.5 %all_to_all.34 = bf16[16,8,256]{2,1,0:T(8,128)(2,1)S(1)} all-to-all(bf16[16,8,256]{2,1,0:T(8,128)(2,1)S(1)} %get-tuple-element.10), channel_id=1, replica_groups=mesh['grp'=2,'ep'=16,'tp'=16] {'ep'}, dimensions={0} | all-to-all | bytes 131072 | tf_op jit(solution)/shard_map/all_to_all | solution.py:21
  83.4 0.8 copy-done.5
  84.2 0.1 convolution_convert_fusion.2
  84.3 0.8 broadcast_in_dim.30
  85.1 7.7 %all-to-all-start.2 = ((bf16[16,96,128]{2,1,0:T(8,128)(2,1)}), bf16[16,96,128]{2,1,0:T(8,128)(2,1)S(1)}, u32[]{:S(2)}, u32[]{:S(2)}) async-start(bf16[16,96,128]{2,1,0:T(8,128)(2,1)} %broadcast_in_dim.30), calls=%async_computation.2 | async-start | bytes 786432 | tf_op jit(solution)/shard_map/all_to_all | solution.py:21
  93.2 13.1 %all-to-all-done.2 = bf16[16,96,128]{2,1,0:T(8,128)(2,1)S(1)} async-done(((bf16[16,96,128]{2,1,0:T(8,128)(2,1)}), bf16[16,96,128]{2,1,0:T(8,128)(2,1)S(1)}, u32[]{:S(2)}, u32[]{:S(2)}) %all-to-all-start.2) | async-done | bytes 393248 | tf_op jit(solution)/shard_map/all_to_all | solution.py:21
  106.3 0.2 convolution_convert_fusion.1
  106.5 16.6 %all_to_all.35 = bf16[16,32,128]{2,1,0:T(8,128)(2,1)S(1)} all-to-all(bf16[16,32,128]{2,1,0:T(8,128)(2,1)S(1)} %convolution_convert_fusion.1), channel_id=1, replica_groups=mesh['grp'=2,'ep'=16,'tp'=16] {'ep'}, dimensions={0} | all-to-all | bytes 262144 | tf_op jit(solution)/shard_map/all_to_all | solution.py:329
  123.2 0.1 fusion.14
  123.3 0.1 convert_reduce_fusion.2
  123.5 0.1 fusion.19
  123.7 1.5 fusion.7
  125.2 0.7 fusion
  125.9 0.7 copy.61
  126.6 6.5 %all-to-all-start.4 = ((bf16[16,32,128]{2,1,0:T(8,128)(2,1)}), bf16[16,32,128]{2,1,0:T(8,128)(2,1)S(1)}, u32[]{:S(2)}, u32[]{:S(2)}) async-start(bf16[16,32,128]{2,1,0:T(8,128)(2,1)} %bitcast.73), calls=%async_computation.4 | async-start | bytes 262144 | tf_op jit(solution)/shard_map/all_to_all | solution.py:21
  133.2 14.5 %all-to-all-done.4 = bf16[16,32,128]{2,1,0:T(8,128)(2,1)S(1)} async-done(((bf16[16,32,128]{2,1,0:T(8,128)(2,1)}), bf16[16,32,128]{2,1,0:T(8,128)(2,1)S(1)}, u32[]{:S(2)}, u32[]{:S(2)}) %all-to-all-start.4) | async-done | bytes 131104 | tf_op jit(solution)/shard_map/all_to_all | solution.py:21
  147.6 0.2 convolution_bitcast_fusion
  147.9 0.2 fusion.2
  148.1 0.8 broadcast_in_dim.35
  148.9 4.0 %all-to-all-start.5 = ((bf16[16,96,128]{2,1,0:T(8,128)(2,1)}), bf16[16,96,128]{2,1,0:T(8,128)(2,1)S(1)}, u32[]{:S(2)}, u32[]{:S(2)}) async-start(bf16[16,96,128]{2,1,0:T(8,128)(2,1)} %broadcast_in_dim.35), calls=%async_computation.5 | async-start | bytes 786432 | tf_op jit(solution)/shard_map/all_to_all | solution.py:21
  152.9 0.6 copy.46
  153.5 0.6 copy.45
  154.1 0.1 reduce.5
  154.2 1.1 multiply_add_fusion
  155.3 10.7 %all-to-all-done.5 = bf16[16,96,128]{2,1,0:T(8,128)(2,1)S(1)} async-done(((bf16[16,96,128]{2,1,0:T(8,128)(2,1)}), bf16[16,96,128]{2,1,0:T(8,128)(2,1)S(1)}, u32[]{:S(2)}, u32[]{:S(2)}) %all-to-all-start.5) | async-done | bytes 393248 | tf_op jit(solution)/shard_map/all_to_all | solution.py:21
  166.1 0.6 add_convert_fusion
  (38 shorter events, 0.6 us)
Async XLA Ops:
  0.6 124.5 %copy-start = (bf16[1,256,2048]{2,1,0:T(8,128)(2,1)S(1)}, bf16[1,256,2048]{2,1,0:T(8,128)(2,1)}, u32[]{:S(2)}) copy-start(bf16[1,256,2048]{2,1,0:T(8,128)(2,1)} %param.41) | copy-start | bytes 3145732
  0.6 63.5 %copy-start.1 = (f32[6,1,128,256]{3,2,1,0:T(8,128)S(1)}, f32[6,1,128,256]{3,2,1,0:T(8,128)}, u32[]{:S(2)}) copy-start(f32[6,1,128,256]{3,2,1,0:T(8,128)} %cell_ref.1) | copy-start | bytes 2359300
  4.1 43.8 %copy-start.8 = (f32[6,1,128]{2,1,0:T(1,128)S(1)}, f32[6,1,128]{2,1,0:T(1,128)}, u32[]{:S(2)}) copy-start(f32[6,1,128]{2,1,0:T(1,128)} %param.34) | copy-start | bytes 9220
  4.1 60.0 %copy-start.2 = (f32[4096]{0:T(1024)S(1)}, f32[4096]{0:T(1024)}, u32[]{:S(2)}) copy-start(f32[4096]{0:T(1024)} %param.31) | copy-start | bytes 49156
  4.2 60.0 %all-to-all-start = ((bf16[16,8,768]{2,1,0:T(8,128)(2,1)}), bf16[16,8,768]{2,1,0:T(8,128)(2,1)S(1)}, u32[]{:S(2)}, u32[]{:S(2)}) async-start(bf16[16,8,768]{2,1,0:T(8,128)(2,1)} %send_parts.1), calls=%async_computation | async-start | bytes 393216 | tf_op jit(solution)/shard_map/all_to_all | solution.py:21
  48.0 0.7 copy-start.10
  83.3 0.8 copy-start.5
  85.1 7.7 %copy-start.7 = (s32[96,2]{0,1:T(2,128)S(1)}, s32[96,2]{0,1:T(2,128)}, u32[]{:S(2)}) copy-start(s32[96,2]{0,1:T(2,128)} %param.37) | copy-start | bytes 2308
  85.1 21.2 %all-to-all-start.2 = ((bf16[16,96,128]{2,1,0:T(8,128)(2,1)}), bf16[16,96,128]{2,1,0:T(8,128)(2,1)S(1)}, u32[]{:S(2)}, u32[]{:S(2)}) async-start(bf16[16,96,128]{2,1,0:T(8,128)(2,1)} %broadcast_in_dim.30), calls=%async_computation.2 | async-start | bytes 786432 | tf_op jit(solution)/shard_map/all_to_all | solution.py:21
  93.2 13.2 %copy-start.4 = (bf16[96,128]{1,0:T(8,128)(2,1)S(1)}, bf16[96,128]{1,0:T(8,128)(2,1)}, u32[]{:S(2)}) copy-start(bf16[96,128]{1,0:T(8,128)(2,1)} %tok_ref.1) | copy-start | bytes 73732
  106.5 16.9 %copy-start.6 = (f32[2048]{0:T(1024)S(1)}, f32[2048]{0:T(1024)}, u32[]{:S(2)}) copy-start(f32[2048]{0:T(1024)} %param.36) | copy-start | bytes 24580
  123.2 2.0 %copy-start.3 = (bf16[1,2048,256]{2,1,0:T(8,128)(2,1)S(1)}, bf16[1,2048,256]{2,1,0:T(8,128)(2,1)}, u32[]{:S(2)}) copy-start(bf16[1,2048,256]{2,1,0:T(8,128)(2,1)} %param.40) | copy-start | bytes 3145732
  126.6 6.6 %copy-start.9 = (f32[96,2]{0,1:T(2,128)S(1)}, f32[96,2]{0,1:T(2,128)}, u32[]{:S(2)}) copy-start(f32[96,2]{0,1:T(2,128)} %param.38) | copy-start | bytes 2308
  126.6 21.0 %all-to-all-start.4 = ((bf16[16,32,128]{2,1,0:T(8,128)(2,1)}), bf16[16,32,128]{2,1,0:T(8,128)(2,1)S(1)}, u32[]{:S(2)}, u32[]{:S(2)}) async-start(bf16[16,32,128]{2,1,0:T(8,128)(2,1)} %bitcast.73), calls=%async_computation.4 | async-start | bytes 262144 | tf_op jit(solution)/shard_map/all_to_all | solution.py:21
  148.9 17.1 %all-to-all-start.5 = ((bf16[16,96,128]{2,1,0:T(8,128)(2,1)}), bf16[16,96,128]{2,1,0:T(8,128)(2,1)S(1)}, u32[]{:S(2)}, u32[]{:S(2)}) async-start(bf16[16,96,128]{2,1,0:T(8,128)(2,1)} %broadcast_in_dim.35), calls=%async_computation.5 | async-start | bytes 786432 | tf_op jit(solution)/shard_map/all_to_all | solution.py:21

commit v3 on v2

v3 whole, which is shorter than its diff:
```python
import functools

import jax
import jax.numpy as jnp
from jax import lax
from jax.experimental import pallas as pl
from jax.experimental.pallas import tpu as pltpu
from jax.sharding import PartitionSpec as P

NORM_EPS = 1e-05
HEAD_EPS = 1e-06
CAPACITY = 2
LANES = 128
PADDED = 8
GATE_SUMS = 16
F32 = jnp.float32
BF16 = jnp.bfloat16


def exchanged(blocks, axis):
    return lax.all_to_all(blocks, axis, split_axis=0, concat_axis=0, tiled=True)


def in_pieces(values, count):
    pieces = []
    for _ in range(count - 1):
        head = lax.reduce_precision(values, 8, 7)
        pieces.append(head)
        values = values - head
    pieces.append(values)
    return pieces


def rounded_pieces(values, count):
    pieces = []
    for _ in range(count):
        head = values.astype(BF16).astype(F32)
        pieces.append(head)
        values = values - head
    return pieces


def dot(a, b):
    return jnp.dot(a, b, preferred_element_type=F32)


def grid_index(shape):
    return lax.broadcasted_iota(jnp.int32, shape, 0), lax.broadcasted_iota(jnp.int32, shape, 1)


def one_hot(condition):
    return jnp.where(condition, 1.0, 0.0).astype(BF16)


def send_kernel(
    tok_ref, gain_ref, wq, wk, wv, wo, wi, wf, max_ref, out_ref, max_out, *, seq_local
):
    max_out[...] = max_ref[...]
    head = lax.axis_index("tp")
    seq_total, columns = tok_ref.shape
    ours = pl.ds(pl.multiple_of(lax.axis_index("ep") * columns, LANES), columns)
    blocks = seq_total // seq_local
    count = blocks * PADDED
    row, col = grid_index((count, seq_total))
    spread_rows = one_hot(
        ((row & (PADDED - 1)) < seq_local)
        & (col == (row >> 3) * seq_local + (row & (PADDED - 1)))
    )
    slot = lax.broadcasted_iota(jnp.int32, (count, columns), 0) & (PADDED - 1)
    values = dot(spread_rows, tok_ref[...])
    values = jnp.where(slot == seq_local, 1.0, values)
    own = slot[:, :1] < seq_local
    block_mean = jnp.where(own, jnp.sum(values, axis=1, keepdims=True) * (1.0 / columns), 0.0)
    offsets = values - block_mean
    moment = jnp.where(own, jnp.sum(offsets * offsets, axis=1, keepdims=True), 0.0)
    gain_row = gain_ref[:, ours]
    down, across = grid_index((columns, columns))
    gain_col = jnp.sum(jnp.where(down == across, gain_row, 0.0), axis=1, keepdims=True)
    exact = values.astype(BF16)
    parts = []
    for ref in (wq, wk, wv, wo):
        high, low = rounded_pieces(ref[...].astype(F32) * gain_col, 2)
        parts.append(dot(exact, high.astype(BF16)) + dot(exact, low.astype(BF16)))
    product = jnp.concatenate(parts, axis=1)
    tiles = product.reshape(blocks, PADDED, product.shape[1])
    sums = tiles[:, seq_local : seq_local + 1, :]
    centred = tiles - block_mean.reshape(blocks, PADDED, 1) * sums

    pick, _ = grid_index((wi.shape[0], columns))

    def gate_part(ref):
        chosen = jnp.sum(jnp.where(pick == head, ref[:, ours].astype(F32), 0.0), axis=0, keepdims=True)
        return jnp.sum(offsets * (chosen * gain_row), axis=1, keepdims=True)

    gates = [*rounded_pieces(gate_part(wi), 2), *rounded_pieces(gate_part(wf), 2)]
    lane = lax.broadcasted_iota(jnp.int32, (count, LANES), 1)
    start = jnp.where(slot[:, :1] == seq_local, GATE_SUMS, 0)
    table = jnp.zeros((count, LANES), F32)
    for k, piece in enumerate(gates):
        table = jnp.where(lane == start + k, piece, table)
    table = jnp.where(slot == PADDED - 1, 0.0, table)
    for k, piece in enumerate([*rounded_pieces(block_mean, 3), *rounded_pieces(moment, 2)]):
        table = jnp.where((lane == 4 + k) & own, piece, table)
    exact_table = table.astype(BF16)
    down, across = grid_index((count, count))
    same = (down >> 3) == (across >> 3)
    last = (down & (PADDED - 1)) == PADDED - 1
    inner = across & (PADDED - 1)
    laid = []
    for r in range(seq_local):
        laid.append(dot(one_hot(same & last & ((inner == r) | (inner == seq_local))), exact_table))
    side = jnp.concatenate(laid, axis=1).reshape(tiles.shape)
    out_ref[...] = (centred + side).astype(BF16)


def receive_kernel(
    in_bias, for_bias, got_ref, cell_ref, norm_ref, max_ref, gain_ref,
    mixed_ref, keep_ref, admit_ref, value_ref, norm_out, max_out, *, columns
):
    head = lax.axis_index("tp")
    blocks, padded, width = got_ref.shape
    seq_local, _, key_size, value_size = cell_ref.shape
    count = blocks * padded
    got = got_ref[...].astype(F32)
    flat = got.reshape(count, width).astype(BF16)
    down, across = grid_index((count, count))
    same = (down >> 3) == (across >> 3)
    inner = across & (PADDED - 1)
    outer = down & (PADDED - 1)
    table = jnp.zeros((count, LANES), F32)
    for r in range(seq_local):
        back = one_hot(same & (outer == r) & (inner == PADDED - 1))
        table = table + dot(back, flat[:, r * LANES : (r + 1) * LANES])
    sums = dot(one_hot(same & (inner == seq_local)), flat).reshape(blocks, padded, width)
    lane = lax.broadcasted_iota(jnp.int32, (count, LANES), 1)

    def lanes(first, number):
        kept = jnp.where((lane >= first) & (lane < first + number), table, 0.0)
        return jnp.sum(kept, axis=1, keepdims=True).reshape(blocks, padded, 1)

    means = lanes(4, 3)
    row_mean = jnp.sum(means, axis=0, keepdims=True) * (1.0 / blocks)
    shifts = means - row_mean
    spread = jnp.sum(lanes(7, 2) + columns * shifts * shifts, axis=0) * (1.0 / (blocks * columns))
    inv_scale = lax.rsqrt(spread + NORM_EPS)
    projected = inv_scale * jnp.sum(got + shifts * sums, axis=0)

    def rounded(a, b):
        return projected[:, a:b].astype(BF16).astype(F32)

    query = rounded(0, key_size) * key_size**-0.5
    key = rounded(key_size, 2 * key_size)
    value = rounded(2 * key_size, 2 * key_size + value_size)
    outgate = rounded(2 * key_size + value_size, width)
    input_pre = (
        inv_scale * jnp.sum(lanes(0, 2) + shifts * lanes(GATE_SUMS, 2), axis=0) + in_bias[head]
    )
    forget_pre = (
        inv_scale * jnp.sum(lanes(2, 2) + shifts * lanes(GATE_SUMS + 2, 2), axis=0)
        + for_bias[head]
    )
    down, across = grid_index((padded, seq_local))
    old_max = jnp.sum(jnp.where(down == across, max_ref[...], 0.0), axis=1, keepdims=True)
    log_forget = jnp.minimum(forget_pre, 0.0) - jnp.log1p(jnp.exp(-jnp.abs(forget_pre)))
    carried = log_forget + old_max
    new_max = jnp.maximum(carried, input_pre)
    keep_old = jnp.exp(carried - new_max)
    admit_key = jnp.exp(input_pre - new_max) * key
    max_out[...] = new_max[:seq_local]
    keep_ref[...] = keep_old[:seq_local]
    admit_ref[...] = admit_key[:seq_local]
    value_ref[...] = value[:seq_local]
    query_cols = query.T
    rows = lax.broadcasted_iota(jnp.int32, (padded, value_size), 0)
    against_cell = jnp.zeros((padded, value_size), F32)
    for s in range(seq_local):
        norm_out[s : s + 1] = keep_old[s : s + 1] * norm_ref[s] + admit_key[s : s + 1]
        read = jnp.sum(query_cols[:, s : s + 1] * cell_ref[s, 0], axis=0, keepdims=True)
        against_cell = jnp.where(rows == s, read, against_cell)
    scores = jnp.sum(query * admit_key, axis=1, keepdims=True)
    readout = jnp.where(rows < seq_local, keep_old * against_cell + scores * value, 0.0)
    outgate = jnp.where(rows < seq_local, outgate, 0.0)
    head_mean = jnp.mean(readout, axis=1, keepdims=True)
    around = readout - head_mean
    head_var = jnp.mean(around * around, axis=1, keepdims=True)
    gain = gain_ref[:, pl.ds(pl.multiple_of(head * value_size, LANES), value_size)]
    opened = 1.0 / (1.0 + jnp.exp(-outgate))
    mixed = around * lax.rsqrt(head_var + HEAD_EPS) * gain * opened
    mixed_ref[...] = jnp.broadcast_to(mixed[None], (blocks, padded, value_size)).astype(BF16)


def project_kernel(got_ref, weight_ref, out_ref, *, seq_local):
    blocks, padded, width = got_ref.shape
    seq_total = out_ref.shape[1]
    rows = got_ref[...].astype(F32).reshape(blocks * padded, width).astype(BF16)
    terms = dot(rows, weight_ref[...]).astype(BF16)
    row, col = grid_index((seq_total, blocks * padded))
    inner = col & (PADDED - 1)
    packed = dot(one_hot((inner < seq_local) & (row == (col >> 3) * seq_local + inner)), terms)
    out_ref[...] = jnp.broadcast_to(packed.astype(BF16)[None], out_ref.shape)


def stream_kernel(got_ref, tok_ref, picker_ref, stream_ref, out_ref):
    mixer_out = jnp.sum(got_ref[...].astype(F32), axis=0)
    stream = (tok_ref[...].astype(F32) + mixer_out).astype(BF16)
    stream_ref[...] = stream
    chosen = lax.dot_general(
        picker_ref[...], stream, (((0,), (0,)), ((), ())), preferred_element_type=F32
    )
    out_ref[...] = chosen.astype(BF16).reshape(out_ref.shape)


def expert_kernel(
    up_hbm, down_hbm, got_ref, gain_ref, gate_ref, out_ref, up_ref, down_ref, arrived
):
    fetches = [
        pltpu.make_async_copy(up_hbm, up_ref, arrived.at[0]),
        pltpu.make_async_copy(down_hbm, down_ref, arrived.at[1]),
    ]
    for fetch in fetches:
        fetch.start()
    blocks, _, columns = got_ref.shape
    values = jnp.concatenate([got_ref[e].astype(F32) for e in range(blocks)], axis=1)
    row_mean = jnp.mean(values, axis=1, keepdims=True)
    spread = jnp.mean(values * values, axis=1, keepdims=True) - row_mean * row_mean
    normed = ((values - row_mean) * lax.rsqrt(spread + NORM_EPS) * gain_ref[...]).astype(BF16)
    gate = dot(normed, gate_ref[0])
    fetches[0].wait()
    active = (gate / (1.0 + jnp.exp(-gate)) * dot(normed, up_ref[0])).astype(BF16)
    fetches[1].wait()
    result = dot(active, down_ref[0]).astype(BF16)
    for e in range(blocks):
        out_ref[e] = result[:, e * columns : (e + 1) * columns]


def combine_kernel(table_ref, back_ref, out_ref):
    seq_total = out_ref.shape[1]
    experts, slots, columns = back_ref.shape
    both = dot(table_ref[...], back_ref[...].reshape(experts * slots, columns))
    added = (both[:seq_total] + both[seq_total:]).astype(BF16)
    out_ref[...] = jnp.broadcast_to(added[None], out_ref.shape)


def in_vmem(array):
    return pltpu.with_memory_space_constraint(array, pltpu.VMEM)


def kernel_call(kernel, name, shapes, near, scalars=(), far=(), left=(), scratch=()):
    vmem = pl.BlockSpec(memory_space=pltpu.VMEM)
    smem = pl.BlockSpec(memory_space=pltpu.SMEM)
    return pl.pallas_call(
        kernel,
        in_specs=[smem] * len(scalars)
        + [pl.BlockSpec(memory_space=pl.ANY)] * len(left)
        + [vmem] * (len(far) + len(near)),
        out_specs=jax.tree.map(lambda _: vmem, shapes),
        out_shape=shapes,
        scratch_shapes=scratch,
        name=name,
    )(*scalars, *left, *far, *(in_vmem(a) for a in near))


def on_device(
    tokens,
    first_gain,
    w_query,
    w_key,
    w_value,
    w_outgate,
    w_input,
    w_forget,
    input_bias,
    forget_bias,
    head_gain,
    w_project,
    cell_state,
    norm_state,
    max_state,
    second_gain,
    routes,
    route_weight,
    expert_gate,
    expert_up,
    expert_down,
):
    blocks = lax.axis_size("ep")
    seq_total, columns = tokens.shape
    seq_local = seq_total // blocks
    value_size = cell_state.shape[3]
    experts = blocks
    slot_count = blocks * CAPACITY
    expert_ids = lax.broadcasted_iota(jnp.int32, (1, 1, experts), 2)
    matches = routes[:, :, None] == expert_ids
    routed = jnp.sum(matches.astype(jnp.int32), axis=1)
    combine = jnp.sum(jnp.where(matches, route_weight[:, :, None], 0.0), axis=1)
    running = (
        jnp.cumsum(routed.reshape(blocks, seq_local, experts), axis=1).reshape(seq_total, experts)
        - routed
    )
    block_ids = lax.broadcasted_iota(jnp.int32, (seq_total, experts), 0) // seq_local
    slot_of = block_ids * CAPACITY + running
    slot_ids = lax.broadcasted_iota(jnp.int32, (experts, slot_count, seq_total), 1)
    placed = (slot_of.T[:, None, :] == slot_ids) & (routed.T[:, None, :] > 0)
    picker = placed.astype(BF16).reshape(experts * slot_count, seq_total).T
    weighted = jnp.where(placed, combine.T[:, None, :], 0.0)

    width = 2 * (w_query.shape[1] + w_value.shape[1])
    outgoing, old_max = kernel_call(
        functools.partial(send_kernel, seq_local=seq_local),
        "send_parts",
        [pltpu.VMEM((blocks, PADDED, width), BF16), pltpu.VMEM((1, seq_local), F32)],
        (),
        far=(
            tokens,
            first_gain.reshape(1, -1),
            w_query,
            w_key,
            w_value,
            w_outgate,
            w_input.T,
            w_forget.T,
            max_state.T,
        ),
    )
    weight_rows = weighted.reshape(experts * slot_count, seq_total).T
    table = jnp.concatenate([t.astype(BF16) for t in in_pieces(weight_rows, 2)], axis=0)
    incoming, picker, table = lax.optimization_barrier((exchanged(outgoing, "ep"), picker, table))

    key_size = cell_state.shape[2]
    mixed, *updates = kernel_call(
        functools.partial(receive_kernel, columns=columns),
        "cell_step",
        [
            pltpu.VMEM((blocks, PADDED, value_size), BF16),
            pltpu.VMEM((seq_local, 1), F32),
            pltpu.VMEM((seq_local, key_size), F32),
            pltpu.VMEM((seq_local, value_size), F32),
            pltpu.VMEM((seq_local, key_size), F32),
            pltpu.VMEM((seq_local, 1), F32),
        ],
        (incoming, cell_state, norm_state, old_max, head_gain.reshape(1, -1)),
        scalars=(input_bias, forget_bias),
    )

    part_shape = pltpu.VMEM((lax.axis_size("tp"), seq_total, columns), BF16)
    head_terms = kernel_call(
        functools.partial(project_kernel, seq_local=seq_local),
        "project_heads",
        part_shape,
        (exchanged(mixed, "ep"), w_project),
    )
    stream, outbound = kernel_call(
        stream_kernel,
        "stream_rows",
        [
            pltpu.VMEM(tokens.shape, BF16),
            pltpu.VMEM((experts, slot_count, columns), BF16),
        ],
        (exchanged(head_terms, "tp"), tokens, picker),
    )

    slot_out = kernel_call(
        expert_kernel,
        "expert",
        pltpu.VMEM((blocks, slot_count, columns), BF16),
        (
            exchanged(outbound, "ep"),
            second_gain.reshape(1, -1),
            expert_gate,
        ),
        left=(expert_up, expert_down),
        scratch=(
            pltpu.VMEM(expert_up.shape, BF16),
            pltpu.VMEM(expert_down.shape, BF16),
            pltpu.SemaphoreType.DMA((2,)),
        ),
    )
    moe_terms = kernel_call(
        combine_kernel, "combine", part_shape, (table, exchanged(slot_out, "ep"))
    )
    moe_terms, *updates = lax.optimization_barrier((moe_terms, *updates))
    keep_old, admit_key, value, new_norm, new_max = updates
    new_cell = (
        keep_old[:, :, None] * cell_state[:, 0] + admit_key[:, :, None] * value[:, None, :]
    )
    moe_out = jnp.sum(exchanged(moe_terms, "tp").astype(F32), axis=0)
    layer_out = (stream.astype(F32) + moe_out).astype(BF16)
    return (layer_out, new_cell[:, None], new_norm[:, None], new_max)


def solution(mesh):
    placed = (
        P("grp", "ep"),
        P(),
        P("ep", "tp"),
        P("ep", "tp"),
        P("ep", "tp"),
        P("ep", "tp"),
        P(),
        P(),
        P(),
        P(),
        P(),
        P("tp", "ep"),
        P(("grp", "ep"), "tp", None, None),
        P(("grp", "ep"), "tp", None),
        P(("grp", "ep"), "tp"),
        P(),
        P("grp", None),
        P("grp", None),
        P("ep", None, "tp"),
        P("ep", None, "tp"),
        P("ep", "tp", None),
    )
    return jax.shard_map(
        on_device,
        mesh=mesh,
        in_specs=placed,
        out_specs=(
            P("grp", "ep"),
            P(("grp", "ep"), "tp", None, None),
            P(("grp", "ep"), "tp", None),
            P(("grp", "ep"), "tp"),
        ),
        check_vma=False,
    )
```

time: 170 us -> 165 us (0.971)
  blocking collectives: 34.2 us -> 75.8 us
  waiting for transfers between devices: 53.7 us -> 24.6 us
  starting transfers between devices: 62.1 us -> 47.7 us
  matrix products: 3.03 us -> 0 us
  Pallas kernels: 4.52 us -> 7.3 us
  local copies, waits for them, and re-layouts: 5.31 us -> 3.16 us
    all_to_all x1 -> x4, blocking collectives: 17.5 us -> 75.8 us  [exchanged(): return lax.all_to_all(blocks, axis, split_axis=0, concat_axis=0, tiled=True)]
    all_to_all x4 -> x2, waiting for transfers between devices: 53.7 us -> 24.6 us  [exchanged(): return lax.all_to_all(blocks, axis, split_axis=0, concat_axis=0, tiled=True)]
    all_to_all x1 -> x0, blocking collectives: 16.6 us -> none  [on_device(): lax.all_to_all(outbound, 'ep', split_axis=0, concat_axis=2, tiled=True)[0]]
    all_to_all x4 -> x2, starting transfers between devices: 62.1 us -> 47.7 us  [exchanged(): return lax.all_to_all(blocks, axis, split_axis=0, concat_axis=0, tiled=True)]
    dot_general x6 -> x0, matrix products: 3.03 us -> none  [the longest x1 1.49 us: on_device(): jnp.dot(normed, expert_gate[0], preferred_element_type=jnp.float32)]
    pallas_call x2 -> x6, Pallas kernels: 4.52 us -> 7.3 us  [kernel_call(): pl.pallas_call(kernel, in_specs=[smem] * len(scalars) + [pl.BlockSpec(mem...]
  transfers between devices with their start and end apart: 4 -> 2, of which waited for: 4 -> 2; matrix products, arithmetic and copies ran while one was open for 2% -> 2% of each run, Pallas kernels for 0% -> 0%
where the time goes in v3:
time: 165 us; the launch traced here: 162 us
  blocking collectives  75.8 us (46%)
  starting transfers between devices  47.7 us (29%)
  waiting for transfers between devices  24.6 us (15%)
  Pallas kernels  7.3 us (4%)
  local copies, waits for them, and re-layouts  3.16 us (2%)
  other arithmetic  2.09 us (1%)
    all_to_all x4, blocking collectives, exchanged(): return lax.all_to_all(blocks, axis, split_axis=0, concat_axis=0, tiled=True)  75.8 us
    all_to_all x2, starting transfers between devices, exchanged(): return lax.all_to_all(blocks, axis, split_axis=0, concat_axis=0, tiled=True)  47.7 us
    all_to_all x2, waiting for transfers between devices, exchanged(): return lax.all_to_all(blocks, axis, split_axis=0, concat_axis=0, tiled=True)  24.6 us
    pallas_call x6, Pallas kernels, kernel_call(): pl.pallas_call(kernel, in_specs=[smem] * len(scalars) + [pl.BlockSpec(mem...  7.3 us
  transfers between devices with their start and end apart: 2, of which 2 were waited for; matrix products, arithmetic and copies ran while one was open for 2% of the time, Pallas kernels for 0%

profile of v3, /device:TPU:80, one launch (start us, length us, event | category | flops | bytes accessed | tf_op | source)
XLA Modules:
  0.0 161.5 jit_solution(14632711492229640733)
XLA Ops:
  0.6 2.3 %send_parts.1 = (bf16[16,8,768]{2,1,0:T(8,128)(2,1)}, f32[1,6]{1,0:T(1,128)S(1)}) custom-call(bf16[96,128]{1,0:T(8,128)(2,1)} %tok_ref.3, f32[1,2048]{1,0:T(1,128)} %bitcast.29, bf16[128,128]{1,0:T(8,128)(2,1)} %wq.1, bf16[128,128]{1,0:T(8,128)(2,1)} %wk.1, bf16[128,256]{1,0:T(8,128)(2,1)} %wv.1, bf16[128,256]{1,0:T(8,128)(2,1)} %wo.1, ...), custom_call_target="tpu_custom_call" | custom-call | tf_op jit(solution)/shard_map/send_parts/pallas_call | solution.py:251
  2.9 43.7 %all-to-all-start = ((bf16[16,8,768]{2,1,0:T(8,128)(2,1)}), bf16[16,8,768]{2,1,0:T(8,128)(2,1)S(1)}, u32[]{:S(2)}, u32[]{:S(2)}) async-start(bf16[16,8,768]{2,1,0:T(8,128)(2,1)} %get-tuple-element.23), calls=%async_computation | async-start | bytes 393216 | tf_op jit(solution)/shard_map/all_to_all | solution.py:21
  46.6 0.0 copy-start.7
  46.7 0.7 copy-done.7
  47.3 0.1 copy.38
  47.4 0.6 copy-done.8
  48.0 0.1 iota.33
  48.1 0.1 reduce_window_sum.11
  48.2 0.1 copy.39
  48.3 0.1 copy.41
  48.5 0.1 copy.40
  48.6 0.1 copy.42
  48.8 0.0 copy-start
  48.8 0.1 reduce-precision_convert_fusion
  48.9 13.8 %all-to-all-done.got_ref = bf16[16,8,768]{2,1,0:T(8,128)(2,1)S(1)} async-done(((bf16[16,8,768]{2,1,0:T(8,128)(2,1)}), bf16[16,8,768]{2,1,0:T(8,128)(2,1)S(1)}, u32[]{:S(2)}, u32[]{:S(2)}) %all-to-all-start) | async-done | bytes 196640 | tf_op jit(solution)/shard_map/all_to_all | solution.py:21
  62.8 1.6 cell_step.1
  64.4 17.7 %all_to_all.30.got_ref = bf16[16,8,256]{2,1,0:T(8,128)(2,1)S(1)} all-to-all(bf16[16,8,256]{2,1,0:T(8,128)(2,1)S(1)} %get-tuple-element.26), channel_id=1, replica_groups=mesh['grp'=2,'ep'=16,'tp'=16] {'ep'}, dimensions={0} | all-to-all | bytes 131072 | tf_op jit(solution)/shard_map/all_to_all | solution.py:21
  82.1 0.3 project_heads.1
  82.4 20.9 %all_to_all.31.got_ref = bf16[16,96,128]{2,1,0:T(8,128)(2,1)S(1)} all-to-all(bf16[16,96,128]{2,1,0:T(8,128)(2,1)S(1)} %project_heads.1), channel_id=1, replica_groups=mesh['grp'=2,'ep'=16,'tp'=16] {'tp'}, dimensions={0} | all-to-all | bytes 786432 | tf_op jit(solution)/shard_map/all_to_all | solution.py:21
  103.3 0.2 stream_rows.1
  103.5 16.6 %all_to_all.32.got_ref = bf16[16,32,128]{2,1,0:T(8,128)(2,1)S(1)} all-to-all(bf16[16,32,128]{2,1,0:T(8,128)(2,1)S(1)} %get-tuple-element.30), channel_id=1, replica_groups=mesh['grp'=2,'ep'=16,'tp'=16] {'ep'}, dimensions={0} | all-to-all | bytes 262144 | tf_op jit(solution)/shard_map/all_to_all | solution.py:21
  120.1 1.9 %expert.1 = bf16[16,32,128]{2,1,0:T(8,128)(2,1)S(1)} custom-call(bf16[1,2048,256]{2,1,0:T(8,128)(2,1)} %up_hbm.1, bf16[1,256,2048]{2,1,0:T(8,128)(2,1)} %down_hbm.1, bf16[16,32,128]{2,1,0:T(8,128)(2,1)S(1)} %all_to_all.32.got_ref, f32[1,2048]{1,0:T(1,128)S(1)} %bitcast.21, bf16[1,2048,256]{2,1,0:T(8,128)(2,1)S(1)} %copy-done.1), custom_call_target="tpu_custom_call" | custom-call | tf_op jit(solution)/shard_map/expert/pallas_call | solution.py:251
  122.1 20.7 %all_to_all.33.back_ref = bf16[16,32,128]{2,1,0:T(8,128)(2,1)S(1)} all-to-all(bf16[16,32,128]{2,1,0:T(8,128)(2,1)S(1)} %expert.1), channel_id=1, replica_groups=mesh['grp'=2,'ep'=16,'tp'=16] {'ep'}, dimensions={0} | all-to-all | bytes 262144 | tf_op jit(solution)/shard_map/all_to_all | solution.py:21
  142.8 1.0 combine.1
  143.7 4.0 %all-to-all-start.5 = ((bf16[16,96,128]{2,1,0:T(8,128)(2,1)}), bf16[16,96,128]{2,1,0:T(8,128)(2,1)S(1)}, u32[]{:S(2)}, u32[]{:S(2)}) async-start(bf16[16,96,128]{2,1,0:T(8,128)(2,1)} %combine.1), calls=%async_computation.5 | async-start | bytes 786432 | tf_op jit(solution)/shard_map/all_to_all | solution.py:21
  147.7 0.6 copy.44
  148.3 0.6 copy.43
  148.9 0.1 reduce
  149.0 1.1 multiply_add_fusion
  150.1 10.7 %all-to-all-done.5 = bf16[16,96,128]{2,1,0:T(8,128)(2,1)S(1)} async-done(((bf16[16,96,128]{2,1,0:T(8,128)(2,1)}), bf16[16,96,128]{2,1,0:T(8,128)(2,1)S(1)}, u32[]{:S(2)}, u32[]{:S(2)}) %all-to-all-start.5) | async-done | bytes 393248 | tf_op jit(solution)/shard_map/all_to_all | solution.py:21
  160.8 0.1 convert_reduce_fusion
  160.9 0.6 add_convert_fusion
  (29 shorter events, 0.2 us)
Async XLA Ops:
  2.9 59.9 %all-to-all-start = ((bf16[16,8,768]{2,1,0:T(8,128)(2,1)}), bf16[16,8,768]{2,1,0:T(8,128)(2,1)S(1)}, u32[]{:S(2)}, u32[]{:S(2)}) async-start(bf16[16,8,768]{2,1,0:T(8,128)(2,1)} %get-tuple-element.23), calls=%async_computation | async-start | bytes 393216 | tf_op jit(solution)/shard_map/all_to_all | solution.py:21
  46.6 0.7 copy-start.7
  47.3 0.7 copy-start.8
  48.8 14.0 %copy-start = (f32[6,1,128,256]{3,2,1,0:T(8,128)S(1)}, f32[6,1,128,256]{3,2,1,0:T(8,128)}, u32[]{:S(2)}) copy-start(f32[6,1,128,256]{3,2,1,0:T(8,128)} %cell_ref.1) | copy-start | bytes 2359300
  48.9 13.9 %copy-start.4 = (f32[4096]{0:T(1024)S(1)}, f32[4096]{0:T(1024)}, u32[]{:S(2)}) copy-start(f32[4096]{0:T(1024)} %param.31) | copy-start | bytes 49156
  48.9 13.9 %copy-start.6 = (f32[6,1,128]{2,1,0:T(1,128)S(1)}, f32[6,1,128]{2,1,0:T(1,128)}, u32[]{:S(2)}) copy-start(f32[6,1,128]{2,1,0:T(1,128)} %norm_ref.1) | copy-start | bytes 9220
  64.4 17.7 %copy-start.3 = (bf16[256,128]{1,0:T(8,128)(2,1)S(1)}, bf16[256,128]{1,0:T(8,128)(2,1)}, u32[]{:S(2)}) copy-start(bf16[256,128]{1,0:T(8,128)(2,1)} %weight_ref.1) | copy-start | bytes 196612
  82.1 38.0 %copy-start.1 = (bf16[1,2048,256]{2,1,0:T(8,128)(2,1)S(1)}, bf16[1,2048,256]{2,1,0:T(8,128)(2,1)}, u32[]{:S(2)}) copy-start(bf16[1,2048,256]{2,1,0:T(8,128)(2,1)} %gate_ref.1) | copy-start | bytes 3145732
  82.4 20.9 %copy-start.2 = (bf16[96,128]{1,0:T(8,128)(2,1)S(1)}, bf16[96,128]{1,0:T(8,128)(2,1)}, u32[]{:S(2)}) copy-start(bf16[96,128]{1,0:T(8,128)(2,1)} %tok_ref.3) | copy-start | bytes 73732
  103.5 16.6 %copy-start.5 = (f32[2048]{0:T(1024)S(1)}, f32[2048]{0:T(1024)}, u32[]{:S(2)}) copy-start(f32[2048]{0:T(1024)} %param.36) | copy-start | bytes 24580
  143.7 17.1 %all-to-all-start.5 = ((bf16[16,96,128]{2,1,0:T(8,128)(2,1)}), bf16[16,96,128]{2,1,0:T(8,128)(2,1)S(1)}, u32[]{:S(2)}, u32[]{:S(2)}) async-start(bf16[16,96,128]{2,1,0:T(8,128)(2,1)} %combine.1), calls=%async_computation.5 | async-start | bytes 786432 | tf_op jit(solution)/shard_map/all_to_all | solution.py:21

commit v4 on v3

--- a/solution.py
+++ b/solution.py
@@ -19,6 +19,22 @@
 
 def exchanged(blocks, axis):
     return lax.all_to_all(blocks, axis, split_axis=0, concat_axis=0, tiled=True)
+
+
+def cores_of_chips(axis):
+    size = lax.axis_size(axis)
+    return [[i, i + 1] for i in range(0, size, 2)]
+
+
+def chips_of_cores(axis):
+    size = lax.axis_size(axis)
+    return [list(range(core, size, 2)) for core in range(2)]
+
+
+def swapped(blocks, groups):
+    return lax.all_to_all(
+        blocks, "tp", split_axis=0, concat_axis=0, tiled=True, axis_index_groups=groups
+    )
 
 
 def in_pieces(values, count):
@@ -198,6 +214,11 @@
     inner = col & (PADDED - 1)
     packed = dot(one_hot((inner < seq_local) & (row == (col >> 3) * seq_local + inner)), terms)
     out_ref[...] = jnp.broadcast_to(packed.astype(BF16)[None], out_ref.shape)
+
+
+def pair_kernel(got_ref, out_ref):
+    added = (got_ref[0].astype(F32) + got_ref[1].astype(F32)).astype(BF16)
+    out_ref[...] = jnp.broadcast_to(added[None], out_ref.shape)
 
 
 def stream_kernel(got_ref, tok_ref, picker_ref, stream_ref, out_ref):
@@ -342,12 +363,16 @@
         scalars=(input_bias, forget_bias),
     )
 
-    part_shape = pltpu.VMEM((lax.axis_size("tp"), seq_total, columns), BF16)
+    part_shape = pltpu.VMEM((2, seq_total, columns), BF16)
+    chip_shape = pltpu.VMEM((lax.axis_size("tp") // 2, seq_total, columns), BF16)
     head_terms = kernel_call(
         functools.partial(project_kernel, seq_local=seq_local),
         "project_heads",
         part_shape,
         (exchanged(mixed, "ep"), w_project),
+    )
+    chip_terms = kernel_call(
+        pair_kernel, "chip_heads", chip_shape, (swapped(head_terms, cores_of_chips("tp")),)
     )
     stream, outbound = kernel_call(
         stream_kernel,
@@ -356,7 +381,7 @@
             pltpu.VMEM(tokens.shape, BF16),
             pltpu.VMEM((experts, slot_count, columns), BF16),
         ],
-        (exchanged(head_terms, "tp"), tokens, picker),
+        (swapped(chip_terms, chips_of_cores("tp")), tokens, picker),
     )
 
     slot_out = kernel_call(
@@ -378,12 +403,15 @@
     moe_terms = kernel_call(
         combine_kernel, "combine", part_shape, (table, exchanged(slot_out, "ep"))
     )
+    moe_terms = kernel_call(
+        pair_kernel, "chip_moe", chip_shape, (swapped(moe_terms, cores_of_chips("tp")),)
+    )
     moe_terms, *updates = lax.optimization_barrier((moe_terms, *updates))
     keep_old, admit_key, value, new_norm, new_max = updates
     new_cell = (
         keep_old[:, :, None] * cell_state[:, 0] + admit_key[:, :, None] * value[:, None, :]
     )
-    moe_out = jnp.sum(exchanged(moe_terms, "tp").astype(F32), axis=0)
+    moe_out = jnp.sum(swapped(moe_terms, chips_of_cores("tp")).astype(F32), axis=0)
     layer_out = (stream.astype(F32) + moe_out).astype(BF16)
     return (layer_out, new_cell[:, None], new_norm[:, None], new_max)
 

time: 165 us -> 161 us (0.976); the launches traced: 162 us -> 160 us
  waiting for transfers between devices: 24.6 us -> 22.9 us
    all_to_all x0 -> x3, blocking collectives: none -> 25.5 us  [swapped(): lax.all_to_all(blocks, 'tp', split_axis=0, concat_axis=0, tiled=True, axi...]
    all_to_all x4 -> x3, blocking collectives: 75.8 us -> 50.9 us  [exchanged(): return lax.all_to_all(blocks, axis, split_axis=0, concat_axis=0, tiled=True)]
    all_to_all x2 -> x1, waiting for transfers between devices: 24.6 us -> 14.4 us  [exchanged(): return lax.all_to_all(blocks, axis, split_axis=0, concat_axis=0, tiled=True)]
    all_to_all x0 -> x1, waiting for transfers between devices: none -> 8.44 us  [swapped(): lax.all_to_all(blocks, 'tp', split_axis=0, concat_axis=0, tiled=True, axi...]
    all_to_all x0 -> x1, starting transfers between devices: none -> 4.38 us  [swapped(): lax.all_to_all(blocks, 'tp', split_axis=0, concat_axis=0, tiled=True, axi...]
    all_to_all x2 -> x1, starting transfers between devices: 47.7 us -> 43.8 us  [exchanged(): return lax.all_to_all(blocks, axis, split_axis=0, concat_axis=0, tiled=True)]
    pallas_call x6 -> x8, Pallas kernels: 7.3 us -> 7.34 us  [kernel_call(): pl.pallas_call(kernel, in_specs=[smem] * len(scalars) + [pl.BlockSpec(mem...]
where the time goes in v4:
time: 161 us; the launch traced here: 160 us
  blocking collectives  76.4 us (47%)
  starting transfers between devices  48.2 us (30%)
  waiting for transfers between devices  22.9 us (14%)
  Pallas kernels  7.34 us (5%)
  local copies, waits for them, and re-layouts  2.59 us (2%)
  other arithmetic  2.07 us (1%)
    all_to_all x3, blocking collectives, exchanged(): return lax.all_to_all(blocks, axis, split_axis=0, concat_axis=0, tiled=True)  50.9 us
    all_to_all x1, starting transfers between devices, exchanged(): return lax.all_to_all(blocks, axis, split_axis=0, concat_axis=0, tiled=True)  43.8 us
    all_to_all x3, blocking collectives, swapped(): lax.all_to_all(blocks, 'tp', split_axis=0, concat_axis=0, tiled=True, axi...  25.5 us
    all_to_all x1, waiting for transfers between devices, exchanged(): return lax.all_to_all(blocks, axis, split_axis=0, concat_axis=0, tiled=True)  14.4 us
    all_to_all x1, waiting for transfers between devices, swapped(): lax.all_to_all(blocks, 'tp', split_axis=0, concat_axis=0, tiled=True, axi...  8.44 us
    pallas_call x8, Pallas kernels, kernel_call(): pl.pallas_call(kernel, in_specs=[smem] * len(scalars) + [pl.BlockSpec(mem...  7.34 us
    all_to_all x1, starting transfers between devices, swapped(): lax.all_to_all(blocks, 'tp', split_axis=0, concat_axis=0, tiled=True, axi...  4.38 us
  transfers between devices with their start and end apart: 2, of which 2 were waited for; matrix products, arithmetic and copies ran while one was open for 2% of the time, Pallas kernels for 0%

profile of v4, /device:TPU:80, one launch (start us, length us, event | category | flops | bytes accessed | tf_op | source)
XLA Modules:
  0.0 160.3 jit_solution(2435679163455410276)
XLA Ops:
  0.6 2.3 %send_parts.1 = (bf16[16,8,768]{2,1,0:T(8,128)(2,1)}, f32[1,6]{1,0:T(1,128)S(1)}) custom-call(bf16[96,128]{1,0:T(8,128)(2,1)} %tok_ref.3, f32[1,2048]{1,0:T(1,128)} %bitcast.29, bf16[128,128]{1,0:T(8,128)(2,1)} %wq.1, bf16[128,128]{1,0:T(8,128)(2,1)} %wk.1, bf16[128,256]{1,0:T(8,128)(2,1)} %wv.1, bf16[128,256]{1,0:T(8,128)(2,1)} %wo.1, ...), custom_call_target="tpu_custom_call" | custom-call | tf_op jit(solution)/shard_map/send_parts/pallas_call | solution.py:272
  2.9 43.8 %all-to-all-start = ((bf16[16,8,768]{2,1,0:T(8,128)(2,1)}), bf16[16,8,768]{2,1,0:T(8,128)(2,1)S(1)}, u32[]{:S(2)}, u32[]{:S(2)}) async-start(bf16[16,8,768]{2,1,0:T(8,128)(2,1)} %get-tuple-element.23), calls=%async_computation | async-start | bytes 393216 | tf_op jit(solution)/shard_map/all_to_all | solution.py:21
  46.8 0.1 copy.38
  46.9 0.0 copy-start.8
  46.9 0.7 copy-done.8
  47.6 0.1 copy.42
  47.8 0.1 copy.41
  47.9 0.1 reduce_window_sum.11
  48.0 0.1 copy.39
  48.1 0.1 copy.40
  48.3 0.1 iota.33
  48.3 0.1 reduce-precision_convert_fusion
  48.5 14.4 %all-to-all-done.got_ref = bf16[16,8,768]{2,1,0:T(8,128)(2,1)S(1)} async-done(((bf16[16,8,768]{2,1,0:T(8,128)(2,1)}), bf16[16,8,768]{2,1,0:T(8,128)(2,1)S(1)}, u32[]{:S(2)}, u32[]{:S(2)}) %all-to-all-start) | async-done | bytes 196640 | tf_op jit(solution)/shard_map/all_to_all | solution.py:21
  63.0 1.7 %cell_step.1 = (bf16[16,8,256]{2,1,0:T(8,128)(2,1)S(1)}, f32[6,1]{1,0:T(8,128)S(1)}, f32[6,128]{1,0:T(8,128)S(1)}, f32[6,256]{1,0:T(8,128)S(1)}, f32[6,128]{1,0:T(8,128)S(1)}, /*index=5*/f32[6,1]{1,0:T(8,128)S(1)}) custom-call(f32[16]{0:T(128)} %in_bias.1, f32[16]{0:T(128)} %for_bias.1, bf16[16,8,768]{2,1,0:T(8,128)(2,1)S(1)} %all-to-all-done.got_ref, ...), custom_call_target="tpu_custom_call" | custom-call | tf_op jit(solution)/shard_map/cell_step/pallas_call | solution.py:272
  64.7 17.6 %all_to_all.40.got_ref = bf16[16,8,256]{2,1,0:T(8,128)(2,1)S(1)} all-to-all(bf16[16,8,256]{2,1,0:T(8,128)(2,1)S(1)} %get-tuple-element.26), channel_id=1, replica_groups=mesh['grp'=2,'ep'=16,'tp'=16] {'ep'}, dimensions={0} | all-to-all | bytes 131072 | tf_op jit(solution)/shard_map/all_to_all | solution.py:21
  82.3 0.3 project_heads.1
  82.6 3.8 %all_to_all.41.got_ref = bf16[2,96,128]{2,1,0:T(8,128)(2,1)S(1)} all-to-all(bf16[2,96,128]{2,1,0:T(8,128)(2,1)S(1)} %project_heads.1), channel_id=1, replica_groups={{0,1},{2,3},{4,5},{6,7},{8,9},{10,11},{12,13},{14,15},{16,17},{18,19},{..., dimensions={0} | all-to-all | bytes 98304 | tf_op jit(solution)/shard_map/all_to_all | solution.py:35
  86.5 17.9 %all_to_all.42.got_ref = bf16[8,96,128]{2,1,0:T(8,128)(2,1)S(1)} all-to-all(bf16[8,96,128]{2,1,0:T(8,128)(2,1)S(1)} %chip_heads.1), channel_id=1, replica_groups={{0,2,4,6,8,10,12,14},{1,3,5,7,9,11,13,15},{16,18,20,22,24,26,28,30},{17..., dimensions={0} | all-to-all | bytes 393216 | tf_op jit(solution)/shard_map/all_to_all | solution.py:35
  104.4 0.2 stream_rows.1
  104.6 17.1 %all_to_all.43.got_ref = bf16[16,32,128]{2,1,0:T(8,128)(2,1)S(1)} all-to-all(bf16[16,32,128]{2,1,0:T(8,128)(2,1)S(1)} %get-tuple-element.30), channel_id=1, replica_groups=mesh['grp'=2,'ep'=16,'tp'=16] {'ep'}, dimensions={0} | all-to-all | bytes 262144 | tf_op jit(solution)/shard_map/all_to_all | solution.py:21
  121.7 1.9 %expert.1 = bf16[16,32,128]{2,1,0:T(8,128)(2,1)S(1)} custom-call(bf16[1,2048,256]{2,1,0:T(8,128)(2,1)} %up_hbm.1, bf16[1,256,2048]{2,1,0:T(8,128)(2,1)} %down_hbm.1, bf16[16,32,128]{2,1,0:T(8,128)(2,1)S(1)} %all_to_all.43.got_ref, f32[1,2048]{1,0:T(1,128)S(1)} %bitcast.21, bf16[1,2048,256]{2,1,0:T(8,128)(2,1)S(1)} %copy-done.1), custom_call_target="tpu_custom_call" | custom-call | tf_op jit(solution)/shard_map/expert/pallas_call | solution.py:272
  123.6 16.2 %all_to_all.44.back_ref = bf16[16,32,128]{2,1,0:T(8,128)(2,1)S(1)} all-to-all(bf16[16,32,128]{2,1,0:T(8,128)(2,1)S(1)} %expert.1), channel_id=1, replica_groups=mesh['grp'=2,'ep'=16,'tp'=16] {'ep'}, dimensions={0} | all-to-all | bytes 262144 | tf_op jit(solution)/shard_map/all_to_all | solution.py:21
  139.8 0.2 combine.1
  140.0 3.8 %all_to_all.45.got_ref = bf16[2,96,128]{2,1,0:T(8,128)(2,1)S(1)} all-to-all(bf16[2,96,128]{2,1,0:T(8,128)(2,1)S(1)} %combine.1), channel_id=1, replica_groups={{0,1},{2,3},{4,5},{6,7},{8,9},{10,11},{12,13},{14,15},{16,17},{18,19},{..., dimensions={0} | all-to-all | bytes 98304 | tf_op jit(solution)/shard_map/all_to_all | solution.py:35
  143.8 0.7 chip_moe.1
  144.5 4.4 %all-to-all-start.7 = ((bf16[8,96,128]{2,1,0:T(8,128)(2,1)}), bf16[8,96,128]{2,1,0:T(8,128)(2,1)S(1)}, u32[]{:S(2)}, u32[]{:S(2)}) async-start(bf16[8,96,128]{2,1,0:T(8,128)(2,1)} %chip_moe.1), calls=%async_computation.7 | async-start | bytes 393216 | tf_op jit(solution)/shard_map/all_to_all | solution.py:35
  148.9 0.6 copy.43
  149.5 0.6 copy.44
  150.1 0.1 reduce
  150.2 1.1 multiply_add_fusion
  151.2 8.4 %all-to-all-done.7 = bf16[8,96,128]{2,1,0:T(8,128)(2,1)S(1)} async-done(((bf16[8,96,128]{2,1,0:T(8,128)(2,1)}), bf16[8,96,128]{2,1,0:T(8,128)(2,1)S(1)}, u32[]{:S(2)}, u32[]{:S(2)}) %all-to-all-start.7) | async-done | bytes 196640 | tf_op jit(solution)/shard_map/all_to_all | solution.py:35
  159.7 0.6 add_convert_fusion
  (33 shorter events, 0.3 us)
Async XLA Ops:
  2.9 43.8 %copy-start.7 = (s32[96,2]{0,1:T(2,128)S(1)}, s32[96,2]{0,1:T(2,128)}, u32[]{:S(2)}) copy-start(s32[96,2]{0,1:T(2,128)} %param.37) | copy-start | bytes 2308
  2.9 60.0 %all-to-all-start = ((bf16[16,8,768]{2,1,0:T(8,128)(2,1)}), bf16[16,8,768]{2,1,0:T(8,128)(2,1)S(1)}, u32[]{:S(2)}, u32[]{:S(2)}) async-start(bf16[16,8,768]{2,1,0:T(8,128)(2,1)} %get-tuple-element.23), calls=%async_computation | async-start | bytes 393216 | tf_op jit(solution)/shard_map/all_to_all | solution.py:21
  46.9 0.7 copy-start.8
  48.2 14.7 %copy-start = (f32[6,1,128,256]{3,2,1,0:T(8,128)S(1)}, f32[6,1,128,256]{3,2,1,0:T(8,128)}, u32[]{:S(2)}) copy-start(f32[6,1,128,256]{3,2,1,0:T(8,128)} %cell_ref.1) | copy-start | bytes 2359300
  48.5 14.5 %copy-start.4 = (f32[4096]{0:T(1024)S(1)}, f32[4096]{0:T(1024)}, u32[]{:S(2)}) copy-start(f32[4096]{0:T(1024)} %param.31) | copy-start | bytes 49156
  48.5 14.4 %copy-start.6 = (f32[6,1,128]{2,1,0:T(1,128)S(1)}, f32[6,1,128]{2,1,0:T(1,128)}, u32[]{:S(2)}) copy-start(f32[6,1,128]{2,1,0:T(1,128)} %norm_ref.1) | copy-start | bytes 9220
  62.9 19.4 %copy-start.3 = (bf16[256,128]{1,0:T(8,128)(2,1)S(1)}, bf16[256,128]{1,0:T(8,128)(2,1)}, u32[]{:S(2)}) copy-start(bf16[256,128]{1,0:T(8,128)(2,1)} %weight_ref.1) | copy-start | bytes 196612
  63.0 41.4 %copy-start.2 = (bf16[96,128]{1,0:T(8,128)(2,1)S(1)}, bf16[96,128]{1,0:T(8,128)(2,1)}, u32[]{:S(2)}) copy-start(bf16[96,128]{1,0:T(8,128)(2,1)} %tok_ref.3) | copy-start | bytes 73732
  64.7 57.0 %copy-start.1 = (bf16[1,2048,256]{2,1,0:T(8,128)(2,1)S(1)}, bf16[1,2048,256]{2,1,0:T(8,128)(2,1)}, u32[]{:S(2)}) copy-start(bf16[1,2048,256]{2,1,0:T(8,128)(2,1)} %gate_ref.1) | copy-start | bytes 3145732
  104.6 17.1 %copy-start.5 = (f32[2048]{0:T(1024)S(1)}, f32[2048]{0:T(1024)}, u32[]{:S(2)}) copy-start(f32[2048]{0:T(1024)} %param.36) | copy-start | bytes 24580
  144.5 15.2 %all-to-all-start.7 = ((bf16[8,96,128]{2,1,0:T(8,128)(2,1)}), bf16[8,96,128]{2,1,0:T(8,128)(2,1)S(1)}, u32[]{:S(2)}, u32[]{:S(2)}) async-start(bf16[8,96,128]{2,1,0:T(8,128)(2,1)} %chip_moe.1), calls=%async_computation.7 | async-start | bytes 393216 | tf_op jit(solution)/shard_map/all_to_all | solution.py:35

commit v5 on v4

--- a/solution.py
+++ b/solution.py
@@ -21,9 +21,9 @@
     return lax.all_to_all(blocks, axis, split_axis=0, concat_axis=0, tiled=True)
 
 
-def cores_of_chips(axis):
-    size = lax.axis_size(axis)
-    return [[i, i + 1] for i in range(0, size, 2)]
+def from_other_core(array):
+    size = lax.axis_size("tp")
+    return lax.ppermute(array, "tp", [(i, i ^ 1) for i in range(size)])
 
 
 def chips_of_cores(axis):
@@ -92,11 +92,11 @@
     gain_row = gain_ref[:, ours]
     down, across = grid_index((columns, columns))
     gain_col = jnp.sum(jnp.where(down == across, gain_row, 0.0), axis=1, keepdims=True)
-    exact = values.astype(BF16)
+    exact = jnp.concatenate([values.astype(BF16)] * 2, axis=1)
     parts = []
     for ref in (wq, wk, wv, wo):
-        high, low = rounded_pieces(ref[...].astype(F32) * gain_col, 2)
-        parts.append(dot(exact, high.astype(BF16)) + dot(exact, low.astype(BF16)))
+        pieces = rounded_pieces(ref[...].astype(F32) * gain_col, 2)
+        parts.append(dot(exact, jnp.concatenate([p.astype(BF16) for p in pieces], axis=0)))
     product = jnp.concatenate(parts, axis=1)
     tiles = product.reshape(blocks, PADDED, product.shape[1])
     sums = tiles[:, seq_local : seq_local + 1, :]
@@ -122,10 +122,13 @@
     same = (down >> 3) == (across >> 3)
     last = (down & (PADDED - 1)) == PADDED - 1
     inner = across & (PADDED - 1)
-    laid = []
-    for r in range(seq_local):
-        laid.append(dot(one_hot(same & last & ((inner == r) | (inner == seq_local))), exact_table))
-    side = jnp.concatenate(laid, axis=1).reshape(tiles.shape)
+    moves = [
+        one_hot(same & last & ((inner == r) | (inner == seq_local))) for r in range(seq_local)
+    ]
+    laid = dot(jnp.concatenate(moves, axis=0), exact_table)
+    side = jnp.concatenate(
+        [laid[r * count : (r + 1) * count] for r in range(seq_local)], axis=1
+    ).reshape(tiles.shape)
     out_ref[...] = (centred + side).astype(BF16)
 
 
@@ -143,11 +146,14 @@
     same = (down >> 3) == (across >> 3)
     inner = across & (PADDED - 1)
     outer = down & (PADDED - 1)
-    table = jnp.zeros((count, LANES), F32)
-    for r in range(seq_local):
-        back = one_hot(same & (outer == r) & (inner == PADDED - 1))
-        table = table + dot(back, flat[:, r * LANES : (r + 1) * LANES])
-    sums = dot(one_hot(same & (inner == seq_local)), flat).reshape(blocks, padded, width)
+    moves = [
+        one_hot(same & (outer == r) & (inner == PADDED - 1)) for r in range(seq_local)
+    ]
+    table = dot(
+        jnp.concatenate(moves, axis=1),
+        jnp.concatenate([flat[:, r * LANES : (r + 1) * LANES] for r in range(seq_local)], axis=0),
+    )
+    sums = got[:, seq_local : seq_local + 1, :]
     lane = lax.broadcasted_iota(jnp.int32, (count, LANES), 1)
 
     def lanes(first, number):
@@ -207,17 +213,17 @@
 
 def project_kernel(got_ref, weight_ref, out_ref, *, seq_local):
     blocks, padded, width = got_ref.shape
-    seq_total = out_ref.shape[1]
+    seq_total = out_ref.shape[0]
     rows = got_ref[...].astype(F32).reshape(blocks * padded, width).astype(BF16)
     terms = dot(rows, weight_ref[...]).astype(BF16)
     row, col = grid_index((seq_total, blocks * padded))
     inner = col & (PADDED - 1)
     packed = dot(one_hot((inner < seq_local) & (row == (col >> 3) * seq_local + inner)), terms)
-    out_ref[...] = jnp.broadcast_to(packed.astype(BF16)[None], out_ref.shape)
-
-
-def pair_kernel(got_ref, out_ref):
-    added = (got_ref[0].astype(F32) + got_ref[1].astype(F32)).astype(BF16)
+    out_ref[...] = packed.astype(BF16)
+
+
+def pair_kernel(own_ref, other_ref, out_ref):
+    added = (own_ref[...].astype(F32) + other_ref[...].astype(F32)).astype(BF16)
     out_ref[...] = jnp.broadcast_to(added[None], out_ref.shape)
 
 
@@ -255,11 +261,10 @@
 
 
 def combine_kernel(table_ref, back_ref, out_ref):
-    seq_total = out_ref.shape[1]
+    seq_total = out_ref.shape[0]
     experts, slots, columns = back_ref.shape
     both = dot(table_ref[...], back_ref[...].reshape(experts * slots, columns))
-    added = (both[:seq_total] + both[seq_total:]).astype(BF16)
-    out_ref[...] = jnp.broadcast_to(added[None], out_ref.shape)
+    out_ref[...] = (both[:seq_total] + both[seq_total:]).astype(BF16)
 
 
 def in_vmem(array):
@@ -363,7 +368,7 @@
         scalars=(input_bias, forget_bias),
     )
 
-    part_shape = pltpu.VMEM((2, seq_total, columns), BF16)
+    part_shape = pltpu.VMEM((seq_total, columns), BF16)
     chip_shape = pltpu.VMEM((lax.axis_size("tp") // 2, seq_total, columns), BF16)
     head_terms = kernel_call(
         functools.partial(project_kernel, seq_local=seq_local),
@@ -372,7 +377,7 @@
         (exchanged(mixed, "ep"), w_project),
     )
     chip_terms = kernel_call(
-        pair_kernel, "chip_heads", chip_shape, (swapped(head_terms, cores_of_chips("tp")),)
+        pair_kernel, "chip_heads", chip_shape, (head_terms, from_other_core(head_terms))
     )
     stream, outbound = kernel_call(
         stream_kernel,
@@ -404,7 +409,7 @@
         combine_kernel, "combine", part_shape, (table, exchanged(slot_out, "ep"))
     )
     moe_terms = kernel_call(
-        pair_kernel, "chip_moe", chip_shape, (swapped(moe_terms, cores_of_chips("tp")),)
+        pair_kernel, "chip_moe", chip_shape, (moe_terms, from_other_core(moe_terms))
     )
     moe_terms, *updates = lax.optimization_barrier((moe_terms, *updates))
     keep_old, admit_key, value, new_norm, new_max = updates

time: 161 us -> 160 us (level)
  blocking collectives: 76.4 us -> 68.9 us
  starting transfers between devices: 48.2 us -> 52.1 us
  waiting for transfers between devices: 22.9 us -> 25.2 us
    all_to_all x3 -> x1, blocking collectives: 25.5 us -> 17.9 us  [swapped(): lax.all_to_all(blocks, 'tp', split_axis=0, concat_axis=0, tiled=True, axi...]
    ppermute x0 -> x2, starting transfers between devices: none -> 3.9 us  [from_other_core(): return lax.ppermute(array, 'tp', [(i, i ^ 1) for i in range(size)])]
    ppermute x0 -> x2, waiting for transfers between devices: none -> 2.32 us  [from_other_core(): return lax.ppermute(array, 'tp', [(i, i ^ 1) for i in range(size)])]
  transfers between devices with their start and end apart: 2 -> 4, of which waited for: 2 -> 4; matrix products, arithmetic and copies ran while one was open for 2% -> 2% of each run, Pallas kernels for 0% -> 0%
where the time goes in v5:
time: 160 us; the launch traced here: 159 us
  blocking collectives  68.9 us (43%)
  starting transfers between devices  52.1 us (33%)
  waiting for transfers between devices  25.2 us (16%)
  Pallas kernels  7.3 us (5%)
  local copies, waits for them, and re-layouts  2.59 us (2%)
  other arithmetic  2.06 us (1%)
    all_to_all x3, blocking collectives, exchanged(): return lax.all_to_all(blocks, axis, split_axis=0, concat_axis=0, tiled=True)  51 us
    all_to_all x1, starting transfers between devices, exchanged(): return lax.all_to_all(blocks, axis, split_axis=0, concat_axis=0, tiled=True)  43.8 us
    all_to_all x1, blocking collectives, swapped(): lax.all_to_all(blocks, 'tp', split_axis=0, concat_axis=0, tiled=True, axi...  17.9 us
    all_to_all x1, waiting for transfers between devices, exchanged(): return lax.all_to_all(blocks, axis, split_axis=0, concat_axis=0, tiled=True)  14.4 us
    all_to_all x1, waiting for transfers between devices, swapped(): lax.all_to_all(blocks, 'tp', split_axis=0, concat_axis=0, tiled=True, axi...  8.44 us
    pallas_call x8, Pallas kernels, kernel_call(): pl.pallas_call(kernel, in_specs=[smem] * len(scalars) + [pl.BlockSpec(mem...  7.3 us
    all_to_all x1, starting transfers between devices, swapped(): lax.all_to_all(blocks, 'tp', split_axis=0, concat_axis=0, tiled=True, axi...  4.36 us
    ppermute x2, starting transfers between devices, from_other_core(): return lax.ppermute(array, 'tp', [(i, i ^ 1) for i in range(size)])  3.9 us
  transfers between devices with their start and end apart: 4, of which 4 were waited for; matrix products, arithmetic and copies ran while one was open for 2% of the time, Pallas kernels for 0%

profile of v5, /device:TPU:80, one launch (start us, length us, event | category | flops | bytes accessed | tf_op | source)
XLA Modules:
  0.0 159.0 jit_solution(349216876297547186)
XLA Ops:
  0.6 2.3 %send_parts.1 = (bf16[16,8,768]{2,1,0:T(8,128)(2,1)}, f32[1,6]{1,0:T(1,128)S(1)}) custom-call(bf16[96,128]{1,0:T(8,128)(2,1)} %tok_ref.3, f32[1,2048]{1,0:T(1,128)} %bitcast.29, bf16[128,128]{1,0:T(8,128)(2,1)} %wq.1, bf16[128,128]{1,0:T(8,128)(2,1)} %wk.1, bf16[128,256]{1,0:T(8,128)(2,1)} %wv.1, bf16[128,256]{1,0:T(8,128)(2,1)} %wo.1, ...), custom_call_target="tpu_custom_call" | custom-call | tf_op jit(solution)/shard_map/send_parts/pallas_call | solution.py:277
  2.9 43.8 %all-to-all-start = ((bf16[16,8,768]{2,1,0:T(8,128)(2,1)}), bf16[16,8,768]{2,1,0:T(8,128)(2,1)S(1)}, u32[]{:S(2)}, u32[]{:S(2)}) async-start(bf16[16,8,768]{2,1,0:T(8,128)(2,1)} %get-tuple-element.23), calls=%async_computation | async-start | bytes 393216 | tf_op jit(solution)/shard_map/all_to_all | solution.py:21
  46.8 0.1 copy.38
  46.9 0.7 copy-done.8
  47.6 0.1 copy.42
  47.8 0.1 copy.41
  47.9 0.1 reduce_window_sum.11
  48.1 0.1 copy.40
  48.3 0.1 iota.33
  48.4 0.1 reduce-precision_convert_fusion
  48.5 14.4 %all-to-all-done.got_ref = bf16[16,8,768]{2,1,0:T(8,128)(2,1)S(1)} async-done(((bf16[16,8,768]{2,1,0:T(8,128)(2,1)}), bf16[16,8,768]{2,1,0:T(8,128)(2,1)S(1)}, u32[]{:S(2)}, u32[]{:S(2)}) %all-to-all-start) | async-done | bytes 196640 | tf_op jit(solution)/shard_map/all_to_all | solution.py:21
  63.0 1.7 %cell_step.1 = (bf16[16,8,256]{2,1,0:T(8,128)(2,1)S(1)}, f32[6,1]{1,0:T(8,128)S(1)}, f32[6,128]{1,0:T(8,128)S(1)}, f32[6,256]{1,0:T(8,128)S(1)}, f32[6,128]{1,0:T(8,128)S(1)}, /*index=5*/f32[6,1]{1,0:T(8,128)S(1)}) custom-call(f32[16]{0:T(128)} %in_bias.1, f32[16]{0:T(128)} %for_bias.1, bf16[16,8,768]{2,1,0:T(8,128)(2,1)S(1)} %all-to-all-done.got_ref, ...), custom_call_target="tpu_custom_call" | custom-call | tf_op jit(solution)/shard_map/cell_step/pallas_call | solution.py:277
  64.7 17.7 %all_to_all.30.got_ref = bf16[16,8,256]{2,1,0:T(8,128)(2,1)S(1)} all-to-all(bf16[16,8,256]{2,1,0:T(8,128)(2,1)S(1)} %get-tuple-element.26), channel_id=1, replica_groups=mesh['grp'=2,'ep'=16,'tp'=16] {'ep'}, dimensions={0} | all-to-all | bytes 131072 | tf_op jit(solution)/shard_map/all_to_all | solution.py:21
  82.3 0.3 project_heads.1.own_ref
  82.6 2.0 %collective-permute-start = (bf16[96,128]{1,0:T(8,128)(2,1)S(1)}, bf16[96,128]{1,0:T(8,128)(2,1)S(1)}, u32[]{:S(2)}, u32[]{:S(2)}) collective-permute-start(bf16[96,128]{1,0:T(8,128)(2,1)S(1)} %project_heads.1.own_ref), channel_id=1, source_target_pairs={{0,1},{1,0},{2,3},{3,2},{4,5},{5,4},{6,7},{7,6},{8,9},{9,8},{10,11... | collective-permute-start | bytes 73736 | tf_op jit(solution)/shard_map/ppermute | solution.py:26
  84.6 1.2 collective-permute-done.other_ref
  85.8 17.9 %all_to_all.31.got_ref = bf16[8,96,128]{2,1,0:T(8,128)(2,1)S(1)} all-to-all(bf16[8,96,128]{2,1,0:T(8,128)(2,1)S(1)} %chip_heads.1), channel_id=1, replica_groups={{0,2,4,6,8,10,12,14},{1,3,5,7,9,11,13,15},{16,18,20,22,24,26,28,30},{17..., dimensions={0} | all-to-all | bytes 393216 | tf_op jit(solution)/shard_map/all_to_all | solution.py:35
  103.7 0.2 stream_rows.1
  103.9 17.0 %all_to_all.32.got_ref = bf16[16,32,128]{2,1,0:T(8,128)(2,1)S(1)} all-to-all(bf16[16,32,128]{2,1,0:T(8,128)(2,1)S(1)} %get-tuple-element.30), channel_id=1, replica_groups=mesh['grp'=2,'ep'=16,'tp'=16] {'ep'}, dimensions={0} | all-to-all | bytes 262144 | tf_op jit(solution)/shard_map/all_to_all | solution.py:21
  121.0 1.9 %expert.1 = bf16[16,32,128]{2,1,0:T(8,128)(2,1)S(1)} custom-call(bf16[1,2048,256]{2,1,0:T(8,128)(2,1)} %up_hbm.1, bf16[1,256,2048]{2,1,0:T(8,128)(2,1)} %down_hbm.1, bf16[16,32,128]{2,1,0:T(8,128)(2,1)S(1)} %all_to_all.32.got_ref, f32[1,2048]{1,0:T(1,128)S(1)} %bitcast.21, bf16[1,2048,256]{2,1,0:T(8,128)(2,1)S(1)} %copy-done.1), custom_call_target="tpu_custom_call" | custom-call | tf_op jit(solution)/shard_map/expert/pallas_call | solution.py:277
  122.9 16.3 %all_to_all.33.back_ref = bf16[16,32,128]{2,1,0:T(8,128)(2,1)S(1)} all-to-all(bf16[16,32,128]{2,1,0:T(8,128)(2,1)S(1)} %expert.1), channel_id=1, replica_groups=mesh['grp'=2,'ep'=16,'tp'=16] {'ep'}, dimensions={0} | all-to-all | bytes 262144 | tf_op jit(solution)/shard_map/all_to_all | solution.py:21
  139.2 0.2 combine.1.own_ref
  139.4 2.0 %collective-permute-start.1 = (bf16[96,128]{1,0:T(8,128)(2,1)S(1)}, bf16[96,128]{1,0:T(8,128)(2,1)S(1)}, u32[]{:S(2)}, u32[]{:S(2)}) collective-permute-start(bf16[96,128]{1,0:T(8,128)(2,1)S(1)} %combine.1.own_ref), channel_id=1, source_target_pairs={{0,1},{1,0},{2,3},{3,2},{4,5},{5,4},{6,7},{7,6},{8,9},{9,8},{10,11... | collective-permute-start | bytes 73736 | tf_op jit(solution)/shard_map/ppermute | solution.py:26
  141.4 1.2 collective-permute-done.1.other_ref
  142.5 0.7 chip_moe.1
  143.2 4.4 %all-to-all-start.5 = ((bf16[8,96,128]{2,1,0:T(8,128)(2,1)}), bf16[8,96,128]{2,1,0:T(8,128)(2,1)S(1)}, u32[]{:S(2)}, u32[]{:S(2)}) async-start(bf16[8,96,128]{2,1,0:T(8,128)(2,1)} %chip_moe.1), calls=%async_computation.5 | async-start | bytes 393216 | tf_op jit(solution)/shard_map/all_to_all | solution.py:35
  147.6 0.6 copy.43
  148.2 0.6 copy.44
  148.8 0.1 reduce
  148.9 1.1 multiply_add_fusion
  150.0 8.4 %all-to-all-done.5 = bf16[8,96,128]{2,1,0:T(8,128)(2,1)S(1)} async-done(((bf16[8,96,128]{2,1,0:T(8,128)(2,1)}), bf16[8,96,128]{2,1,0:T(8,128)(2,1)S(1)}, u32[]{:S(2)}, u32[]{:S(2)}) %all-to-all-start.5) | async-done | bytes 196640 | tf_op jit(solution)/shard_map/all_to_all | solution.py:35
  158.4 0.6 add_convert_fusion
  (35 shorter events, 0.4 us)
Async XLA Ops:
  2.9 43.8 %copy-start.7 = (s32[96,2]{0,1:T(2,128)S(1)}, s32[96,2]{0,1:T(2,128)}, u32[]{:S(2)}) copy-start(s32[96,2]{0,1:T(2,128)} %param.37) | copy-start | bytes 2308
  2.9 60.0 %all-to-all-start = ((bf16[16,8,768]{2,1,0:T(8,128)(2,1)}), bf16[16,8,768]{2,1,0:T(8,128)(2,1)S(1)}, u32[]{:S(2)}, u32[]{:S(2)}) async-start(bf16[16,8,768]{2,1,0:T(8,128)(2,1)} %get-tuple-element.23), calls=%async_computation | async-start | bytes 393216 | tf_op jit(solution)/shard_map/all_to_all | solution.py:21
  46.9 0.7 copy-start.8
  48.2 14.7 %copy-start = (f32[6,1,128,256]{3,2,1,0:T(8,128)S(1)}, f32[6,1,128,256]{3,2,1,0:T(8,128)}, u32[]{:S(2)}) copy-start(f32[6,1,128,256]{3,2,1,0:T(8,128)} %cell_ref.1) | copy-start | bytes 2359300
  48.5 14.5 %copy-start.4 = (f32[4096]{0:T(1024)S(1)}, f32[4096]{0:T(1024)}, u32[]{:S(2)}) copy-start(f32[4096]{0:T(1024)} %param.31) | copy-start | bytes 49156
  48.5 14.4 %copy-start.6 = (f32[6,1,128]{2,1,0:T(1,128)S(1)}, f32[6,1,128]{2,1,0:T(1,128)}, u32[]{:S(2)}) copy-start(f32[6,1,128]{2,1,0:T(1,128)} %norm_ref.1) | copy-start | bytes 9220
  63.0 58.0 %copy-start.1 = (bf16[1,2048,256]{2,1,0:T(8,128)(2,1)S(1)}, bf16[1,2048,256]{2,1,0:T(8,128)(2,1)}, u32[]{:S(2)}) copy-start(bf16[1,2048,256]{2,1,0:T(8,128)(2,1)} %gate_ref.1) | copy-start | bytes 3145732
  64.6 17.7 %copy-start.3 = (bf16[256,128]{1,0:T(8,128)(2,1)S(1)}, bf16[256,128]{1,0:T(8,128)(2,1)}, u32[]{:S(2)}) copy-start(bf16[256,128]{1,0:T(8,128)(2,1)} %weight_ref.1) | copy-start | bytes 196612
  82.6 3.1 %collective-permute-start = (bf16[96,128]{1,0:T(8,128)(2,1)S(1)}, bf16[96,128]{1,0:T(8,128)(2,1)S(1)}, u32[]{:S(2)}, u32[]{:S(2)}) collective-permute-start(bf16[96,128]{1,0:T(8,128)(2,1)S(1)} %project_heads.1.own_ref), channel_id=1, source_target_pairs={{0,1},{1,0},{2,3},{3,2},{4,5},{5,4},{6,7},{7,6},{8,9},{9,8},{10,11... | collective-permute-start | bytes 73736 | tf_op jit(solution)/shard_map/ppermute | solution.py:26
  85.8 17.9 %copy-start.2 = (bf16[96,128]{1,0:T(8,128)(2,1)S(1)}, bf16[96,128]{1,0:T(8,128)(2,1)}, u32[]{:S(2)}) copy-start(bf16[96,128]{1,0:T(8,128)(2,1)} %tok_ref.3) | copy-start | bytes 73732
  103.9 17.0 %copy-start.5 = (f32[2048]{0:T(1024)S(1)}, f32[2048]{0:T(1024)}, u32[]{:S(2)}) copy-start(f32[2048]{0:T(1024)} %param.36) | copy-start | bytes 24580
  139.4 3.1 %collective-permute-start.1 = (bf16[96,128]{1,0:T(8,128)(2,1)S(1)}, bf16[96,128]{1,0:T(8,128)(2,1)S(1)}, u32[]{:S(2)}, u32[]{:S(2)}) collective-permute-start(bf16[96,128]{1,0:T(8,128)(2,1)S(1)} %combine.1.own_ref), channel_id=1, source_target_pairs={{0,1},{1,0},{2,3},{3,2},{4,5},{5,4},{6,7},{7,6},{8,9},{9,8},{10,11... | collective-permute-start | bytes 73736 | tf_op jit(solution)/shard_map/ppermute | solution.py:26
  143.2 15.2 %all-to-all-start.5 = ((bf16[8,96,128]{2,1,0:T(8,128)(2,1)}), bf16[8,96,128]{2,1,0:T(8,128)(2,1)S(1)}, u32[]{:S(2)}, u32[]{:S(2)}) async-start(bf16[8,96,128]{2,1,0:T(8,128)(2,1)} %chip_moe.1), calls=%async_computation.5 | async-start | bytes 393216 | tf_op jit(solution)/shard_map/all_to_all | solution.py:35

commit v6 on v5

--- a/solution.py
+++ b/solution.py
@@ -37,16 +37,6 @@
     )
 
 
-def in_pieces(values, count):
-    pieces = []
-    for _ in range(count - 1):
-        head = lax.reduce_precision(values, 8, 7)
-        pieces.append(head)
-        values = values - head
-    pieces.append(values)
-    return pieces
-
-
 def rounded_pieces(values, count):
     pieces = []
     for _ in range(count):
@@ -60,6 +50,11 @@
     return jnp.dot(a, b, preferred_element_type=F32)
 
 
+def lane_sums(values, count):
+    ones = jnp.ones((values.shape[1], LANES), BF16)
+    return sum(dot(piece.astype(BF16), ones) for piece in rounded_pieces(values, count))
+
+
 def grid_index(shape):
     return lax.broadcasted_iota(jnp.int32, shape, 0), lax.broadcasted_iota(jnp.int32, shape, 1)
 
@@ -68,10 +63,11 @@
     return jnp.where(condition, 1.0, 0.0).astype(BF16)
 
 
-def send_kernel(
-    tok_ref, gain_ref, wq, wk, wv, wo, wi, wf, max_ref, out_ref, max_out, *, seq_local
-):
-    max_out[...] = max_ref[...]
+def send_kernel(tok_ref, gain_ref, wq, wk, wv, wo, wi, wf, *rest, seq_local):
+    handed = len(rest) // 2
+    out_ref = rest[handed]
+    for kept, copy in zip(rest[:handed], rest[handed + 1 :]):
+        copy[...] = kept[...]
     head = lax.axis_index("tp")
     seq_total, columns = tok_ref.shape
     ours = pl.ds(pl.multiple_of(lax.axis_index("ep") * columns, LANES), columns)
@@ -85,32 +81,34 @@
     slot = lax.broadcasted_iota(jnp.int32, (count, columns), 0) & (PADDED - 1)
     values = dot(spread_rows, tok_ref[...])
     values = jnp.where(slot == seq_local, 1.0, values)
-    own = slot[:, :1] < seq_local
-    block_mean = jnp.where(own, jnp.sum(values, axis=1, keepdims=True) * (1.0 / columns), 0.0)
+    own = slot < seq_local
+    block_mean = jnp.where(own, lane_sums(values, 1) * (1.0 / columns), 0.0)
     offsets = values - block_mean
-    moment = jnp.where(own, jnp.sum(offsets * offsets, axis=1, keepdims=True), 0.0)
+    moment = jnp.where(own, lane_sums(offsets * offsets, 2), 0.0)
     gain_row = gain_ref[:, ours]
     down, across = grid_index((columns, columns))
-    gain_col = jnp.sum(jnp.where(down == across, gain_row, 0.0), axis=1, keepdims=True)
+    gain_col = lane_sums(jnp.where(down == across, gain_row, 0.0), 3)
     exact = jnp.concatenate([values.astype(BF16)] * 2, axis=1)
     parts = []
     for ref in (wq, wk, wv, wo):
-        pieces = rounded_pieces(ref[...].astype(F32) * gain_col, 2)
+        spread_gain = jnp.concatenate([gain_col] * (ref.shape[1] // LANES), axis=1)
+        pieces = rounded_pieces(ref[...].astype(F32) * spread_gain, 2)
         parts.append(dot(exact, jnp.concatenate([p.astype(BF16) for p in pieces], axis=0)))
     product = jnp.concatenate(parts, axis=1)
     tiles = product.reshape(blocks, PADDED, product.shape[1])
     sums = tiles[:, seq_local : seq_local + 1, :]
-    centred = tiles - block_mean.reshape(blocks, PADDED, 1) * sums
+    wide_mean = jnp.concatenate([block_mean] * (product.shape[1] // LANES), axis=1)
+    centred = tiles - wide_mean.reshape(tiles.shape) * sums
 
     pick, _ = grid_index((wi.shape[0], columns))
 
     def gate_part(ref):
         chosen = jnp.sum(jnp.where(pick == head, ref[:, ours].astype(F32), 0.0), axis=0, keepdims=True)
-        return jnp.sum(offsets * (chosen * gain_row), axis=1, keepdims=True)
+        return lane_sums(offsets * (chosen * gain_row), 3)
 
     gates = [*rounded_pieces(gate_part(wi), 2), *rounded_pieces(gate_part(wf), 2)]
     lane = lax.broadcasted_iota(jnp.int32, (count, LANES), 1)
-    start = jnp.where(slot[:, :1] == seq_local, GATE_SUMS, 0)
+    start = jnp.where(slot == seq_local, GATE_SUMS, 0)
     table = jnp.zeros((count, LANES), F32)
     for k, piece in enumerate(gates):
         table = jnp.where(lane == start + k, piece, table)
@@ -133,9 +131,11 @@
 
 
 def receive_kernel(
-    in_bias, for_bias, got_ref, cell_ref, norm_ref, max_ref, gain_ref,
-    mixed_ref, keep_ref, admit_ref, value_ref, norm_out, max_out, *, columns
+    in_bias, for_bias, cell_hbm, got_ref, norm_ref, max_ref, gain_ref,
+    mixed_ref, keep_ref, admit_ref, value_ref, norm_out, max_out, cell_ref, arrived, *, columns
 ):
+    fetch = pltpu.make_async_copy(cell_hbm, cell_ref, arrived)
+    fetch.start()
     head = lax.axis_index("tp")
     blocks, padded, width = got_ref.shape
     seq_local, _, key_size, value_size = cell_ref.shape
@@ -154,18 +154,24 @@
         jnp.concatenate([flat[:, r * LANES : (r + 1) * LANES] for r in range(seq_local)], axis=0),
     )
     sums = got[:, seq_local : seq_local + 1, :]
-    lane = lax.broadcasted_iota(jnp.int32, (count, LANES), 1)
-
-    def lanes(first, number):
-        kept = jnp.where((lane >= first) & (lane < first + number), table, 0.0)
-        return jnp.sum(kept, axis=1, keepdims=True).reshape(blocks, padded, 1)
-
-    means = lanes(4, 3)
+    lane, _ = grid_index((LANES, LANES))
+    spans = ((4, 3), (7, 2), (0, 2), (GATE_SUMS, 2), (2, 2), (GATE_SUMS + 2, 2))
+    chosen = [one_hot((lane >= first) & (lane < first + number)) for first, number in spans]
+    gathered = dot(table.astype(BF16), jnp.concatenate(chosen, axis=1))
+
+    def term(k):
+        return gathered[:, k * LANES : (k + 1) * LANES].reshape(blocks, padded, LANES)
+
+    means = term(0)
     row_mean = jnp.sum(means, axis=0, keepdims=True) * (1.0 / blocks)
     shifts = means - row_mean
-    spread = jnp.sum(lanes(7, 2) + columns * shifts * shifts, axis=0) * (1.0 / (blocks * columns))
+    spread = jnp.sum(term(1) + columns * shifts * shifts, axis=0) * (1.0 / (blocks * columns))
     inv_scale = lax.rsqrt(spread + NORM_EPS)
-    projected = inv_scale * jnp.sum(got + shifts * sums, axis=0)
+    parts = width // LANES
+    wide_shifts = jnp.concatenate([shifts] * parts, axis=2)
+    projected = jnp.concatenate([inv_scale] * parts, axis=1) * jnp.sum(
+        got + wide_shifts * sums, axis=0
+    )
 
     def rounded(a, b):
         return projected[:, a:b].astype(BF16).astype(F32)
@@ -175,10 +181,10 @@
     value = rounded(2 * key_size, 2 * key_size + value_size)
     outgate = rounded(2 * key_size + value_size, width)
     input_pre = (
-        inv_scale * jnp.sum(lanes(0, 2) + shifts * lanes(GATE_SUMS, 2), axis=0) + in_bias[head]
+        inv_scale * jnp.sum(term(2) + shifts * term(3), axis=0) + in_bias[head]
     )
     forget_pre = (
-        inv_scale * jnp.sum(lanes(2, 2) + shifts * lanes(GATE_SUMS + 2, 2), axis=0)
+        inv_scale * jnp.sum(term(4) + shifts * term(5), axis=0)
         + for_bias[head]
     )
     down, across = grid_index((padded, seq_local))
@@ -188,19 +194,21 @@
     new_max = jnp.maximum(carried, input_pre)
     keep_old = jnp.exp(carried - new_max)
     admit_key = jnp.exp(input_pre - new_max) * key
-    max_out[...] = new_max[:seq_local]
-    keep_ref[...] = keep_old[:seq_local]
+    max_out[...] = new_max[:seq_local, :1]
+    keep_ref[...] = keep_old[:seq_local, :1]
     admit_ref[...] = admit_key[:seq_local]
     value_ref[...] = value[:seq_local]
     query_cols = query.T
     rows = lax.broadcasted_iota(jnp.int32, (padded, value_size), 0)
     against_cell = jnp.zeros((padded, value_size), F32)
+    fetch.wait()
     for s in range(seq_local):
         norm_out[s : s + 1] = keep_old[s : s + 1] * norm_ref[s] + admit_key[s : s + 1]
         read = jnp.sum(query_cols[:, s : s + 1] * cell_ref[s, 0], axis=0, keepdims=True)
         against_cell = jnp.where(rows == s, read, against_cell)
     scores = jnp.sum(query * admit_key, axis=1, keepdims=True)
-    readout = jnp.where(rows < seq_local, keep_old * against_cell + scores * value, 0.0)
+    wide_keep = jnp.concatenate([keep_old] * (value_size // LANES), axis=1)
+    readout = jnp.where(rows < seq_local, wide_keep * against_cell + scores * value, 0.0)
     outgate = jnp.where(rows < seq_local, outgate, 0.0)
     head_mean = jnp.mean(readout, axis=1, keepdims=True)
     around = readout - head_mean
@@ -227,12 +235,38 @@
     out_ref[...] = jnp.broadcast_to(added[None], out_ref.shape)
 
 
-def stream_kernel(got_ref, tok_ref, picker_ref, stream_ref, out_ref):
+def column_of(row):
+    down, across = grid_index((row.shape[1], row.shape[1]))
+    return jnp.sum(jnp.where(down == across, row, 0.0), axis=1, keepdims=True)
+
+
+def stream_kernel(
+    got_ref, tok_ref, route_ref, weight_ref, stream_ref, out_ref, table_ref, *, seq_local
+):
     mixer_out = jnp.sum(got_ref[...].astype(F32), axis=0)
     stream = (tok_ref[...].astype(F32) + mixer_out).astype(BF16)
     stream_ref[...] = stream
+    top, seq_total = route_ref.shape
+    experts, slots, _ = out_ref.shape
+    names = [route_ref[k : k + 1].astype(F32) for k in range(top)]
+    down, across = grid_index((seq_total, seq_total))
+    block_down = jnp.floor((down.astype(F32) + 0.5) * (1.0 / seq_local))
+    block_across = jnp.floor((across.astype(F32) + 0.5) * (1.0 / seq_local))
+    earlier = (block_down == block_across) & (across < down)
+    place = lax.broadcasted_iota(jnp.int32, (seq_total, experts * slots), 1).astype(F32)
+    picked = jnp.zeros(place.shape, F32)
+    weights = jnp.zeros(place.shape, F32)
+    for k in range(top):
+        name = column_of(names[k])
+        same = sum(jnp.where(earlier & (other == name), 1.0, 0.0) for other in names)
+        slot = name * slots + block_down[:, :1] * CAPACITY + jnp.sum(same, axis=1, keepdims=True)
+        here = place == slot
+        picked = jnp.where(here, 1.0, picked)
+        weights = jnp.where(here, column_of(weight_ref[k : k + 1]), weights)
+    table = [piece.astype(BF16) for piece in rounded_pieces(weights, 2)]
+    table_ref[...] = jnp.concatenate(table, axis=0)
     chosen = lax.dot_general(
-        picker_ref[...], stream, (((0,), (0,)), ((), ())), preferred_element_type=F32
+        picked.astype(BF16), stream, (((0,), (0,)), ((), ())), preferred_element_type=F32
     )
     out_ref[...] = chosen.astype(BF16).reshape(out_ref.shape)
 
@@ -315,26 +349,16 @@
     value_size = cell_state.shape[3]
     experts = blocks
     slot_count = blocks * CAPACITY
-    expert_ids = lax.broadcasted_iota(jnp.int32, (1, 1, experts), 2)
-    matches = routes[:, :, None] == expert_ids
-    routed = jnp.sum(matches.astype(jnp.int32), axis=1)
-    combine = jnp.sum(jnp.where(matches, route_weight[:, :, None], 0.0), axis=1)
-    running = (
-        jnp.cumsum(routed.reshape(blocks, seq_local, experts), axis=1).reshape(seq_total, experts)
-        - routed
-    )
-    block_ids = lax.broadcasted_iota(jnp.int32, (seq_total, experts), 0) // seq_local
-    slot_of = block_ids * CAPACITY + running
-    slot_ids = lax.broadcasted_iota(jnp.int32, (experts, slot_count, seq_total), 1)
-    placed = (slot_of.T[:, None, :] == slot_ids) & (routed.T[:, None, :] > 0)
-    picker = placed.astype(BF16).reshape(experts * slot_count, seq_total).T
-    weighted = jnp.where(placed, combine.T[:, None, :], 0.0)
 
     width = 2 * (w_query.shape[1] + w_value.shape[1])
-    outgoing, old_max = kernel_call(
+    handed = (max_state.T, norm_state, head_gain.reshape(1, -1), routes.T, route_weight.T)
+    outgoing, old_max, old_norm, gains, route_rows, weight_rows = kernel_call(
         functools.partial(send_kernel, seq_local=seq_local),
         "send_parts",
-        [pltpu.VMEM((blocks, PADDED, width), BF16), pltpu.VMEM((1, seq_local), F32)],
+        [
+            pltpu.VMEM((blocks, PADDED, width), BF16),
+            *(pltpu.VMEM(a.shape, a.dtype) for a in handed),
+        ],
         (),
         far=(
             tokens,
@@ -345,12 +369,10 @@
             w_outgate,
             w_input.T,
             w_forget.T,
-            max_state.T,
+            *handed,
         ),
     )
-    weight_rows = weighted.reshape(experts * slot_count, seq_total).T
-    table = jnp.concatenate([t.astype(BF16) for t in in_pieces(weight_rows, 2)], axis=0)
-    incoming, picker, table = lax.optimization_barrier((exchanged(outgoing, "ep"), picker, table))
+    incoming = exchanged(outgoing, "ep")
 
     key_size = cell_state.shape[2]
     mixed, *updates = kernel_call(
@@ -364,8 +386,10 @@
             pltpu.VMEM((seq_local, key_size), F32),
             pltpu.VMEM((seq_local, 1), F32),
         ],
-        (incoming, cell_state, norm_state, old_max, head_gain.reshape(1, -1)),
+        (incoming, old_norm, old_max, gains),
         scalars=(input_bias, forget_bias),
+        left=(cell_state,),
+        scratch=(pltpu.VMEM(cell_state.shape, F32), pltpu.SemaphoreType.DMA),
     )
 
     part_shape = pltpu.VMEM((seq_total, columns), BF16)
@@ -379,14 +403,15 @@
     chip_terms = kernel_call(
         pair_kernel, "chip_heads", chip_shape, (head_terms, from_other_core(head_terms))
     )
-    stream, outbound = kernel_call(
-        stream_kernel,
+    stream, outbound, table = kernel_call(
+        functools.partial(stream_kernel, seq_local=seq_local),
         "stream_rows",
         [
             pltpu.VMEM(tokens.shape, BF16),
             pltpu.VMEM((experts, slot_count, columns), BF16),
+            pltpu.VMEM((2 * seq_total, experts * slot_count), BF16),
         ],
-        (swapped(chip_terms, chips_of_cores("tp")), tokens, picker),
+        (swapped(chip_terms, chips_of_cores("tp")), tokens, route_rows, weight_rows),
     )
 
     slot_out = kernel_call(

time: 160 us -> 160 us (level)
  blocking collectives: 68.9 us -> 129 us
  starting transfers between devices: 52.1 us -> 8.26 us
  waiting for transfers between devices: 25.2 us -> 10.8 us
    all_to_all x3 -> x4, blocking collectives: 51 us -> 111 us  [exchanged(): return lax.all_to_all(blocks, axis, split_axis=0, concat_axis=0, tiled=True)]
    all_to_all x1 -> x0, starting transfers between devices: 43.8 us -> none  [exchanged(): return lax.all_to_all(blocks, axis, split_axis=0, concat_axis=0, tiled=True)]
    all_to_all x1 -> x0, waiting for transfers between devices: 14.4 us -> none  [exchanged(): return lax.all_to_all(blocks, axis, split_axis=0, concat_axis=0, tiled=True)]
  transfers between devices with their start and end apart: 4 -> 3, of which waited for: 4 -> 3; matrix products, arithmetic and copies ran while one was open for 2% -> 1% of each run, Pallas kernels for 0% -> 0%
where the time goes in v6:
time: 160 us
  blocking collectives  129 us (81%)
  waiting for transfers between devices  10.8 us (7%)
  starting transfers between devices  8.26 us (5%)
  Pallas kernels  8.19 us (5%)
  other arithmetic  1.82 us (1%)
    all_to_all x4, blocking collectives, exchanged(): return lax.all_to_all(blocks, axis, split_axis=0, concat_axis=0, tiled=True)  111 us
    all_to_all x1, blocking collectives, swapped(): lax.all_to_all(blocks, 'tp', split_axis=0, concat_axis=0, tiled=True, axi...  17.9 us
    all_to_all x1, waiting for transfers between devices, swapped(): lax.all_to_all(blocks, 'tp', split_axis=0, concat_axis=0, tiled=True, axi...  8.44 us
    pallas_call x8, Pallas kernels, kernel_call(): pl.pallas_call(kernel, in_specs=[smem] * len(scalars) + [pl.BlockSpec(mem...  8.19 us
    all_to_all x1, starting transfers between devices, swapped(): lax.all_to_all(blocks, 'tp', split_axis=0, concat_axis=0, tiled=True, axi...  4.36 us
    ppermute x2, starting transfers between devices, from_other_core(): return lax.ppermute(array, 'tp', [(i, i ^ 1) for i in range(size)])  3.9 us
  transfers between devices with their start and end apart: 3, of which 3 were waited for; matrix products, arithmetic and copies ran while one was open for 1% of the time, Pallas kernels for 0%

profile of v6, /device:TPU:80, one launch (start us, length us, event | category | flops | bytes accessed | tf_op | source)
XLA Modules:
  0.0 159.7 jit_solution(11220110898209654021)
XLA Ops:
  0.6 1.9 %send_parts.1 = (bf16[16,8,768]{2,1,0:T(8,128)(2,1)S(1)}, f32[1,6]{1,0:T(1,128)S(1)}, f32[6,1,128]{2,1,0:T(1,128)S(1)}, f32[1,4096]{1,0:T(1,128)S(1)}, s32[2,96]{1,0:T(2,128)S(1)}, /*index=5*/f32[2,96]{1,0:T(2,128)S(1)}) custom-call(bf16[96,128]{1,0:T(8,128)(2,1)} %tok_ref.3, f32[1,2048]{1,0:T(1,128)} %bitcast.14, bf16[128,128]{1,0:T(8,128)(2,1)} %wq.1, ...), custom_call_target="tpu_custom_call" | custom-call | tf_op jit(solution)/shard_map/send_parts/pallas_call | solution.py:311
  2.5 59.7 %all_to_all.30.got_ref = bf16[16,8,768]{2,1,0:T(8,128)(2,1)S(1)} all-to-all(bf16[16,8,768]{2,1,0:T(8,128)(2,1)S(1)} %get-tuple-element.25), channel_id=1, replica_groups=mesh['grp'=2,'ep'=16,'tp'=16] {'ep'}, dimensions={0} | all-to-all | bytes 393216 | tf_op jit(solution)/shard_map/all_to_all | solution.py:21
  62.2 2.8 %cell_step.1 = (bf16[16,8,256]{2,1,0:T(8,128)(2,1)S(1)}, f32[6,1]{1,0:T(8,128)S(1)}, f32[6,128]{1,0:T(8,128)S(1)}, f32[6,256]{1,0:T(8,128)S(1)}, f32[6,128]{1,0:T(8,128)S(1)}, /*index=5*/f32[6,1]{1,0:T(8,128)S(1)}) custom-call(f32[16]{0:T(128)} %in_bias.1, f32[16]{0:T(128)} %for_bias.1, f32[6,1,128,256]{3,2,1,0:T(8,128)} %cell_hbm.1, ...), custom_call_target="tpu_custom_call" | custom-call | tf_op jit(solution)/shard_map/cell_step/pallas_call | solution.py:311
  65.0 0.0 copy-start.2
  65.0 17.7 %all_to_all.31.got_ref = bf16[16,8,256]{2,1,0:T(8,128)(2,1)S(1)} all-to-all(bf16[16,8,256]{2,1,0:T(8,128)(2,1)S(1)} %get-tuple-element.29), channel_id=1, replica_groups=mesh['grp'=2,'ep'=16,'tp'=16] {'ep'}, dimensions={0} | all-to-all | bytes 131072 | tf_op jit(solution)/shard_map/all_to_all | solution.py:21
  82.7 0.0 copy-done.2
  82.7 0.3 project_heads.1.own_ref
  83.0 2.0 %collective-permute-start = (bf16[96,128]{1,0:T(8,128)(2,1)S(1)}, bf16[96,128]{1,0:T(8,128)(2,1)S(1)}, u32[]{:S(2)}, u32[]{:S(2)}) collective-permute-start(bf16[96,128]{1,0:T(8,128)(2,1)S(1)} %project_heads.1.own_ref), channel_id=1, source_target_pairs={{0,1},{1,0},{2,3},{3,2},{4,5},{5,4},{6,7},{7,6},{8,9},{9,8},{10,11... | collective-permute-start | bytes 73736 | tf_op jit(solution)/shard_map/ppermute | solution.py:26
  85.0 1.2 collective-permute-done.other_ref
  86.2 0.0 copy-start.1
  86.2 17.9 %all_to_all.32.got_ref = bf16[8,96,128]{2,1,0:T(8,128)(2,1)S(1)} all-to-all(bf16[8,96,128]{2,1,0:T(8,128)(2,1)S(1)} %chip_heads.1), channel_id=1, replica_groups={{0,2,4,6,8,10,12,14},{1,3,5,7,9,11,13,15},{16,18,20,22,24,26,28,30},{17..., dimensions={0} | all-to-all | bytes 393216 | tf_op jit(solution)/shard_map/all_to_all | solution.py:35
  104.1 0.0 copy-done.1
  104.1 0.4 stream_rows.1
  104.5 0.0 copy-start.3
  104.5 17.0 %all_to_all.33.got_ref = bf16[16,32,128]{2,1,0:T(8,128)(2,1)S(1)} all-to-all(bf16[16,32,128]{2,1,0:T(8,128)(2,1)S(1)} %get-tuple-element.34), channel_id=1, replica_groups=mesh['grp'=2,'ep'=16,'tp'=16] {'ep'}, dimensions={0} | all-to-all | bytes 262144 | tf_op jit(solution)/shard_map/all_to_all | solution.py:21
  121.5 0.0 copy-done
  121.5 0.0 copy-done.3
  121.5 1.9 %expert.1 = bf16[16,32,128]{2,1,0:T(8,128)(2,1)S(1)} custom-call(bf16[1,2048,256]{2,1,0:T(8,128)(2,1)} %up_hbm.1, bf16[1,256,2048]{2,1,0:T(8,128)(2,1)} %down_hbm.1, bf16[16,32,128]{2,1,0:T(8,128)(2,1)S(1)} %all_to_all.33.got_ref, f32[1,2048]{1,0:T(1,128)S(1)} %bitcast.9, bf16[1,2048,256]{2,1,0:T(8,128)(2,1)S(1)} %copy-done), custom_call_target="tpu_custom_call" | custom-call | tf_op jit(solution)/shard_map/expert/pallas_call | solution.py:311
  123.5 0.0 copy-start.4
  123.5 16.5 %all_to_all.34.back_ref = bf16[16,32,128]{2,1,0:T(8,128)(2,1)S(1)} all-to-all(bf16[16,32,128]{2,1,0:T(8,128)(2,1)S(1)} %expert.1), channel_id=1, replica_groups=mesh['grp'=2,'ep'=16,'tp'=16] {'ep'}, dimensions={0} | all-to-all | bytes 262144 | tf_op jit(solution)/shard_map/all_to_all | solution.py:21
  139.9 0.2 combine.1.own_ref
  140.1 2.0 %collective-permute-start.1 = (bf16[96,128]{1,0:T(8,128)(2,1)S(1)}, bf16[96,128]{1,0:T(8,128)(2,1)S(1)}, u32[]{:S(2)}, u32[]{:S(2)}) collective-permute-start(bf16[96,128]{1,0:T(8,128)(2,1)S(1)} %combine.1.own_ref), channel_id=1, source_target_pairs={{0,1},{1,0},{2,3},{3,2},{4,5},{5,4},{6,7},{7,6},{8,9},{9,8},{10,11... | collective-permute-start | bytes 73736 | tf_op jit(solution)/shard_map/ppermute | solution.py:26
  142.1 1.2 collective-permute-done.1.other_ref
  143.2 0.7 chip_moe.1
  143.9 4.4 %all-to-all-start.5 = ((bf16[8,96,128]{2,1,0:T(8,128)(2,1)}), bf16[8,96,128]{2,1,0:T(8,128)(2,1)S(1)}, u32[]{:S(2)}, u32[]{:S(2)}) async-start(bf16[8,96,128]{2,1,0:T(8,128)(2,1)} %chip_moe.1), calls=%async_computation.5 | async-start | bytes 393216 | tf_op jit(solution)/shard_map/all_to_all | solution.py:35
  148.3 0.6 copy.28
  148.9 0.6 copy.27
  149.5 0.1 reduce
  149.6 0.0 copy-done.4
  149.6 1.1 multiply_add_fusion
  150.6 8.4 %all-to-all-done.5 = bf16[8,96,128]{2,1,0:T(8,128)(2,1)S(1)} async-done(((bf16[8,96,128]{2,1,0:T(8,128)(2,1)}), bf16[8,96,128]{2,1,0:T(8,128)(2,1)S(1)}, u32[]{:S(2)}, u32[]{:S(2)}) %all-to-all-start.5) | async-done | bytes 196640 | tf_op jit(solution)/shard_map/all_to_all | solution.py:35
  159.1 0.6 add_convert_fusion
  (3 shorter events, 0.0 us)
Async XLA Ops:
  62.2 59.3 %copy-start = (bf16[1,2048,256]{2,1,0:T(8,128)(2,1)S(1)}, bf16[1,2048,256]{2,1,0:T(8,128)(2,1)}, u32[]{:S(2)}) copy-start(bf16[1,2048,256]{2,1,0:T(8,128)(2,1)} %gate_ref.1) | copy-start | bytes 3145732
  65.0 17.7 %copy-start.2 = (bf16[256,128]{1,0:T(8,128)(2,1)S(1)}, bf16[256,128]{1,0:T(8,128)(2,1)}, u32[]{:S(2)}) copy-start(bf16[256,128]{1,0:T(8,128)(2,1)} %weight_ref.1) | copy-start | bytes 196612
  83.0 3.1 %collective-permute-start = (bf16[96,128]{1,0:T(8,128)(2,1)S(1)}, bf16[96,128]{1,0:T(8,128)(2,1)S(1)}, u32[]{:S(2)}, u32[]{:S(2)}) collective-permute-start(bf16[96,128]{1,0:T(8,128)(2,1)S(1)} %project_heads.1.own_ref), channel_id=1, source_target_pairs={{0,1},{1,0},{2,3},{3,2},{4,5},{5,4},{6,7},{7,6},{8,9},{9,8},{10,11... | collective-permute-start | bytes 73736 | tf_op jit(solution)/shard_map/ppermute | solution.py:26
  86.2 17.9 %copy-start.1 = (bf16[96,128]{1,0:T(8,128)(2,1)S(1)}, bf16[96,128]{1,0:T(8,128)(2,1)}, u32[]{:S(2)}) copy-start(bf16[96,128]{1,0:T(8,128)(2,1)} %tok_ref.3) | copy-start | bytes 73732
  104.5 17.0 %copy-start.3 = (f32[2048]{0:T(1024)S(1)}, f32[2048]{0:T(1024)}, u32[]{:S(2)}) copy-start(f32[2048]{0:T(1024)} %param.36) | copy-start | bytes 24580
  123.5 26.1 %copy-start.4 = (f32[6,1,128,256]{3,2,1,0:T(8,128)S(1)}, f32[6,1,128,256]{3,2,1,0:T(8,128)}, u32[]{:S(2)}) copy-start(f32[6,1,128,256]{3,2,1,0:T(8,128)} %cell_hbm.1) | copy-start | bytes 2359300
  140.1 3.1 %collective-permute-start.1 = (bf16[96,128]{1,0:T(8,128)(2,1)S(1)}, bf16[96,128]{1,0:T(8,128)(2,1)S(1)}, u32[]{:S(2)}, u32[]{:S(2)}) collective-permute-start(bf16[96,128]{1,0:T(8,128)(2,1)S(1)} %combine.1.own_ref), channel_id=1, source_target_pairs={{0,1},{1,0},{2,3},{3,2},{4,5},{5,4},{6,7},{7,6},{8,9},{9,8},{10,11... | collective-permute-start | bytes 73736 | tf_op jit(solution)/shard_map/ppermute | solution.py:26
  143.9 15.2 %all-to-all-start.5 = ((bf16[8,96,128]{2,1,0:T(8,128)(2,1)}), bf16[8,96,128]{2,1,0:T(8,128)(2,1)S(1)}, u32[]{:S(2)}, u32[]{:S(2)}) async-start(bf16[8,96,128]{2,1,0:T(8,128)(2,1)} %chip_moe.1), calls=%async_computation.5 | async-start | bytes 393216 | tf_op jit(solution)/shard_map/all_to_all | solution.py:35

commit v7 on v6

--- a/solution.py
+++ b/solution.py
@@ -63,7 +63,10 @@
     return jnp.where(condition, 1.0, 0.0).astype(BF16)
 
 
-def send_kernel(tok_ref, gain_ref, wq, wk, wv, wo, wi, wf, *rest, seq_local):
+def send_kernel(cell_hbm, tok_ref, gain_ref, wq, wk, wv, wo, wi, wf, *rest, seq_local):
+    *rest, cell_ref, arrived = rest
+    fetch = pltpu.make_async_copy(cell_hbm, cell_ref, arrived)
+    fetch.start()
     handed = len(rest) // 2
     out_ref = rest[handed]
     for kept, copy in zip(rest[:handed], rest[handed + 1 :]):
@@ -128,14 +131,13 @@
         [laid[r * count : (r + 1) * count] for r in range(seq_local)], axis=1
     ).reshape(tiles.shape)
     out_ref[...] = (centred + side).astype(BF16)
+    fetch.wait()
 
 
 def receive_kernel(
-    in_bias, for_bias, cell_hbm, got_ref, norm_ref, max_ref, gain_ref,
-    mixed_ref, keep_ref, admit_ref, value_ref, norm_out, max_out, cell_ref, arrived, *, columns
+    in_bias, for_bias, got_ref, cell_ref, norm_ref, max_ref, gain_ref,
+    mixed_ref, keep_ref, admit_ref, value_ref, norm_out, max_out, *, columns
 ):
-    fetch = pltpu.make_async_copy(cell_hbm, cell_ref, arrived)
-    fetch.start()
     head = lax.axis_index("tp")
     blocks, padded, width = got_ref.shape
     seq_local, _, key_size, value_size = cell_ref.shape
@@ -201,7 +203,6 @@
     query_cols = query.T
     rows = lax.broadcasted_iota(jnp.int32, (padded, value_size), 0)
     against_cell = jnp.zeros((padded, value_size), F32)
-    fetch.wait()
     for s in range(seq_local):
         norm_out[s : s + 1] = keep_old[s : s + 1] * norm_ref[s] + admit_key[s : s + 1]
         read = jnp.sum(query_cols[:, s : s + 1] * cell_ref[s, 0], axis=0, keepdims=True)
@@ -272,23 +273,18 @@
 
 
 def expert_kernel(
-    up_hbm, down_hbm, got_ref, gain_ref, gate_ref, out_ref, up_ref, down_ref, arrived
+    down_hbm, got_ref, gain_ref, gate_ref, up_ref, out_ref, down_ref, arrived
 ):
-    fetches = [
-        pltpu.make_async_copy(up_hbm, up_ref, arrived.at[0]),
-        pltpu.make_async_copy(down_hbm, down_ref, arrived.at[1]),
-    ]
-    for fetch in fetches:
-        fetch.start()
+    fetch = pltpu.make_async_copy(down_hbm, down_ref, arrived)
+    fetch.start()
     blocks, _, columns = got_ref.shape
     values = jnp.concatenate([got_ref[e].astype(F32) for e in range(blocks)], axis=1)
     row_mean = jnp.mean(values, axis=1, keepdims=True)
     spread = jnp.mean(values * values, axis=1, keepdims=True) - row_mean * row_mean
     normed = ((values - row_mean) * lax.rsqrt(spread + NORM_EPS) * gain_ref[...]).astype(BF16)
     gate = dot(normed, gate_ref[0])
-    fetches[0].wait()
     active = (gate / (1.0 + jnp.exp(-gate)) * dot(normed, up_ref[0])).astype(BF16)
-    fetches[1].wait()
+    fetch.wait()
     result = dot(active, down_ref[0]).astype(BF16)
     for e in range(blocks):
         out_ref[e] = result[:, e * columns : (e + 1) * columns]
@@ -352,12 +348,12 @@
 
     width = 2 * (w_query.shape[1] + w_value.shape[1])
     handed = (max_state.T, norm_state, head_gain.reshape(1, -1), routes.T, route_weight.T)
-    outgoing, old_max, old_norm, gains, route_rows, weight_rows = kernel_call(
+    outgoing, old_max, old_norm, gains, route_rows, weight_rows, old_cell = kernel_call(
         functools.partial(send_kernel, seq_local=seq_local),
         "send_parts",
         [
             pltpu.VMEM((blocks, PADDED, width), BF16),
-            *(pltpu.VMEM(a.shape, a.dtype) for a in handed),
+            *(pltpu.VMEM(a.shape, a.dtype) for a in (*handed, cell_state)),
         ],
         (),
         far=(
@@ -371,6 +367,8 @@
             w_forget.T,
             *handed,
         ),
+        left=(cell_state,),
+        scratch=(pltpu.SemaphoreType.DMA,),
     )
     incoming = exchanged(outgoing, "ep")
 
@@ -386,10 +384,8 @@
             pltpu.VMEM((seq_local, key_size), F32),
             pltpu.VMEM((seq_local, 1), F32),
         ],
-        (incoming, old_norm, old_max, gains),
+        (incoming, old_cell, old_norm, old_max, gains),
         scalars=(input_bias, forget_bias),
-        left=(cell_state,),
-        scratch=(pltpu.VMEM(cell_state.shape, F32), pltpu.SemaphoreType.DMA),
     )
 
     part_shape = pltpu.VMEM((seq_total, columns), BF16)
@@ -422,13 +418,10 @@
             exchanged(outbound, "ep"),
             second_gain.reshape(1, -1),
             expert_gate,
+            expert_up,
         ),
-        left=(expert_up, expert_down),
-        scratch=(
-            pltpu.VMEM(expert_up.shape, BF16),
-            pltpu.VMEM(expert_down.shape, BF16),
-            pltpu.SemaphoreType.DMA((2,)),
-        ),
+        left=(expert_down,),
+        scratch=(pltpu.VMEM(expert_down.shape, BF16), pltpu.SemaphoreType.DMA),
     )
     moe_terms = kernel_call(
         combine_kernel, "combine", part_shape, (table, exchanged(slot_out, "ep"))

time: 160 us -> 162 us (1.012)
  local copies, waits for them, and re-layouts: 1.21 us -> 3.21 us
    unnamed x12 -> x18, local copies, waits for them, and re-layouts: 1.21 us -> 3.21 us
where the time goes in v7:
time: 162 us; the launch traced here: 161 us
  blocking collectives  129 us (80%)
  waiting for transfers between devices  10.8 us (7%)
  starting transfers between devices  8.27 us (5%)
  Pallas kernels  7.43 us (5%)
  local copies, waits for them, and re-layouts  3.21 us (2%)
  other arithmetic  1.82 us (1%)
    all_to_all x4, blocking collectives, exchanged(): return lax.all_to_all(blocks, axis, split_axis=0, concat_axis=0, tiled=True)  111 us
    all_to_all x1, blocking collectives, swapped(): lax.all_to_all(blocks, 'tp', split_axis=0, concat_axis=0, tiled=True, axi...  17.9 us
    all_to_all x1, waiting for transfers between devices, swapped(): lax.all_to_all(blocks, 'tp', split_axis=0, concat_axis=0, tiled=True, axi...  8.45 us
    pallas_call x8, Pallas kernels, kernel_call(): pl.pallas_call(kernel, in_specs=[smem] * len(scalars) + [pl.BlockSpec(mem...  7.43 us
    all_to_all x1, starting transfers between devices, swapped(): lax.all_to_all(blocks, 'tp', split_axis=0, concat_axis=0, tiled=True, axi...  4.37 us
    ppermute x2, starting transfers between devices, from_other_core(): return lax.ppermute(array, 'tp', [(i, i ^ 1) for i in range(size)])  3.9 us
  transfers between devices with their start and end apart: 3, of which 3 were waited for; matrix products, arithmetic and copies ran while one was open for 1% of the time, Pallas kernels for 0%

profile of v7, /device:TPU:80, one launch (start us, length us, event | category | flops | bytes accessed | tf_op | source)
XLA Modules:
  0.0 160.9 jit_solution(17089551450786648579)
XLA Ops:
  0.6 2.2 %send_parts.1 = (bf16[16,8,768]{2,1,0:T(8,128)(2,1)S(1)}, f32[1,6]{1,0:T(1,128)S(1)}, f32[6,1,128]{2,1,0:T(1,128)S(1)}, f32[1,4096]{1,0:T(1,128)S(1)}, s32[2,96]...) custom-call(f32[6,1,128,256]{3,2,1,0:T(8,128)} %cell_hbm.1, bf16[96,128]{1,0:T(8,128)(2,1)} %tok_ref.3, ...), custom_call_target="tpu_custom_call" | custom-call | tf_op jit(solution)/shard_map/send_parts/pallas_call | solution.py:307
  2.8 0.0 copy-start.2
  2.9 0.9 copy-done.2
  3.7 59.8 %all_to_all.30.got_ref = bf16[16,8,768]{2,1,0:T(8,128)(2,1)S(1)} all-to-all(bf16[16,8,768]{2,1,0:T(8,128)(2,1)S(1)} %get-tuple-element.26), channel_id=1, replica_groups=mesh['grp'=2,'ep'=16,'tp'=16] {'ep'}, dimensions={0} | all-to-all | bytes 393216 | tf_op jit(solution)/shard_map/all_to_all | solution.py:21
  63.5 1.1 copy-done.3
  64.7 1.7 %cell_step.1 = (bf16[16,8,256]{2,1,0:T(8,128)(2,1)S(1)}, f32[6,1]{1,0:T(8,128)S(1)}, f32[6,128]{1,0:T(8,128)S(1)}, f32[6,256]{1,0:T(8,128)S(1)}, f32[6,128]{1,0:T(8,128)S(1)}, /*index=5*/f32[6,1]{1,0:T(8,128)S(1)}) custom-call(f32[16]{0:T(128)} %in_bias.1, f32[16]{0:T(128)} %for_bias.1, bf16[16,8,768]{2,1,0:T(8,128)(2,1)S(1)} %all_to_all.30.got_ref, ...), custom_call_target="tpu_custom_call" | custom-call | tf_op jit(solution)/shard_map/cell_step/pallas_call | solution.py:307
  66.4 17.5 %all_to_all.31.got_ref = bf16[16,8,256]{2,1,0:T(8,128)(2,1)S(1)} all-to-all(bf16[16,8,256]{2,1,0:T(8,128)(2,1)S(1)} %get-tuple-element.31), channel_id=1, replica_groups=mesh['grp'=2,'ep'=16,'tp'=16] {'ep'}, dimensions={0} | all-to-all | bytes 131072 | tf_op jit(solution)/shard_map/all_to_all | solution.py:21
  83.9 0.0 copy-done.5
  83.9 0.3 project_heads.1.own_ref
  84.2 2.0 %collective-permute-start = (bf16[96,128]{1,0:T(8,128)(2,1)S(1)}, bf16[96,128]{1,0:T(8,128)(2,1)S(1)}, u32[]{:S(2)}, u32[]{:S(2)}) collective-permute-start(bf16[96,128]{1,0:T(8,128)(2,1)S(1)} %project_heads.1.own_ref), channel_id=1, source_target_pairs={{0,1},{1,0},{2,3},{3,2},{4,5},{5,4},{6,7},{7,6},{8,9},{9,8},{10,11... | collective-permute-start | bytes 73736 | tf_op jit(solution)/shard_map/ppermute | solution.py:26
  86.1 1.2 collective-permute-done.other_ref
  87.3 17.9 %all_to_all.32.got_ref = bf16[8,96,128]{2,1,0:T(8,128)(2,1)S(1)} all-to-all(bf16[8,96,128]{2,1,0:T(8,128)(2,1)S(1)} %chip_heads.1), channel_id=1, replica_groups={{0,2,4,6,8,10,12,14},{1,3,5,7,9,11,13,15},{16,18,20,22,24,26,28,30},{17..., dimensions={0} | all-to-all | bytes 393216 | tf_op jit(solution)/shard_map/all_to_all | solution.py:35
  105.2 0.0 copy-done.4
  105.2 0.4 stream_rows.1
  105.6 0.0 copy-start.6
  105.7 17.1 %all_to_all.33.got_ref = bf16[16,32,128]{2,1,0:T(8,128)(2,1)S(1)} all-to-all(bf16[16,32,128]{2,1,0:T(8,128)(2,1)S(1)} %get-tuple-element.36), channel_id=1, replica_groups=mesh['grp'=2,'ep'=16,'tp'=16] {'ep'}, dimensions={0} | all-to-all | bytes 262144 | tf_op jit(solution)/shard_map/all_to_all | solution.py:21
  122.7 0.0 copy-done
  122.7 0.0 copy-done.6
  122.7 1.9 %expert.1 = bf16[16,32,128]{2,1,0:T(8,128)(2,1)S(1)} custom-call(bf16[1,256,2048]{2,1,0:T(8,128)(2,1)} %down_hbm.1, bf16[16,32,128]{2,1,0:T(8,128)(2,1)S(1)} %all_to_all.33.got_ref, f32[1,2048]{1,0:T(1,128)S(1)} %bitcast.9, bf16[1,2048,256]{2,1,0:T(8,128)(2,1)S(1)} %copy-done, bf16[1,2048,256]{2,1,0:T(8,128)(2,1)S(1)} %copy-done.1), custom_call_target="tpu_custom_call" | custom-call | tf_op jit(solution)/shard_map/expert/pallas_call | solution.py:307
  124.7 0.0 copy-start.7
  124.7 16.4 %all_to_all.34.back_ref = bf16[16,32,128]{2,1,0:T(8,128)(2,1)S(1)} all-to-all(bf16[16,32,128]{2,1,0:T(8,128)(2,1)S(1)} %expert.1), channel_id=1, replica_groups=mesh['grp'=2,'ep'=16,'tp'=16] {'ep'}, dimensions={0} | all-to-all | bytes 262144 | tf_op jit(solution)/shard_map/all_to_all | solution.py:21
  141.0 0.2 combine.1.own_ref
  141.2 2.0 %collective-permute-start.1 = (bf16[96,128]{1,0:T(8,128)(2,1)S(1)}, bf16[96,128]{1,0:T(8,128)(2,1)S(1)}, u32[]{:S(2)}, u32[]{:S(2)}) collective-permute-start(bf16[96,128]{1,0:T(8,128)(2,1)S(1)} %combine.1.own_ref), channel_id=1, source_target_pairs={{0,1},{1,0},{2,3},{3,2},{4,5},{5,4},{6,7},{7,6},{8,9},{9,8},{10,11... | collective-permute-start | bytes 73736 | tf_op jit(solution)/shard_map/ppermute | solution.py:26
  143.2 1.2 collective-permute-done.1.other_ref
  144.4 0.7 chip_moe.1
  145.0 4.4 %all-to-all-start.5 = ((bf16[8,96,128]{2,1,0:T(8,128)(2,1)}), bf16[8,96,128]{2,1,0:T(8,128)(2,1)S(1)}, u32[]{:S(2)}, u32[]{:S(2)}) async-start(bf16[8,96,128]{2,1,0:T(8,128)(2,1)} %chip_moe.1), calls=%async_computation.5 | async-start | bytes 393216 | tf_op jit(solution)/shard_map/all_to_all | solution.py:35
  149.4 0.6 copy.28
  150.0 0.6 copy.27
  150.6 0.1 reduce
  150.7 1.1 multiply_add_fusion
  151.8 8.4 %all-to-all-done.5 = bf16[8,96,128]{2,1,0:T(8,128)(2,1)S(1)} async-done(((bf16[8,96,128]{2,1,0:T(8,128)(2,1)}), bf16[8,96,128]{2,1,0:T(8,128)(2,1)S(1)}, u32[]{:S(2)}, u32[]{:S(2)}) %all-to-all-start.5) | async-done | bytes 196640 | tf_op jit(solution)/shard_map/all_to_all | solution.py:35
  160.3 0.6 add_convert_fusion
  (9 shorter events, 0.1 us)
Async XLA Ops:
  2.8 0.9 copy-start.2
  3.7 80.2 %copy-start.5 = (bf16[256,128]{1,0:T(8,128)(2,1)S(1)}, bf16[256,128]{1,0:T(8,128)(2,1)}, u32[]{:S(2)}) copy-start(bf16[256,128]{1,0:T(8,128)(2,1)} %weight_ref.1) | copy-start | bytes 196612
  3.7 101.5 %copy-start.4 = (bf16[96,128]{1,0:T(8,128)(2,1)S(1)}, bf16[96,128]{1,0:T(8,128)(2,1)}, u32[]{:S(2)}) copy-start(bf16[96,128]{1,0:T(8,128)(2,1)} %tok_ref.3) | copy-start | bytes 73732
  63.5 1.1 copy-start.3
  64.7 58.1 %copy-start = (bf16[1,2048,256]{2,1,0:T(8,128)(2,1)S(1)}, bf16[1,2048,256]{2,1,0:T(8,128)(2,1)}, u32[]{:S(2)}) copy-start(bf16[1,2048,256]{2,1,0:T(8,128)(2,1)} %gate_ref.1) | copy-start | bytes 3145732
  64.7 58.1 %copy-start.1 = (bf16[1,2048,256]{2,1,0:T(8,128)(2,1)S(1)}, bf16[1,2048,256]{2,1,0:T(8,128)(2,1)}, u32[]{:S(2)}) copy-start(bf16[1,2048,256]{2,1,0:T(8,128)(2,1)} %up_ref.1) | copy-start | bytes 3145732
  84.2 3.1 %collective-permute-start = (bf16[96,128]{1,0:T(8,128)(2,1)S(1)}, bf16[96,128]{1,0:T(8,128)(2,1)S(1)}, u32[]{:S(2)}, u32[]{:S(2)}) collective-permute-start(bf16[96,128]{1,0:T(8,128)(2,1)S(1)} %project_heads.1.own_ref), channel_id=1, source_target_pairs={{0,1},{1,0},{2,3},{3,2},{4,5},{5,4},{6,7},{7,6},{8,9},{9,8},{10,11... | collective-permute-start | bytes 73736 | tf_op jit(solution)/shard_map/ppermute | solution.py:26
  105.6 17.1 %copy-start.6 = (f32[2048]{0:T(1024)S(1)}, f32[2048]{0:T(1024)}, u32[]{:S(2)}) copy-start(f32[2048]{0:T(1024)} %param.36) | copy-start | bytes 24580
  124.7 26.1 %copy-start.7 = (f32[6,1,128,256]{3,2,1,0:T(8,128)S(1)}, f32[6,1,128,256]{3,2,1,0:T(8,128)}, u32[]{:S(2)}) copy-start(f32[6,1,128,256]{3,2,1,0:T(8,128)} %cell_hbm.1) | copy-start | bytes 2359300
  141.2 3.1 %collective-permute-start.1 = (bf16[96,128]{1,0:T(8,128)(2,1)S(1)}, bf16[96,128]{1,0:T(8,128)(2,1)S(1)}, u32[]{:S(2)}, u32[]{:S(2)}) collective-permute-start(bf16[96,128]{1,0:T(8,128)(2,1)S(1)} %combine.1.own_ref), channel_id=1, source_target_pairs={{0,1},{1,0},{2,3},{3,2},{4,5},{5,4},{6,7},{7,6},{8,9},{9,8},{10,11... | collective-permute-start | bytes 73736 | tf_op jit(solution)/shard_map/ppermute | solution.py:26
  145.0 15.2 %all-to-all-start.5 = ((bf16[8,96,128]{2,1,0:T(8,128)(2,1)}), bf16[8,96,128]{2,1,0:T(8,128)(2,1)S(1)}, u32[]{:S(2)}, u32[]{:S(2)}) async-start(bf16[8,96,128]{2,1,0:T(8,128)(2,1)} %chip_moe.1), calls=%async_computation.5 | async-start | bytes 393216 | tf_op jit(solution)/shard_map/all_to_all | solution.py:35

commit v8 on v0

--- a/solution.py
+++ b/solution.py
@@ -1,13 +1,66 @@
+import functools
+
 import jax
 import jax.numpy as jnp
 from jax import lax
+from jax.experimental import pallas as pl
+from jax.experimental.pallas import tpu as pltpu
 from jax.sharding import PartitionSpec as P
-
-EXP_DEV = 1
-
 
 NORM_EPS = 1e-05
 HEAD_EPS = 1e-06
+CAPACITY = 2
+LANES = 128
+PADDED = 8
+GATE_SUMS = 16
+F32 = jnp.float32
+BF16 = jnp.bfloat16
+
+
+def exchanged(blocks, axis):
+    return lax.all_to_all(blocks, axis, split_axis=0, concat_axis=0, tiled=True)
+
+
+def from_other_core(array):
+    size = lax.axis_size("tp")
+    return lax.ppermute(array, "tp", [(i, i ^ 1) for i in range(size)])
+
+
+def chips_of_cores(axis):
+    size = lax.axis_size(axis)
+    return [list(range(core, size, 2)) for core in range(2)]
+
+
+def swapped(blocks, groups):
+    return lax.all_to_all(
+        blocks, "tp", split_axis=0, concat_axis=0, tiled=True, axis_index_groups=groups
+    )
+
+
+def rounded_pieces(values, count):
+    pieces = []
+    for _ in range(count):
+        head = values.astype(BF16).astype(F32)
+        pieces.append(head)
+        values = values - head
+    return pieces
+
+
+def dot(a, b):
+    return jnp.dot(a, b, preferred_element_type=F32)
+
+
+def lane_sums(values, count):
+    ones = jnp.ones((values.shape[1], LANES), BF16)
+    return sum(dot(piece.astype(BF16), ones) for piece in rounded_pieces(values, count))
+
+
+def grid_index(shape):
+    return lax.broadcasted_iota(jnp.int32, shape, 0), lax.broadcasted_iota(jnp.int32, shape, 1)
+
+
+def one_hot(condition):
+    return jnp.where(condition, 1.0, 0.0).astype(BF16)
 
 
 def from_everyone(array, axis):
@@ -34,12 +87,6 @@
     lengths = array.shape
     blocks = array.reshape(*lengths[:dim], peers, lengths[dim] // peers, *lengths[dim + 1 :])
     return jnp.moveaxis(blocks, dim, 0)
-
-
-def summed_on_arrival(array, axis, dim):
-    blocks = cut_along(array, dim, lax.axis_size(axis))
-    arrived = lax.all_to_all(blocks, axis, split_axis=0, concat_axis=0, tiled=True)
-    return arrived.astype(jnp.float32).sum(axis=0)
 
 
 def summed_on_arrival_2(array, axis, dim):
@@ -55,21 +102,6 @@
         ends.append(at)
     both = jnp.concatenate(arrays, axis=along)
     return tuple(jnp.split(summed_on_arrival_2(both, axis, dim), ends, axis=along))
-
-
-def joined_along(blocks, dim):
-    lengths = list(blocks.shape[1:])
-    lengths[dim] *= blocks.shape[0]
-    return jnp.moveaxis(blocks, 0, dim).reshape(lengths)
-
-
-def gather_directly(array, axis, dim):
-    return joined_along(from_everyone(array, axis), dim)
-
-
-def gathered_total(array, axis):
-    blocks = lax.all_gather(array, axis)
-    return blocks.sum(axis=0)
 
 
 def row_norm(stream_rows, gain_whole):
@@ -84,19 +116,105 @@
     return ((values - row_mean[:, None]) * inv_scale[:, None] * gain_cols).astype(jnp.bfloat16)
 
 
-def expert_act(gate_sum, up_sum):
-    return (jax.nn.silu(gate_sum) * up_sum).astype(jnp.bfloat16)
-
-
-def scatter_slots(active, expert_down):
-    slot_major = jnp.moveaxis(active, 1, 0)
-    return summed_on_arrival(
-        jnp.einsum(
-            "pef,efd->ped", slot_major, expert_down, preferred_element_type=jnp.float32
-        ).astype(jnp.bfloat16),
-        "tp",
-        0,
-    ).astype(jnp.bfloat16)
+def project_kernel(got_ref, weight_ref, out_ref, *, seq_local):
+    blocks, padded, width = got_ref.shape
+    seq_total = out_ref.shape[0]
+    rows = got_ref[...].astype(F32).reshape(blocks * padded, width).astype(BF16)
+    terms = dot(rows, weight_ref[...]).astype(BF16)
+    row, col = grid_index((seq_total, blocks * padded))
+    inner = col & (PADDED - 1)
+    packed = dot(one_hot((inner < seq_local) & (row == (col >> 3) * seq_local + inner)), terms)
+    out_ref[...] = packed.astype(BF16)
+
+
+def pair_kernel(own_ref, other_ref, out_ref):
+    added = (own_ref[...].astype(F32) + other_ref[...].astype(F32)).astype(BF16)
+    out_ref[...] = jnp.broadcast_to(added[None], out_ref.shape)
+
+
+def column_of(row):
+    down, across = grid_index((row.shape[1], row.shape[1]))
+    return jnp.sum(jnp.where(down == across, row, 0.0), axis=1, keepdims=True)
+
+
+def stream_kernel(
+    got_ref, tok_ref, route_ref, weight_ref, stream_ref, out_ref, table_ref, *, seq_local
+):
+    mixer_out = jnp.sum(got_ref[...].astype(F32), axis=0)
+    stream = (tok_ref[...].astype(F32) + mixer_out).astype(BF16)
+    stream_ref[...] = stream
+    top, seq_total = route_ref.shape
+    experts, slots, _ = out_ref.shape
+    names = [route_ref[k : k + 1].astype(F32) for k in range(top)]
+    down, across = grid_index((seq_total, seq_total))
+    block_down = jnp.floor((down.astype(F32) + 0.5) * (1.0 / seq_local))
+    block_across = jnp.floor((across.astype(F32) + 0.5) * (1.0 / seq_local))
+    earlier = (block_down == block_across) & (across < down)
+    place = lax.broadcasted_iota(jnp.int32, (seq_total, experts * slots), 1).astype(F32)
+    picked = jnp.zeros(place.shape, F32)
+    weights = jnp.zeros(place.shape, F32)
+    for k in range(top):
+        name = column_of(names[k])
+        same = sum(jnp.where(earlier & (other == name), 1.0, 0.0) for other in names)
+        slot = name * slots + block_down[:, :1] * CAPACITY + jnp.sum(same, axis=1, keepdims=True)
+        here = place == slot
+        picked = jnp.where(here, 1.0, picked)
+        weights = jnp.where(here, column_of(weight_ref[k : k + 1]), weights)
+    table = [piece.astype(BF16) for piece in rounded_pieces(weights, 2)]
+    table_ref[...] = jnp.concatenate(table, axis=0)
+    chosen = lax.dot_general(
+        picked.astype(BF16), stream, (((0,), (0,)), ((), ())), preferred_element_type=F32
+    )
+    out_ref[...] = chosen.astype(BF16).reshape(out_ref.shape)
+
+
+def expert_kernel(
+    up_hbm, down_hbm, got_ref, gain_ref, gate_ref, out_ref, up_ref, down_ref, arrived
+):
+    fetches = [
+        pltpu.make_async_copy(up_hbm, up_ref, arrived.at[0]),
+        pltpu.make_async_copy(down_hbm, down_ref, arrived.at[1]),
+    ]
+    for fetch in fetches:
+        fetch.start()
+    blocks, _, columns = got_ref.shape
+    values = jnp.concatenate([got_ref[e].astype(F32) for e in range(blocks)], axis=1)
+    row_mean = jnp.mean(values, axis=1, keepdims=True)
+    spread = jnp.mean(values * values, axis=1, keepdims=True) - row_mean * row_mean
+    normed = ((values - row_mean) * lax.rsqrt(spread + NORM_EPS) * gain_ref[...]).astype(BF16)
+    gate = dot(normed, gate_ref[0])
+    fetches[0].wait()
+    active = (gate / (1.0 + jnp.exp(-gate)) * dot(normed, up_ref[0])).astype(BF16)
+    fetches[1].wait()
+    result = dot(active, down_ref[0]).astype(BF16)
+    for e in range(blocks):
+        out_ref[e] = result[:, e * columns : (e + 1) * columns]
+
+
+def combine_kernel(table_ref, back_ref, out_ref):
+    seq_total = out_ref.shape[0]
+    experts, slots, columns = back_ref.shape
+    both = dot(table_ref[...], back_ref[...].reshape(experts * slots, columns))
+    out_ref[...] = (both[:seq_total] + both[seq_total:]).astype(BF16)
+
+
+def in_vmem(array):
+    return pltpu.with_memory_space_constraint(array, pltpu.VMEM)
+
+
+def kernel_call(kernel, name, shapes, near, scalars=(), far=(), left=(), scratch=()):
+    vmem = pl.BlockSpec(memory_space=pltpu.VMEM)
+    smem = pl.BlockSpec(memory_space=pltpu.SMEM)
+    return pl.pallas_call(
+        kernel,
+        in_specs=[smem] * len(scalars)
+        + [pl.BlockSpec(memory_space=pl.ANY)] * len(left)
+        + [vmem] * (len(far) + len(near)),
+        out_specs=jax.tree.map(lambda _: vmem, shapes),
+        out_shape=shapes,
+        scratch_shapes=scratch,
+        name=name,
+    )(*scalars, *left, *far, *(in_vmem(a) for a in near))
 
 
 def on_device(
@@ -123,8 +241,7 @@
     expert_down,
 ):
     blocks = lax.axis_size("ep")
-    columns = tokens.shape[1]
-    seq_total = tokens.shape[0]
+    seq_total, columns = tokens.shape
     seq_local = seq_total // blocks
     heads_local = cell_state.shape[1]
     key_size = cell_state.shape[2]
@@ -181,44 +298,56 @@
         * gains_here
         * jax.nn.sigmoid(outgate.astype(jnp.float32))
     ).astype(jnp.bfloat16)
-    head_terms = jnp.dot(
-        gather_directly(mixed_heads, "ep", 0), w_project, preferred_element_type=jnp.float32
-    )
-    mixer_out = gathered_total(head_terms, "tp")
-    stream = (tokens.astype(jnp.float32) + mixer_out).astype(jnp.bfloat16)
-    second_normed = row_norm(stream, second_gain)
-    experts = blocks * EXP_DEV
-    top_count = routes.shape[1]
-    capacity = max(2, 2 * seq_local * top_count // experts)
-    slot_count = blocks * capacity
-    expert_ids = lax.broadcasted_iota(jnp.int32, (1, 1, experts), 2)
-    matches = routes[:, :, None] == expert_ids
-    routed = jnp.sum(matches.astype(jnp.int32), axis=1)
-    combine = jnp.sum(jnp.where(matches, route_weight[:, :, None], 0.0), axis=1)
-    running = (
-        jnp.cumsum(routed.reshape(blocks, seq_local, experts), axis=1).reshape(seq_total, experts)
-        - routed
-    )
-    block_ids = lax.broadcasted_iota(jnp.int32, (seq_total, experts), 0) // seq_local
-    slot_of = block_ids * capacity + running
-    slot_ids = lax.broadcasted_iota(jnp.int32, (experts, slot_count, seq_total), 1)
-    placed = (slot_of.T[:, None, :] == slot_ids) & (routed.T[:, None, :] > 0)
-    picker = placed.astype(jnp.bfloat16)
-    weighted = jnp.where(placed, combine.T[:, None, :], 0.0)
-    outbound = jnp.einsum(
-        "eps,sd->epd", picker, second_normed, preferred_element_type=jnp.float32
-    ).astype(jnp.bfloat16)
-    arrived = lax.all_to_all(outbound, "ep", split_axis=0, concat_axis=2, tiled=True)
-    gate_sum = jnp.einsum("end,edf->enf", arrived, expert_gate, preferred_element_type=jnp.float32)
-    up_sum = jnp.einsum("end,edf->enf", arrived, expert_up, preferred_element_type=jnp.float32)
-    active = expert_act(gate_sum, up_sum)
-    share = scatter_slots(active, expert_down)
-    back = lax.all_to_all(share, "ep", split_axis=2, concat_axis=1, tiled=True)
-    every_slot = gather_directly(back, "tp", 0)
-    moe_out = jnp.einsum(
-        "eps,ped->sd", weighted, every_slot.astype(jnp.float32), precision=lax.Precision.HIGHEST
-    )
-    layer_out = (stream.astype(jnp.float32) + moe_out).astype(jnp.bfloat16)
+    experts = blocks
+    slot_count = blocks * CAPACITY
+    padded = jnp.pad(mixed_heads, ((0, PADDED - seq_local), (0, 0)))
+    mixed = jnp.broadcast_to(padded[None], (blocks, PADDED, value_size))
+    part_shape = pltpu.VMEM((seq_total, columns), BF16)
+    chip_shape = pltpu.VMEM((lax.axis_size("tp") // 2, seq_total, columns), BF16)
+    head_terms = kernel_call(
+        functools.partial(project_kernel, seq_local=seq_local),
+        "project_heads",
+        part_shape,
+        (exchanged(mixed, "ep"), w_project),
+    )
+    chip_terms = kernel_call(
+        pair_kernel, "chip_heads", chip_shape, (head_terms, from_other_core(head_terms))
+    )
+    stream, outbound, table = kernel_call(
+        functools.partial(stream_kernel, seq_local=seq_local),
+        "stream_rows",
+        [
+            pltpu.VMEM(tokens.shape, BF16),
+            pltpu.VMEM((experts, slot_count, columns), BF16),
+            pltpu.VMEM((2 * seq_total, experts * slot_count), BF16),
+        ],
+        (swapped(chip_terms, chips_of_cores("tp")), tokens, routes.T, route_weight.T),
+    )
+
+    slot_out = kernel_call(
+        expert_kernel,
+        "expert",
+        pltpu.VMEM((blocks, slot_count, columns), BF16),
+        (
+            exchanged(outbound, "ep"),
+            second_gain.reshape(1, -1),
+            expert_gate,
+        ),
+        left=(expert_up, expert_down),
+        scratch=(
+            pltpu.VMEM(expert_up.shape, BF16),
+            pltpu.VMEM(expert_down.shape, BF16),
+            pltpu.SemaphoreType.DMA((2,)),
+        ),
+    )
+    moe_terms = kernel_call(
+        combine_kernel, "combine", part_shape, (table, exchanged(slot_out, "ep"))
+    )
+    moe_terms = kernel_call(
+        pair_kernel, "chip_moe", chip_shape, (moe_terms, from_other_core(moe_terms))
+    )
+    moe_out = jnp.sum(swapped(moe_terms, chips_of_cores("tp")).astype(F32), axis=0)
+    layer_out = (stream.astype(F32) + moe_out).astype(BF16)
     return (layer_out, new_cell, new_norm, new_max)
 
 

time: 234 us -> 194 us (0.83)
  waiting for transfers between devices: 62.8 us -> 44.7 us
  other arithmetic: 15.6 us -> 4.1 us
  local copies, waits for them, and re-layouts: 17.4 us -> 9.85 us
  starting transfers between devices: 63 us -> 56 us
  blocking collectives: 66 us -> 70.9 us
  Pallas kernels: 0 us -> 3.5 us
  matrix products: 5.14 us -> 2.77 us
    all_to_all x4 -> x1, waiting for transfers between devices: 42.3 us -> 11.5 us  [from_everyone(): lax.all_to_all(jnp.broadcast_to(array[None], (peers, *array.shape)), axis...]
    all_to_all x3 -> x4, blocking collectives: 45.9 us -> 70.9 us  [the longest x3 53 us: exchanged(): return lax.all_to_all(blocks, axis, split_axis=0, concat_axis=0, tiled=True)]
    all_gather x1 -> x0, blocking collectives: 20.2 us -> none  [gathered_total(): blocks = lax.all_gather(array, axis)]
    all_to_all x4 -> x1, starting transfers between devices: 58.9 us -> 43.7 us  [from_everyone(): lax.all_to_all(jnp.broadcast_to(array[None], (peers, *array.shape)), axis...]
    unnamed x1 -> x0, other arithmetic: 11.5 us -> none
    all_to_all x0 -> x1, waiting for transfers between devices: none -> 9.46 us  [swapped(): lax.all_to_all(blocks, 'tp', split_axis=0, concat_axis=0, tiled=True, axi...]
    all_to_all x0 -> x1, starting transfers between devices: none -> 4.23 us  [swapped(): lax.all_to_all(blocks, 'tp', split_axis=0, concat_axis=0, tiled=True, axi...]
    ppermute x0 -> x2, starting transfers between devices: none -> 3.9 us  [from_other_core(): return lax.ppermute(array, 'tp', [(i, i ^ 1) for i in range(size)])]
where the time goes in v8:
time: 194 us; the launch traced here: 193 us
  blocking collectives  70.9 us (37%)
  starting transfers between devices  56 us (29%)
  waiting for transfers between devices  44.7 us (23%)
  local copies, waits for them, and re-layouts  9.85 us (5%)
  other arithmetic  4.1 us (2%)
  Pallas kernels  3.5 us (2%)
  matrix products  2.77 us (1%)
    all_to_all x3, blocking collectives, exchanged(): return lax.all_to_all(blocks, axis, split_axis=0, concat_axis=0, tiled=True)  53 us
    all_to_all x1, starting transfers between devices, from_everyone(): lax.all_to_all(jnp.broadcast_to(array[None], (peers, *array.shape)), axis...  43.7 us
    all_to_all x1, waiting for transfers between devices, summed_on_arrival_2(): lax.all_to_all(blocks, axis, split_axis=0, concat_axis=0, tiled=True)  21.4 us
    all_to_all x1, blocking collectives, swapped(): lax.all_to_all(blocks, 'tp', split_axis=0, concat_axis=0, tiled=True, axi...  17.9 us
    all_to_all x1, waiting for transfers between devices, from_everyone(): lax.all_to_all(jnp.broadcast_to(array[None], (peers, *array.shape)), axis...  11.5 us
    all_to_all x1, waiting for transfers between devices, swapped(): lax.all_to_all(blocks, 'tp', split_axis=0, concat_axis=0, tiled=True, axi...  9.46 us
    unnamed x35, local copies, waits for them, and re-layouts  5.1 us
    all_to_all x1, starting transfers between devices, swapped(): lax.all_to_all(blocks, 'tp', split_axis=0, concat_axis=0, tiled=True, axi...  4.23 us
  transfers between devices with their start and end apart: 5, of which 5 were waited for; matrix products, arithmetic and copies ran while one was open for 2% of the time, Pallas kernels for 0%

profile of v8, /device:TPU:80, one launch (start us, length us, event | category | flops | bytes accessed | tf_op | source)
XLA Modules:
  0.0 192.6 jit_solution(9556450271002648326)
XLA Ops:
  0.6 0.9 convert_reduce_fusion.1
  1.6 0.6 broadcast_in_dim.4
  2.2 43.7 %all-to-all-start = ((f32[16,1,192]{2,1,0:T(1,128)}), f32[16,1,192]{2,1,0:T(1,128)S(1)}, u32[]{:S(2)}, u32[]{:S(2)}) async-start(f32[16,1,192]{2,1,0:T(1,128)} %broadcast_in_dim.4), calls=%async_computation | async-start | bytes 32768 | tf_op jit(solution)/shard_map/all_to_all | solution.py:68
  45.9 0.8 dynamic_slice.18
  46.7 11.5 %all-to-all-done = f32[16,1,192]{2,1,0:T(1,128)S(1)} async-done(((f32[16,1,192]{2,1,0:T(1,128)}), f32[16,1,192]{2,1,0:T(1,128)S(1)}, u32[]{:S(2)}, u32[]{:S(2)}) %all-to-all-start) | async-done | bytes 12320 | tf_op jit(solution)/shard_map/all_to_all | solution.py:68
  58.5 0.9 fusion.6
  59.5 0.9 fusion.8
  60.5 0.6 copy-done.10
  61.3 0.7 copy-done.11
  62.6 0.8 copy-done.9
  63.6 0.9 concatenate.20
  64.4 4.1 %all-to-all-start.1 = ((f32[16,6,770]{2,1,0:T(8,128)}), f32[16,6,770]{2,1,0:T(8,128)S(1)}, u32[]{:S(2)}, u32[]{:S(2)}) async-start(f32[16,6,770]{2,1,0:T(8,128)} %concatenate.20), calls=%async_computation.1 | async-start | bytes 917504 | tf_op jit(solution)/shard_map/all_to_all | solution.py:94
  68.6 0.6 copy-done.14
  70.6 0.8 dynamic_slice.23
  71.4 21.4 %all-to-all-done.1 = f32[16,6,770]{2,1,0:T(8,128)S(1)} async-done(((f32[16,6,770]{2,1,0:T(8,128)}), f32[16,6,770]{2,1,0:T(8,128)S(1)}, u32[]{:S(2)}, u32[]{:S(2)}) %all-to-all-start.1) | async-done | bytes 295712 | tf_op jit(solution)/shard_map/all_to_all | solution.py:94
  92.8 1.5 exponential_reduce_fusion.1
  95.6 19.5 %all_to_all.36.got_ref = bf16[16,8,256]{2,1,0:T(8,128)(2,1)S(1)} all-to-all(bf16[16,8,256]{2,1,0:T(8,128)(2,1)S(1)} %broadcast_in_dim.5), channel_id=1, replica_groups=mesh['grp'=2,'ep'=16,'tp'=16] {'ep'}, dimensions={0} | all-to-all | bytes 131072 | tf_op jit(solution)/shard_map/all_to_all | solution.py:21
  115.4 2.0 %collective-permute-start = (bf16[96,128]{1,0:T(8,128)(2,1)S(1)}, bf16[96,128]{1,0:T(8,128)(2,1)S(1)}, u32[]{:S(2)}, u32[]{:S(2)}) collective-permute-start(bf16[96,128]{1,0:T(8,128)(2,1)S(1)} %project_heads.1.own_ref), channel_id=1, source_target_pairs={{0,1},{1,0},{2,3},{3,2},{4,5},{5,4},{6,7},{7,6},{8,9},{9,8},{10,11... | collective-permute-start | bytes 73736 | tf_op jit(solution)/shard_map/ppermute | solution.py:26
  117.3 1.2 collective-permute-done.other_ref
  118.5 17.9 %all_to_all.37.got_ref = bf16[8,96,128]{2,1,0:T(8,128)(2,1)S(1)} all-to-all(bf16[8,96,128]{2,1,0:T(8,128)(2,1)S(1)} %chip_heads.1), channel_id=1, replica_groups={{0,2,4,6,8,10,12,14},{1,3,5,7,9,11,13,15},{16,18,20,22,24,26,28,30},{17..., dimensions={0} | all-to-all | bytes 393216 | tf_op jit(solution)/shard_map/all_to_all | solution.py:35
  136.4 0.7 copy-done.5
  137.5 17.0 %all_to_all.38.got_ref = bf16[16,32,128]{2,1,0:T(8,128)(2,1)S(1)} all-to-all(bf16[16,32,128]{2,1,0:T(8,128)(2,1)S(1)} %get-tuple-element.9), channel_id=1, replica_groups=mesh['grp'=2,'ep'=16,'tp'=16] {'ep'}, dimensions={0} | all-to-all | bytes 262144 | tf_op jit(solution)/shard_map/all_to_all | solution.py:21
  154.5 1.9 %expert.1 = bf16[16,32,128]{2,1,0:T(8,128)(2,1)S(1)} custom-call(bf16[1,2048,256]{2,1,0:T(8,128)(2,1)} %up_hbm.1, bf16[1,256,2048]{2,1,0:T(8,128)(2,1)} %down_hbm.1, bf16[16,32,128]{2,1,0:T(8,128)(2,1)S(1)} %all_to_all.38.got_ref, f32[1,2048]{1,0:T(1,128)S(1)} %bitcast.49, bf16[1,2048,256]{2,1,0:T(8,128)(2,1)S(1)} %copy-done.1), custom_call_target="tpu_custom_call" | custom-call | tf_op jit(solution)/shard_map/expert/pallas_call | solution.py:208
  156.4 16.5 %all_to_all.39.back_ref = bf16[16,32,128]{2,1,0:T(8,128)(2,1)S(1)} all-to-all(bf16[16,32,128]{2,1,0:T(8,128)(2,1)S(1)} %expert.1), channel_id=1, replica_groups=mesh['grp'=2,'ep'=16,'tp'=16] {'ep'}, dimensions={0} | all-to-all | bytes 262144 | tf_op jit(solution)/shard_map/all_to_all | solution.py:21
  173.1 2.0 %collective-permute-start.1 = (bf16[96,128]{1,0:T(8,128)(2,1)S(1)}, bf16[96,128]{1,0:T(8,128)(2,1)S(1)}, u32[]{:S(2)}, u32[]{:S(2)}) collective-permute-start(bf16[96,128]{1,0:T(8,128)(2,1)S(1)} %combine.1.own_ref), channel_id=1, source_target_pairs={{0,1},{1,0},{2,3},{3,2},{4,5},{5,4},{6,7},{7,6},{8,9},{9,8},{10,11... | collective-permute-start | bytes 73736 | tf_op jit(solution)/shard_map/ppermute | solution.py:26
  175.1 1.2 collective-permute-done.1.other_ref
  176.2 0.7 chip_moe.1
  176.9 4.2 %all-to-all-start.6 = ((bf16[8,96,128]{2,1,0:T(8,128)(2,1)}), bf16[8,96,128]{2,1,0:T(8,128)(2,1)S(1)}, u32[]{:S(2)}, u32[]{:S(2)}) async-start(bf16[8,96,128]{2,1,0:T(8,128)(2,1)} %chip_moe.1), calls=%async_computation.6 | async-start | bytes 393216 | tf_op jit(solution)/shard_map/all_to_all | solution.py:35
  181.2 0.6 copy.65
  181.9 0.6 copy.64
  182.5 9.5 %all-to-all-done.6 = bf16[8,96,128]{2,1,0:T(8,128)(2,1)S(1)} async-done(((bf16[8,96,128]{2,1,0:T(8,128)(2,1)}), bf16[8,96,128]{2,1,0:T(8,128)(2,1)S(1)}, u32[]{:S(2)}, u32[]{:S(2)}) %all-to-all-start.6) | async-done | bytes 196640 | tf_op jit(solution)/shard_map/all_to_all | solution.py:35
  192.0 0.6 add_convert_fusion
  (66 shorter events, 5.1 us)
Async XLA Ops:
  0.6 61.8 %copy-start = (bf16[128,256]{1,0:T(8,128)(2,1)S(1)}, bf16[128,256]{1,0:T(8,128)(2,1)}, u32[]{:S(2)}) copy-start(bf16[128,256]{1,0:T(8,128)(2,1)} %param.26) | copy-start | bytes 196612
  2.2 56.0 %all-to-all-start = ((f32[16,1,192]{2,1,0:T(1,128)}), f32[16,1,192]{2,1,0:T(1,128)S(1)}, u32[]{:S(2)}, u32[]{:S(2)}) async-start(f32[16,1,192]{2,1,0:T(1,128)} %broadcast_in_dim.4), calls=%async_computation | async-start | bytes 32768 | tf_op jit(solution)/shard_map/all_to_all | solution.py:68
  45.9 12.4 %copy-start.2 = (bf16[96,128]{1,0:T(8,128)(2,1)S(1)}, bf16[96,128]{1,0:T(8,128)(2,1)}, u32[]{:S(2)}) copy-start(bf16[96,128]{1,0:T(8,128)(2,1)} %tok_ref.1) | copy-start | bytes 73732
  60.3 0.8 copy-start.10
  61.2 0.8 copy-start.11
  62.6 0.9 copy-start.9
  64.4 30.0 %copy-start.8 = (f32[6,1,128,256]{3,2,1,0:T(8,128)S(1)}, f32[6,1,128,256]{3,2,1,0:T(8,128)}, u32[]{:S(2)}) copy-start(f32[6,1,128,256]{3,2,1,0:T(8,128)} %param.33) | copy-start | bytes 2359300
  64.4 28.3 %all-to-all-start.1 = ((f32[16,6,770]{2,1,0:T(8,128)}), f32[16,6,770]{2,1,0:T(8,128)S(1)}, u32[]{:S(2)}, u32[]{:S(2)}) async-start(f32[16,6,770]{2,1,0:T(8,128)} %concatenate.20), calls=%async_computation.1 | async-start | bytes 917504 | tf_op jit(solution)/shard_map/all_to_all | solution.py:94
  68.6 0.7 copy-start.14
  69.2 0.7 copy-start.15
  69.9 0.7 copy-start.13
  94.4 20.7 %copy-start.3 = (bf16[256,128]{1,0:T(8,128)(2,1)S(1)}, bf16[256,128]{1,0:T(8,128)(2,1)}, u32[]{:S(2)}) copy-start(bf16[256,128]{1,0:T(8,128)(2,1)} %weight_ref.1) | copy-start | bytes 196612
  94.6 41.8 %copy-start.7 = (f32[6,1,128,256]{3,2,1,0:T(8,128)}, f32[6,1,128,256]{3,2,1,0:T(8,128)S(1)}, u32[]{:S(2)}) copy-start(f32[6,1,128,256]{3,2,1,0:T(8,128)S(1)} %multiply_add_fusion) | copy-start | bytes 2359300
  94.6 59.9 %copy-start.1 = (bf16[1,2048,256]{2,1,0:T(8,128)(2,1)S(1)}, bf16[1,2048,256]{2,1,0:T(8,128)(2,1)}, u32[]{:S(2)}) copy-start(bf16[1,2048,256]{2,1,0:T(8,128)(2,1)} %gate_ref.1) | copy-start | bytes 3145732
  115.4 3.1 %collective-permute-start = (bf16[96,128]{1,0:T(8,128)(2,1)S(1)}, bf16[96,128]{1,0:T(8,128)(2,1)S(1)}, u32[]{:S(2)}, u32[]{:S(2)}) collective-permute-start(bf16[96,128]{1,0:T(8,128)(2,1)S(1)} %project_heads.1.own_ref), channel_id=1, source_target_pairs={{0,1},{1,0},{2,3},{3,2},{4,5},{5,4},{6,7},{7,6},{8,9},{9,8},{10,11... | collective-permute-start | bytes 73736 | tf_op jit(solution)/shard_map/ppermute | solution.py:26
  118.5 17.9 %copy-start.6 = (f32[96,2]{0,1:T(2,128)S(1)}, f32[96,2]{0,1:T(2,128)}, u32[]{:S(2)}) copy-start(f32[96,2]{0,1:T(2,128)} %param.38) | copy-start | bytes 2308
  136.4 0.7 copy-start.5
  137.5 17.0 %copy-start.4 = (f32[2048]{0:T(1024)S(1)}, f32[2048]{0:T(1024)}, u32[]{:S(2)}) copy-start(f32[2048]{0:T(1024)} %param.36) | copy-start | bytes 24580
  173.1 3.1 %collective-permute-start.1 = (bf16[96,128]{1,0:T(8,128)(2,1)S(1)}, bf16[96,128]{1,0:T(8,128)(2,1)S(1)}, u32[]{:S(2)}, u32[]{:S(2)}) collective-permute-start(bf16[96,128]{1,0:T(8,128)(2,1)S(1)} %combine.1.own_ref), channel_id=1, source_target_pairs={{0,1},{1,0},{2,3},{3,2},{4,5},{5,4},{6,7},{7,6},{8,9},{9,8},{10,11... | collective-permute-start | bytes 73736 | tf_op jit(solution)/shard_map/ppermute | solution.py:26
  176.9 15.0 %all-to-all-start.6 = ((bf16[8,96,128]{2,1,0:T(8,128)(2,1)}), bf16[8,96,128]{2,1,0:T(8,128)(2,1)S(1)}, u32[]{:S(2)}, u32[]{:S(2)}) async-start(bf16[8,96,128]{2,1,0:T(8,128)(2,1)} %chip_moe.1), calls=%async_computation.6 | async-start | bytes 393216 | tf_op jit(solution)/shard_map/all_to_all | solution.py:35
  181.2 0.7 copy-start.12
